TPU v7x, 256 devices: a whole 4x4x8 slice. The times are simulated.
256 devices in a mesh: sp: 64 (over z, x, core), tp: 4 (over y).
Axes of the slice: x: 4, y: 4, z: 8, core: 2. Of those that a mesh axis runs over, the one named last changes fastest.
Arguments:
- hidden_in: bfloat16 [16384, 2048], P('sp'), may hold values from -6 to 6
- cotangent: bfloat16 [16384, 2048], P('sp'), may hold values from -16 to 16
- routes: int32 [16384, 2], P('sp'), may hold values from 0 to 63, all different within a row; in each aligned block of 256 rows (0 to 255, 256 to 511, ...) at most 12 rows name the same one
- routing_weights: float32 [16384, 2], P('sp'), may hold values from 0.1 to 1
- w_gate: bfloat16 [64, 2048, 1024], P('sp', None, 'tp'), may hold values from -0.125 to 0.125
- w_up: bfloat16 [64, 2048, 1024], P('sp', None, 'tp'), may hold values from -0.125 to 0.125
- w_down: bfloat16 [64, 1024, 2048], P('sp', 'tp'), may hold values from -0.1875 to 0.1875
- b_gate: bfloat16 [16384, 1024], P('sp', 'tp'), may hold values from -6 to 6
- c_gate: bfloat16 [16384, 1024], P('sp', 'tp'), may hold values from -6 to 6
- x_in: bfloat16 [16384, 1024], P('sp', 'tp'), may hold values from -6 to 6
- taps: bfloat16 [3, 1024], P(None, 'tp'), may hold values from -3 to 3
- w_out: bfloat16 [2048, 1024], P(None, 'tp'), may hold values from -0.1875 to 0.1875
Outputs:
- grad_gate: bfloat16 [64, 2048, 1024], P('sp', None, 'tp')
- grad_up: bfloat16 [64, 2048, 1024], P('sp', None, 'tp')
- grad_down: bfloat16 [64, 1024, 2048], P('sp', 'tp')
- out_proj_grad: float32 [2048, 1024], P('sp', 'tp')
- residual_grad: bfloat16 [16384, 2048], P('sp', 'tp')
- grad_b: bfloat16 [16384, 1024], P('sp', 'tp')
- grad_c: bfloat16 [16384, 1024], P('sp', 'tp')
- grad_x: bfloat16 [16384, 1024], P('sp', 'tp')
Inputs may be any that keep to these rules, and one draw needn't show every extreme that they name: `routes`: each row names 2 different experts. Among the rows of one index of sp no expert is named more than 12 times, a bound that some block reaches in some of them.
All inputs are finite; a program needn't handle non-finite values.
Results may differ from a plain program's by a relative error of at most 0.01.
Values may be sent and summed in bfloat16 or wider, within the bound.
No kernel may reach another device: no remote copies, remote signals or barrier semaphores. Data moves between devices by JAX's collectives and lax.ppermute only.
A program may use at most 64 MiB of HBM per device.

v0:
```python
import jax
import jax.numpy as jnp
from jax import lax
from jax.sharding import PartitionSpec as P


def in_one_piece(arrays, axis, split_dim, concat_dim, along):
    widths = [a.shape[along] for a in arrays]
    both = jnp.concatenate(arrays, axis=along)
    whole = lax.all_to_all(both, axis, split_axis=split_dim, concat_axis=concat_dim, tiled=True)
    return tuple(jnp.split(whole, [sum(widths[:k]) for k in range(1, len(widths))], axis=along))


def sent_together(arrays, axis, dim, along):
    ends, at = ([], 0)
    for a in arrays[:-1]:
        at += a.shape[along]
        ends.append(at)
    both = jnp.concatenate(arrays, axis=along)
    return tuple(jnp.split(lax.all_gather(both, axis, axis=dim, tiled=True), ends, axis=along))


def cut_along(x, dim, devices):
    before, after = (x.shape[:dim], x.shape[dim + 1 :])
    return jnp.moveaxis(x.reshape(*before, devices, -1, *after), dim, 0)


def summed_on_arrival(x, axis, dim):
    blocks = cut_along(x, dim, lax.axis_size(axis))
    arrived = lax.all_to_all(blocks, axis, split_axis=0, concat_axis=0, tiled=True)
    return arrived.astype(jnp.float32).sum(axis=0)


def laid_out(blocks, dim):
    lengths = list(blocks.shape[1:])
    lengths[dim] *= blocks.shape[0]
    return jnp.moveaxis(blocks, 0, dim).reshape(lengths)


def copy_for_each(x, axis):
    copies = jnp.broadcast_to(x, (lax.axis_size(axis), *x.shape))
    return lax.all_to_all(copies, axis, split_axis=0, concat_axis=0, tiled=True)


def gathered_copies(x, axis, dim):
    return laid_out(copy_for_each(x, axis), dim)


def from_behind(x, axis, by):
    devices = lax.axis_size(axis)
    pairs = [(i, i + by) for i in range(devices) if 0 <= i + by < devices]
    return lax.ppermute(x, axis, pairs)


def per_device(
    hidden_in,
    cotangent,
    routes,
    routing_weights,
    w_gate,
    w_up,
    w_down,
    b_gate,
    c_gate,
    x_in,
    taps,
    w_out,
):
    tok_rows, model_width = hidden_in.shape
    top_k = routes.shape[1]
    local_experts = w_gate.shape[0]
    sp_size = lax.axis_size("sp")
    tp_size = lax.axis_size("tp")
    experts = local_experts * sp_size
    capacity = 3 * tok_rows * top_k // (2 * experts)
    slot_count = tok_rows * top_k
    feature_share = model_width // tp_size
    share_offset = lax.axis_index("tp") * feature_share
    flat_ids = routes.reshape(-1)
    onehot = (flat_ids[:, None] == jnp.arange(experts, dtype=jnp.int32)[None, :]).astype(jnp.int32)
    before = jnp.cumsum(onehot, axis=0) - onehot
    position = jnp.sum(before * onehot, axis=1)
    target = flat_ids * capacity + position
    source = (
        jnp.full((experts * capacity,), slot_count, jnp.int32)
        .at[target]
        .set(jnp.arange(slot_count, dtype=jnp.int32))
    )
    filled = source < slot_count
    clipped = jnp.minimum(source, slot_count - 1)
    token_of = clipped // top_k
    weight_of = jnp.where(filled, routing_weights.reshape(-1)[clipped], 0.0)
    rows_src = lax.dynamic_slice_in_dim(hidden_in, share_offset, feature_share, 1)
    cot_src = lax.dynamic_slice_in_dim(cotangent, share_offset, feature_share, 1)
    send_rows = jnp.where(filled[:, None], rows_src[token_of], jnp.zeros((), jnp.bfloat16))
    send_rows = send_rows.reshape(experts, capacity, -1)
    send_cot = (weight_of[:, None] * cot_src[token_of].astype(jnp.float32)).astype(jnp.bfloat16)
    send_cot = send_cot.reshape(experts, capacity, -1)
    part_rows, part_cot = in_one_piece((send_rows, send_cot), "sp", 0, 1, 2)
    rows_h, rows_s = sent_together((part_rows, part_cot), "tp", 2, 0)
    pre_gate = jnp.einsum("erd,edf->erf", rows_h, w_gate, preferred_element_type=jnp.float32)
    pre_up = jnp.einsum("erd,edf->erf", rows_h, w_up, preferred_element_type=jnp.float32)
    sigma = jax.nn.sigmoid(pre_gate)
    silu_gate = pre_gate * sigma
    hid = (silu_gate * pre_up).astype(jnp.bfloat16)
    d_hid = jnp.einsum("erd,efd->erf", rows_s, w_down, preferred_element_type=jnp.float32)
    d_up = (d_hid * silu_gate).astype(jnp.bfloat16)
    d_pre = (d_hid * pre_up * sigma * (1.0 + pre_gate * (1.0 - sigma))).astype(jnp.bfloat16)
    grad_down = jnp.einsum("erf,erd->efd", hid, rows_s, preferred_element_type=jnp.float32).astype(
        jnp.bfloat16
    )
    grad_gate = jnp.einsum(
        "erd,erf->edf", rows_h, d_pre, preferred_element_type=jnp.float32
    ).astype(jnp.bfloat16)
    grad_up = jnp.einsum("erd,erf->edf", rows_h, d_up, preferred_element_type=jnp.float32).astype(
        jnp.bfloat16
    )
    partial_grad = jnp.einsum("erf,edf->erd", d_pre, w_gate, preferred_element_type=jnp.float32)
    partial_grad = partial_grad + jnp.einsum(
        "erf,edf->erd", d_up, w_up, preferred_element_type=jnp.float32
    )
    partial_low = partial_grad.astype(jnp.bfloat16)
    shared_rows = summed_on_arrival(partial_low, "tp", 2).astype(jnp.bfloat16)
    back = lax.all_to_all(shared_rows, "sp", split_axis=1, concat_axis=0, tiled=True)
    back_flat = back.reshape(experts * capacity, feature_share)
    per_token = back_flat[target].astype(jnp.float32).reshape(tok_rows, top_k, feature_share)
    own_cot = lax.dynamic_slice_in_dim(cotangent, share_offset, feature_share, 1).astype(
        jnp.float32
    )
    residual_grad = (own_cot + jnp.sum(per_token, axis=1)).astype(jnp.bfloat16)
    full_grad = gathered_copies(residual_grad, "tp", 1)
    taps_f = taps.astype(jnp.float32)
    gated = c_gate.astype(jnp.float32) * x_in.astype(jnp.float32)
    earlier = from_behind(gated[tok_rows - 2 :], "sp", 1)
    padded = jnp.concatenate([earlier, gated], axis=0)
    conv = (
        taps_f[0] * padded[0:tok_rows]
        + taps_f[1] * padded[1 : tok_rows + 1]
        + taps_f[2] * padded[2 : tok_rows + 2]
    )
    b_f = b_gate.astype(jnp.float32)
    y_short = (b_f * conv).astype(jnp.bfloat16)
    d_y = jnp.dot(full_grad, w_out, preferred_element_type=jnp.float32)
    grad_b = (d_y * conv).astype(jnp.bfloat16)
    d_conv = b_f * d_y
    following = from_behind(d_conv[0:2], "sp", -1)
    later = jnp.concatenate([d_conv, following], axis=0)
    d_v = (
        taps_f[2] * later[0:tok_rows]
        + taps_f[1] * later[1 : tok_rows + 1]
        + taps_f[0] * later[2 : tok_rows + 2]
    )
    grad_c = (d_v * x_in.astype(jnp.float32)).astype(jnp.bfloat16)
    grad_x = (d_v * c_gate.astype(jnp.float32)).astype(jnp.bfloat16)
    out_proj_grad = summed_on_arrival(
        jnp.einsum("td,tc->dc", full_grad, y_short, preferred_element_type=jnp.float32).astype(
            jnp.bfloat16
        ),
        "sp",
        0,
    )
    return (grad_gate, grad_up, grad_down, out_proj_grad, residual_grad, grad_b, grad_c, grad_x)


def solution(mesh):
    return jax.shard_map(
        per_device,
        mesh=mesh,
        in_specs=(
            P("sp", None),
            P("sp", None),
            P("sp", None),
            P("sp", None),
            P("sp", None, "tp"),
            P("sp", None, "tp"),
            P("sp", "tp", None),
            P("sp", "tp"),
            P("sp", "tp"),
            P("sp", "tp"),
            P(None, "tp"),
            P(None, "tp"),
        ),
        out_specs=(
            P("sp", None, "tp"),
            P("sp", None, "tp"),
            P("sp", "tp", None),
            P("sp", "tp"),
            P("sp", "tp"),
            P("sp", "tp"),
            P("sp", "tp"),
            P("sp", "tp"),
        ),
        check_vma=False,
    )
```

profile of v0, /device:TPU:1, one launch (start us, length us, event | category | flops | bytes accessed | tf_op | source)
XLA Modules:
  0.0 338.7 jit_solution(15847824969472595862)
XLA Ops:
  11.0 2.4 scatter_custom_fusion
  14.5 3.3 gather_fusion.2
  19.4 5.0 %gather_fusion.1 = f32[768]{0:T(1024)S(1)} fusion(f32[512]{0:T(512)S(1)} %reshape.169, s32[1024]{0:T(1024)S(1)} %get-tuple-element.24), kind=kCustom, calls=%fused_computation.1 | custom fusion | bytes 9216 | tf_op jit(solution)/shard_map/gather | solution.py:92
  25.5 3.3 gather_fusion
  32.8 62.5 %all_to_all.36 = bf16[64,12,1024]{2,1,0:T(8,128)(2,1)S(1)} all-to-all(bf16[64,12,1024]{2,1,0:T(8,128)(2,1)S(1)} %pad_maximum_fusion), channel_id=1, replica_groups=mesh['sp'=64,'tp'=4] {'sp'}, dimensions={0} | all-to-all | bytes 3145728 | tf_op jit(solution)/shard_map/all_to_all | solution.py:10
  99.4 66.0 %all-gather.2.cloned.1.call-done = bf16[2,768,2048]{2,1,0:T(8,128)(2,1)} async-done(((bf16[2,768,512]{2,1,0:T(8,128)(2,1)}), bf16[2,768,2048]{2,1,0:T(8,128)(2,1)}) %all-gather.2.cloned.1.call-update) | async-done | bytes 6291472 | tf_op jit(solution)/shard_map/all_gather | solution.py:20
  165.3 3.0 fusion.6
  172.8 2.8 add_convert_fusion
  175.6 4.8 %reshape.175 = bf16[1,768,4,512]{3,2,1,0:T(4,128)(2,1)S(1)} reshape(bf16[768,2048]{1,0:T(8,128)(2,1)} %add_convert_fusion) | data formatting | bytes 6291456 | tf_op jit(solution)/shard_map/reshape | solution.py:25
  181.1 39.7 %all_to_all.37 = bf16[4,1,768,512]{3,2,1,0:T(8,128)(2,1)S(1)} all-to-all(bf16[4,1,768,512]{3,2,1,0:T(8,128)(2,1)S(1)} %bitcast.84), channel_id=1, replica_groups=mesh['sp'=64,'tp'=4] {'tp'}, dimensions={0} | all-to-all | bytes 6291456 | tf_op jit(solution)/shard_map/all_to_all | solution.py:30
  222.4 2.3 copy.49
  225.2 5.4 %reduce.4 = bf16[768,512]{1,0:T(8,128)(2,1)S(1)} reduce(bf16[768,1,512]{2,1,0:T(2,128)(2,1)S(1)} %bitcast.87, bf16[]{:T(256)} %broadcast.112), dimensions={1}, to_apply=%bitcast.82.reduce_sub_computation | reduce | bytes 1572866
  231.9 12.0 %all-to-all-start.2 = ((bf16[64,2,3072]{2,1,0:T(2,128)(2,1)}), bf16[64,2,3072]{2,1,0:T(2,128)(2,1)S(1)}, u32[]{:S(2)}, u32[]{:S(2)}) async-start(bf16[64,2,3072]{2,1,0:T(2,128)(2,1)} %reshape.227), calls=%async_computation.2 | async-start | bytes 1572864 | tf_op jit(solution)/shard_map/all_to_all | solution.py:124
  243.9 23.0 %all-to-all-done.2 = bf16[64,2,3072]{2,1,0:T(2,128)(2,1)S(1)} async-done(((bf16[64,2,3072]{2,1,0:T(2,128)(2,1)}), bf16[64,2,3072]{2,1,0:T(2,128)(2,1)S(1)}, u32[]{:S(2)}, u32[]{:S(2)}) %all-to-all-start.2) | async-done | bytes 786464 | tf_op jit(solution)/shard_map/all_to_all | solution.py:124
  273.9 3.8 %all-to-all-start.3 = ((bf16[4,256,512]{1,2,0:T(8,128)(2,1)}), bf16[4,256,512]{1,2,0:T(8,128)(2,1)S(1)}, u32[]{:S(2)}, u32[]{:S(2)}) async-start(bf16[4,256,512]{1,2,0:T(8,128)(2,1)} %broadcast_in_dim.39), calls=%async_computation.3 | async-start | bytes 2097152 | tf_op jit(solution)/shard_map/all_to_all | solution.py:42
  277.7 3.7 %collective-permute-start = (f32[2,256]{1,0:T(2,128)S(1)}, f32[2,256]{1,0:T(2,128)S(1)}, u32[]{:S(2)}, u32[]{:S(2)}) collective-permute-start(f32[2,256]{1,0:T(2,128)S(1)} %slice.57), channel_id=1, source_target_pairs={{0,4},{4,8},{8,12},{12,16},{16,20},{20,24},{24,28},{28,32},{32,36}... | collective-permute-start | bytes 6152 | tf_op jit(solution)/shard_map/ppermute | solution.py:52
  282.1 9.7 %all-to-all-done.3 = bf16[4,256,512]{1,2,0:T(8,128)(2,1)S(1)} async-done(((bf16[4,256,512]{1,2,0:T(8,128)(2,1)}), bf16[4,256,512]{1,2,0:T(8,128)(2,1)S(1)}, u32[]{:S(2)}, u32[]{:S(2)}) %all-to-all-start.3) | async-done | bytes 1048608 | tf_op jit(solution)/shard_map/all_to_all | solution.py:42
  293.9 2.3 convolution_convert_fusion
  296.2 6.6 %all-to-all-start.4 = ((bf16[64,32,256]{2,1,0:T(8,128)(2,1)}), bf16[64,32,256]{2,1,0:T(8,128)(2,1)S(1)}, u32[]{:S(2)}, u32[]{:S(2)}) async-start(bf16[64,32,256]{2,1,0:T(8,128)(2,1)} %bitcast.18), calls=%async_computation.4 | async-start | bytes 2097152 | tf_op jit(solution)/shard_map/all_to_all | solution.py:30
  302.9 4.0 %fusion.3 = bf16[1,2048,256]{2,1,0:T(8,128)(2,1)} fusion(bf16[768,256]{1,0:T(8,128)(2,1)S(1)} %get-tuple-element.15, bf16[2,768,2048]{2,1,0:T(8,128)(2,1)} %all-gather.2.cloned.1.call-done), kind=kOutput, calls=%fused_computation.15 | convolution fusion | flops 805830656 | bytes 4587520 | tf_op jit(solution)/shard_map/erd,erf->edf/dot_general | solution.py:112
  306.9 4.0 %fusion.5 = bf16[1,256,2048]{2,1,0:T(8,128)(2,1)} fusion(bf16[2,768,2048]{2,1,0:T(8,128)(2,1)} %all-gather.2.cloned.1.call-done, f32[768,256]{1,0:T(8,128)S(1)} %copy-done.19, f32[768,256]{1,0:T(8,128)S(1)} %copy-done.17), kind=kOutput, calls=%fused_computation.17 | convolution fusion | flops 807010304 | bytes 5767168 | tf_op jit(solution)/shard_map/erf,erd->efd/dot_general | solution.py:109
  310.9 2.5 collective-permute-start.1
  313.4 4.0 %fusion.4 = bf16[1,2048,256]{2,1,0:T(8,128)(2,1)} fusion(bf16[768,256]{1,0:T(8,128)(2,1)S(1)} %copy-done.11, bf16[2,768,2048]{2,1,0:T(8,128)(2,1)} %all-gather.2.cloned.1.call-done), kind=kOutput, calls=%fused_computation.16 | convolution fusion | flops 805830656 | bytes 4587520 | tf_op jit(solution)/shard_map/erd,erf->edf/dot_general | solution.py:115
  318.9 12.2 %all-to-all-done.4 = bf16[64,32,256]{2,1,0:T(8,128)(2,1)S(1)} async-done(((bf16[64,32,256]{2,1,0:T(8,128)(2,1)}), bf16[64,32,256]{2,1,0:T(8,128)(2,1)S(1)}, u32[]{:S(2)}, u32[]{:S(2)}) %all-to-all-start.4) | async-done | bytes 1048608 | tf_op jit(solution)/shard_map/all_to_all | solution.py:30
  (99 shorter events, 35.7 us)
Async XLA Ops:
  7.2 158.2 %copy-start = (bf16[1,2048,256]{2,1,0:T(8,128)(2,1)S(1)}, bf16[1,2048,256]{2,1,0:T(8,128)(2,1)}, u32[]{:S(2)}) copy-start(bf16[1,2048,256]{2,1,0:T(8,128)(2,1)} %param.16) | copy-start | bytes 3145732
  7.2 158.2 %all-gather.2.cloned.1.call-start = ((), (), s32[]{:S(2)}) async-start(), calls=%async_computation.5 | async-start | bytes 7864320 | tf_op jit(solution)/shard_map/all_gather | solution.py:20
  14.5 4.6 %copy-start.13 = (f32[256,2]{0,1:T(2,128)S(1)}, f32[256,2]{0,1:T(2,128)}, u32[]{:S(2)}) copy-start(f32[256,2]{0,1:T(2,128)} %param.15) | copy-start | bytes 6148
  31.0 1.2 copy-start.2
  99.4 69.0 %copy-start.5 = (bf16[1,2048,256]{2,1,0:T(8,128)(2,1)S(1)}, bf16[1,2048,256]{2,1,0:T(8,128)(2,1)}, u32[]{:S(2)}) copy-start(bf16[1,2048,256]{2,1,0:T(8,128)(2,1)} %param.17) | copy-start | bytes 3145732
  165.3 3.7 %copy-start.14 = (bf16[2,768,2048]{2,1,0:T(8,128)(2,1)S(1)}, bf16[2,768,2048]{2,1,0:T(8,128)(2,1)}, u32[]{:S(2)}) copy-start(bf16[2,768,2048]{2,1,0:T(8,128)(2,1)} %all-gather.2.cloned.1.call-done) | copy-start | bytes 18874372
  169.1 1.5 copy-start.15
  170.6 1.2 copy-start.18
  231.9 35.0 %all-to-all-start.2 = ((bf16[64,2,3072]{2,1,0:T(2,128)(2,1)}), bf16[64,2,3072]{2,1,0:T(2,128)(2,1)S(1)}, u32[]{:S(2)}, u32[]{:S(2)}) async-start(bf16[64,2,3072]{2,1,0:T(2,128)(2,1)} %reshape.227), calls=%async_computation.2 | async-start | bytes 1572864 | tf_op jit(solution)/shard_map/all_to_all | solution.py:124
  270.3 7.3 %copy-start.6 = (bf16[256,256]{1,0:T(8,128)(2,1)S(1)}, bf16[256,256]{1,0:T(8,128)(2,1)}, u32[]{:S(2)}) copy-start(bf16[256,256]{1,0:T(8,128)(2,1)} %param.20) | copy-start | bytes 393220
  270.4 7.3 %copy-start.8 = (bf16[256,256]{1,0:T(8,128)(2,1)S(1)}, bf16[256,256]{1,0:T(8,128)(2,1)}, u32[]{:S(2)}) copy-start(bf16[256,256]{1,0:T(8,128)(2,1)} %param.21) | copy-start | bytes 393220
  271.6 9.8 %copy-start.12 = (bf16[3,256]{1,0:T(4,128)(2,1)S(1)}, bf16[3,256]{1,0:T(4,128)(2,1)}, u32[]{:S(2)}) copy-start(bf16[3,256]{1,0:T(4,128)(2,1)} %param.22) | copy-start | bytes 4612
  272.7 21.2 %copy-start.4 = (bf16[256,512]{1,0:T(8,128)(2,1)}, bf16[256,512]{1,0:T(8,128)(2,1)S(1)}, u32[]{:S(2)}) copy-start(bf16[256,512]{1,0:T(8,128)(2,1)S(1)} %add_convert_fusion.1) | copy-start | bytes 786436
  272.7 19.2 %copy-start.3 = (bf16[2048,256]{1,0:T(8,128)(2,1)S(1)}, bf16[2048,256]{1,0:T(8,128)(2,1)}, u32[]{:S(2)}) copy-start(bf16[2048,256]{1,0:T(8,128)(2,1)} %param.23) | copy-start | bytes 3145732
  273.9 18.0 %all-to-all-start.3 = ((bf16[4,256,512]{1,2,0:T(8,128)(2,1)}), bf16[4,256,512]{1,2,0:T(8,128)(2,1)S(1)}, u32[]{:S(2)}, u32[]{:S(2)}) async-start(bf16[4,256,512]{1,2,0:T(8,128)(2,1)} %broadcast_in_dim.39), calls=%async_computation.3 | async-start | bytes 2097152 | tf_op jit(solution)/shard_map/all_to_all | solution.py:42
  277.7 4.4 %collective-permute-start = (f32[2,256]{1,0:T(2,128)S(1)}, f32[2,256]{1,0:T(2,128)S(1)}, u32[]{:S(2)}, u32[]{:S(2)}) collective-permute-start(f32[2,256]{1,0:T(2,128)S(1)} %slice.57), channel_id=1, source_target_pairs={{0,4},{4,8},{8,12},{12,16},{16,20},{20,24},{24,28},{28,32},{32,36}... | collective-permute-start | bytes 6152 | tf_op jit(solution)/shard_map/ppermute | solution.py:52
  296.2 34.8 %all-to-all-start.4 = ((bf16[64,32,256]{2,1,0:T(8,128)(2,1)}), bf16[64,32,256]{2,1,0:T(8,128)(2,1)S(1)}, u32[]{:S(2)}, u32[]{:S(2)}) async-start(bf16[64,32,256]{2,1,0:T(8,128)(2,1)} %bitcast.18), calls=%async_computation.4 | async-start | bytes 2097152 | tf_op jit(solution)/shard_map/all_to_all | solution.py:30
  302.9 4.0 %copy-start.17 = (f32[768,256]{1,0:T(8,128)S(1)}, f32[768,256]{1,0:T(8,128)}, u32[]{:S(2)}) copy-start(f32[768,256]{1,0:T(8,128)} %copy-done.16) | copy-start | bytes 2359300
  302.9 4.0 %copy-start.19 = (f32[768,256]{1,0:T(8,128)S(1)}, f32[768,256]{1,0:T(8,128)}, u32[]{:S(2)}) copy-start(f32[768,256]{1,0:T(8,128)} %copy-done.18) | copy-start | bytes 2359300
  306.9 6.5 %copy-start.11 = (bf16[768,256]{1,0:T(8,128)(2,1)S(1)}, bf16[768,256]{1,0:T(8,128)(2,1)}, u32[]{:S(2)}) copy-start(bf16[768,256]{1,0:T(8,128)(2,1)} %copy-done.10) | copy-start | bytes 1179652
  310.9 6.5 %copy-start.7 = (bf16[256,256]{1,0:T(8,128)(2,1)S(1)}, bf16[256,256]{1,0:T(8,128)(2,1)}, u32[]{:S(2)}) copy-start(bf16[256,256]{1,0:T(8,128)(2,1)} %param.20) | copy-start | bytes 393220
  310.9 7.3 %copy-start.9 = (bf16[256,256]{1,0:T(8,128)(2,1)S(1)}, bf16[256,256]{1,0:T(8,128)(2,1)}, u32[]{:S(2)}) copy-start(bf16[256,256]{1,0:T(8,128)(2,1)} %param.21) | copy-start | bytes 393220
  310.9 6.5 %collective-permute-start.1 = (f32[2,256]{1,0:T(2,128)S(1)}, f32[2,256]{1,0:T(2,128)S(1)}, u32[]{:S(2)}, u32[]{:S(2)}) collective-permute-start(f32[2,256]{1,0:T(2,128)S(1)} %slice.62), channel_id=1, source_target_pairs={{4,0},{8,4},{12,8},{16,12},{20,16},{24,20},{28,24},{32,28},{36,32}... | collective-permute-start | bytes 6152 | tf_op jit(solution)/shard_map/ppermute | solution.py:52
  313.4 18.4 %copy-start.1 = (bf16[1,2048,256]{2,1,0:T(8,128)(2,1)S(1)}, bf16[1,2048,256]{2,1,0:T(8,128)(2,1)}, u32[]{:S(2)}) copy-start(bf16[1,2048,256]{2,1,0:T(8,128)(2,1)} %param.16) | copy-start | bytes 3145732
  (2 other events, 2.0 us)
Sparse Core Ops, SparseCore 0:
  99.5 65.8 all-gather.1
where the time goes:
time: 340 us; the launch traced here: 339 us
  waiting for transfers between devices  112 us (33%)
  blocking collectives  102 us (30%)
  local copies, waits for them, and re-layouts  40.7 us (12%)
  starting transfers between devices  28.6 us (8%)
  matrix products  25.4 us (7%)
  other arithmetic  15.7 us (5%)
  between operations  14.6 us (4%)
    all_gather x1, waiting for transfers between devices, sent_together(): lax.all_gather(both, axis, axis=dim, tiled=True)  66 us
    all_to_all x1, blocking collectives, in_one_piece(): lax.all_to_all(both, axis, split_axis=split_dim, concat_axis=concat_dim,...  62.5 us
    all_to_all x1, blocking collectives, summed_on_arrival(): lax.all_to_all(blocks, axis, split_axis=0, concat_axis=0, tiled=True)  39.7 us
    all_to_all x1, waiting for transfers between devices, per_device(): lax.all_to_all(shared_rows, 'sp', split_axis=1, concat_axis=0, tiled=True)  23 us
    all_to_all x1, waiting for transfers between devices, summed_on_arrival(): lax.all_to_all(blocks, axis, split_axis=0, concat_axis=0, tiled=True)  12.2 us
    all_to_all x1, starting transfers between devices, per_device(): lax.all_to_all(shared_rows, 'sp', split_axis=1, concat_axis=0, tiled=True)  12 us
    all_to_all x1, waiting for transfers between devices, copy_for_each(): return lax.all_to_all(copies, axis, split_axis=0, concat_axis=0, tiled=True)  9.72 us
  transfers between devices with their start and end apart: 6, of which 5 were waited for; matrix products, arithmetic and copies ran while one was open for 4% of the time, Pallas kernels for 0%

commit v1 on v0

v1 whole, which is shorter than its diff:
```python
import functools

import jax
import jax.numpy as jnp
from jax import lax
from jax.experimental import pallas as pl
from jax.experimental.pallas import tpu as pltpu
from jax.sharding import Mesh, PartitionSpec as P

BF = jnp.bfloat16
F32 = jnp.float32
SP = ("z", "x", "c")
MAIN = 8
VMEM_LIMIT = 56 * 1024 * 1024


def dot(a, b, contract):
    return lax.dot_general(a, b, ((contract[0], contract[1]), ((), ())), preferred_element_type=F32)


def nn(a, b):
    return dot(a, b, ((1,), (0,)))


def nt(a, b):
    return dot(a, b, ((1,), (1,)))


def tn(a, b):
    return dot(a, b, ((0,), (0,)))


def shifted(x, axis, by):
    n = lax.axis_size(axis)
    return lax.ppermute(x, axis, [(i, (i + by) % n) for i in range(n)])


def selection(row, base=0):
    n_rows = 64 * MAIN
    at = lax.broadcasted_iota(jnp.int32, (n_rows, row.shape[1]), 0)
    return at == (row + base)


def route_kernel(tp_ref, ids_ref, w_ref, h_ref, c_ref, out_ref, rows_ref):
    tokens = ids_ref.shape[1]
    expert = lax.broadcasted_iota(jnp.int32, (64, tokens), 0)
    upper = (
        lax.broadcasted_iota(jnp.int32, (tokens, tokens), 0)
        < lax.broadcasted_iota(jnp.int32, (tokens, tokens), 1)
    ).astype(F32).astype(BF)
    ids0, ids1 = ids_ref[0:1, :], ids_ref[1:2, :]
    hot0 = (expert == ids0).astype(F32)
    hot1 = (expert == ids1).astype(F32)
    before0 = nn(hot0.astype(BF), upper)
    before1 = nn(hot1.astype(BF), upper) + jnp.sum(hot0, axis=1, keepdims=True)
    pos0 = jnp.sum(hot0 * before0, axis=0, keepdims=True).astype(jnp.int32)
    pos1 = jnp.sum(hot1 * before1, axis=0, keepdims=True).astype(jnp.int32)
    w0, w1 = w_ref[0:1, :], w_ref[1:2, :]
    none = jnp.full_like(ids0, -64)
    a0 = jnp.where(pos0 < MAIN, ids0 * MAIN + pos0, none)
    a1 = jnp.where(pos1 < MAIN, ids1 * MAIN + pos1, none)
    b0 = jnp.where((pos0 >= MAIN) & (pos0 < MAIN + 4), ids0 * MAIN + pos0 - MAIN, none)
    b1 = jnp.where((pos1 >= MAIN) & (pos1 < MAIN + 4), ids1 * MAIN + pos1 - MAIN, none)
    rows_ref[0:1, :] = a0
    rows_ref[1:2, :] = a1
    rows_ref[2:3, :] = b0
    rows_ref[3:4, :] = b1
    h, c = h_ref[...], c_ref[...]
    width = h.shape[1]

    def picked(r0, r1, base):
        s0, s1 = selection(r0, base), selection(r1, base)
        weight = jnp.sum(jnp.where(s0, w0, 0.0) + jnp.where(s1, w1, 0.0), axis=1, keepdims=True)
        return (s0 | s1).astype(F32).astype(BF), weight

    sel, weight = picked(a0, a1, 0)
    out_ref[:, 0:width] = nn(sel, h).astype(BF)
    out_ref[:, width : 2 * width] = (nn(sel, c) * weight).astype(BF)
    sel_h, _ = picked(b0, b1, 0)
    sel_s, weight = picked(b0, b1, 4)
    out_ref[:, 2 * width : 3 * width] = (nn(sel_h, h) + nn(sel_s, c) * weight).astype(BF)


def route(tp, ids, weights, hidden_in, cotangent):
    tokens, width = hidden_in.shape[0], hidden_in.shape[1] // 4
    share = pl.BlockSpec((tokens, width), lambda i, t: (0, t[0]))
    whole = lambda shape: pl.BlockSpec(shape, lambda i, t: (0, 0))
    return pl.pallas_call(
        route_kernel,
        grid_spec=pltpu.PrefetchScalarGridSpec(
            num_scalar_prefetch=1,
            grid=(1,),
            in_specs=[whole(ids.shape), whole(weights.shape), share, share],
            out_specs=[whole((64 * MAIN, 3 * width)), whole((4, tokens))],
        ),
        out_shape=[
            jax.ShapeDtypeStruct((64 * MAIN, 3 * width), BF),
            jax.ShapeDtypeStruct((4, tokens), jnp.int32),
        ],
        compiler_params=pltpu.CompilerParams(vmem_limit_bytes=VMEM_LIMIT),
        name="route",
    )(tp, ids, weights, hidden_in, cotangent)


def combine_kernel(tp_ref, rows_ref, back_ref, c_ref, out_ref):
    width = c_ref.shape[1]
    a0, a1, b0, b1 = (rows_ref[k : k + 1, :] for k in range(4))

    def sel(r0, r1, base):
        return (selection(r0, base) | selection(r1, base)).astype(F32).astype(BF)

    main = tn(sel(a0, a1, 0), back_ref[:, 0:width])
    rest = back_ref[:, width:]
    low = tn(sel(b0, b1, 0), rest)
    high = tn(sel(b0, b1, 4), rest)
    half = width // 2
    out_ref[:, 0:half] = (c_ref[:, 0:half].astype(F32) + (main[:, 0:half] + low)).astype(BF)
    out_ref[:, half:] = (c_ref[:, half:].astype(F32) + (main[:, half:] + high)).astype(BF)


def combine(tp, rows, back, cotangent):
    tokens, width = cotangent.shape[0], cotangent.shape[1] // 4
    whole = lambda shape: pl.BlockSpec(shape, lambda i, t: (0, 0))
    return pl.pallas_call(
        combine_kernel,
        grid_spec=pltpu.PrefetchScalarGridSpec(
            num_scalar_prefetch=1,
            grid=(1,),
            in_specs=[
                whole(rows.shape),
                whole(back.shape),
                pl.BlockSpec((tokens, width), lambda i, t: (0, t[0])),
            ],
            out_specs=whole((tokens, width)),
        ),
        out_shape=jax.ShapeDtypeStruct((tokens, width), BF),
        compiler_params=pltpu.CompilerParams(vmem_limit_bytes=VMEM_LIMIT),
        name="combine",
    )(tp, rows, back, cotangent)


def block_at(tp, by):
    return lax.rem(tp + by, 4)


def expert_kernel(
    tp_ref, own_ref, prev_ref, next_ref, far_lo_ref, far_hi_ref, wg_ref, wu_ref, wd_ref,
    far_lo_out, far_hi_out, up_lo_out, up_hi_out, down_lo_out, down_hi_out, own_out, da_out, db_out,
    ga, ua, da, gb, ub, db,
):
    tp = tp_ref[0]
    n_rows = own_ref.shape[0]
    half = n_rows // 2
    width = own_ref.shape[1] // 3
    ff = wg_ref.shape[1]

    def rows_of(j):
        return pl.ds(pl.multiple_of(j * width, width), width)

    def add(ref, lo, x, first):
        if first:
            ref[lo : lo + x.shape[0], :] = x
        else:
            ref[lo : lo + x.shape[0], :] += x

    def take(x_ref, by, lo, first):
        j = block_at(tp, by)
        wg, wu, wd = wg_ref[rows_of(j), :], wu_ref[rows_of(j), :], wd_ref[:, rows_of(j)]
        h, s, m = x_ref[:, 0:width], x_ref[:, width : 2 * width], x_ref[:, 2 * width :]
        add(ga, lo, nn(h, wg), first)
        add(ua, lo, nn(h, wu), first)
        add(da, lo, nt(s, wd), first)
        add(gb, lo, nn(m, wg), first)
        add(ub, lo, nn(m, wu), first)
        add(db, lo, nt(m, wd), first)

    take(own_ref, 0, 0, True)
    take(prev_ref, 3, 0, False)
    take(next_ref, 1, 0, False)
    take(far_lo_ref, 2, 0, False)
    take(far_hi_ref, 2, half, False)

    def local(g, u, d):
        sigma = 1.0 / (1.0 + jnp.exp(-g))
        silu = g * sigma
        return d * u * sigma * (1.0 + g * (1.0 - sigma)), d * silu, silu * u

    p, q, r = local(ga[...], ua[...], da[...])
    da_out[:, 0:ff] = p.astype(BF)
    da_out[:, ff : 2 * ff] = q.astype(BF)
    da_out[:, 2 * ff :] = r.astype(BF)
    keep = lax.rem(lax.broadcasted_iota(jnp.int32, (n_rows, ff), 0), 8) < 4
    p, q, r = local(gb[...], ub[...], pltpu.roll(db[...], n_rows - 4, 0))
    p, q, r = (jnp.where(keep, v, 0.0) for v in (p, q, r))
    db_out[:, 0:ff] = p.astype(BF)
    db_out[:, ff : 2 * ff] = q.astype(BF)
    db_out[:, 2 * ff :] = pltpu.roll(r, 4, 0).astype(BF)
    high_p = pltpu.roll(p, 4, 0).astype(BF)
    high_q = pltpu.roll(q, 4, 0).astype(BF)

    def give(by, pieces):
        j = block_at(tp, by)
        wg, wu = wg_ref[rows_of(j), :], wu_ref[rows_of(j), :]
        cut = width // 2
        main = nt(da_out[:, 0:ff], wg) + nt(da_out[:, ff : 2 * ff], wu)
        rest = nt(db_out[:, 0:ff], wg[0:cut]) + nt(db_out[:, ff : 2 * ff], wu[0:cut])
        rest = rest + nt(high_p, wg[cut:]) + nt(high_q, wu[cut:])
        main, rest = main.astype(BF), rest.astype(BF)
        at = 0
        for ref in pieces:
            ref[:, 0:width] = main[at : at + ref.shape[0]]
            ref[:, width:] = rest[at : at + ref.shape[0]]
            at += ref.shape[0]

    give(2, (far_lo_out, far_hi_out))
    give(1, (up_lo_out, up_hi_out))
    give(3, (down_lo_out, down_hi_out))
    give(0, (own_out,))


def vmem_specs(n):
    return [pl.BlockSpec(memory_space=pltpu.VMEM) for _ in range(n)]


def expert(tp, blocks, wg, wu, wd):
    n_rows = blocks[0].shape[0]
    ff = wg.shape[1]
    width = blocks[0].shape[1] // 3
    half = jax.ShapeDtypeStruct((n_rows // 2, width + width // 2), BF)
    return pl.pallas_call(
        expert_kernel,
        in_specs=[pl.BlockSpec(memory_space=pltpu.SMEM)] + vmem_specs(8),
        out_specs=vmem_specs(9),
        out_shape=[half] * 6
        + [
            jax.ShapeDtypeStruct((n_rows, width + width // 2), BF),
            jax.ShapeDtypeStruct((n_rows, 3 * ff), BF),
            jax.ShapeDtypeStruct((n_rows, 3 * ff), BF),
        ],
        scratch_shapes=[pltpu.VMEM((n_rows, ff), F32)] * 6,
        compiler_params=pltpu.CompilerParams(vmem_limit_bytes=VMEM_LIMIT),
        name="expert",
    )(tp, *blocks, wg, wu, wd)


def weights_kernel(
    tp_ref, own_ref, prev_ref, next_ref, far_lo_ref, far_hi_ref, da_ref, db_ref, gg_ref, gu_ref, gd_ref
):
    tp = tp_ref[0]
    width = own_ref.shape[1] // 3
    half = own_ref.shape[0] // 2
    ff = gd_ref.shape[0]

    def sums(x_ref, lo):
        n = x_ref.shape[0]
        da, db = da_ref[lo : lo + n, :], db_ref[lo : lo + n, :]
        h, s, m = x_ref[:, 0:width], x_ref[:, width : 2 * width], x_ref[:, 2 * width :]
        both = tn(h, da[:, 0 : 2 * ff]) + tn(m, db[:, 0 : 2 * ff])
        down = tn(da[:, 2 * ff :], s) + tn(db[:, 2 * ff :], m)
        return both, down

    def put(by, both, down):
        at = pl.ds(pl.multiple_of(block_at(tp, by) * width, width), width)
        gg_ref[at, :] = both[:, 0:ff].astype(BF)
        gu_ref[at, :] = both[:, ff:].astype(BF)
        gd_ref[:, at] = down.astype(BF)

    put(0, *sums(own_ref, 0))
    put(3, *sums(prev_ref, 0))
    put(1, *sums(next_ref, 0))
    both, down = sums(far_lo_ref, 0)
    both_hi, down_hi = sums(far_hi_ref, half)
    put(2, both + both_hi, down + down_hi)


def weight_grads(tp, blocks, da, db):
    width = blocks[0].shape[1] // 3
    ff = da.shape[1] // 3
    return pl.pallas_call(
        weights_kernel,
        in_specs=[pl.BlockSpec(memory_space=pltpu.SMEM)] + vmem_specs(7),
        out_specs=vmem_specs(3),
        out_shape=[
            jax.ShapeDtypeStruct((4 * width, ff), BF),
            jax.ShapeDtypeStruct((4 * width, ff), BF),
            jax.ShapeDtypeStruct((ff, 4 * width), BF),
        ],
        compiler_params=pltpu.CompilerParams(vmem_limit_bytes=VMEM_LIMIT),
        name="weight_grads",
    )(tp, *blocks, da, db)


def mixer_kernel(
    where_ref, own_ref, prev_ref, next_ref, far_ref, wo_ref, conv_ref, y_ref, b_ref,
    gb_ref, dc_ref, mine_ref, other_ref,
):
    tp, core = where_ref[0], where_ref[1]
    width = own_ref.shape[1]
    y = y_ref[...]
    d_y = None
    for ref, by in ((own_ref, 0), (prev_ref, 3), (next_ref, 1), (far_ref, 2)):
        at = pl.multiple_of(block_at(tp, by) * width, width)
        part = nn(ref[...], wo_ref[pl.ds(at, width), :])
        d_y = part if d_y is None else d_y + part
        grad = tn(ref[...], y).astype(BF).reshape(width // 64, 2, 32, y.shape[1])
        low, high = grad[:, 0], grad[:, 1]
        shape = (width // 2, y.shape[1])
        to = pl.ds(pl.multiple_of(block_at(tp, by) * (width // 2), width // 2), width // 2)
        first = core == 0
        mine_ref[to, :] = jnp.where(first, low, high).reshape(shape)
        other_ref[to, :] = jnp.where(first, high, low).reshape(shape)
    gb_ref[...] = (d_y * conv_ref[...]).astype(BF)
    dc_ref[...] = b_ref[...].astype(F32) * d_y


def mixer(where, blocks, w_out, conv, y_short, b_gate):
    tokens, width = blocks[0].shape
    chan = w_out.shape[1]
    return pl.pallas_call(
        mixer_kernel,
        in_specs=[pl.BlockSpec(memory_space=pltpu.SMEM)] + vmem_specs(8),
        out_specs=vmem_specs(4),
        out_shape=[
            jax.ShapeDtypeStruct((tokens, chan), BF),
            jax.ShapeDtypeStruct((tokens, chan), F32),
            jax.ShapeDtypeStruct((2 * width, chan), BF),
            jax.ShapeDtypeStruct((2 * width, chan), BF),
        ],
        compiler_params=pltpu.CompilerParams(vmem_limit_bytes=VMEM_LIMIT),
        name="mixer",
    )(where, *blocks, w_out, conv, y_short, b_gate)


def from_behind(x, by):
    n = lax.axis_size(SP)
    return lax.ppermute(x, SP, [(i, i + by) for i in range(n) if 0 <= i + by < n])


def per_device(
    hidden_in, cotangent, routes, routing_weights, w_gate, w_up, w_down, b_gate, c_gate, x_in, taps, w_out
):
    tok_rows, model_width = hidden_in.shape
    share = model_width // 4
    y_at = lax.axis_index("y").astype(jnp.int32)
    tp = y_at.reshape(1)
    where = jnp.stack([y_at, lax.axis_index("c").astype(jnp.int32)])
    wg, wu, wd = w_gate[0], w_up[0], w_down[0]

    sent, rows = route(tp, routes.T, routing_weights.T, hidden_in, cotangent)
    own = lax.all_to_all(sent.reshape(64, MAIN, 3 * share), SP, split_axis=0, concat_axis=0, tiled=True)
    own = own.reshape(64 * MAIN, 3 * share)
    half = own.shape[0] // 2

    prev = shifted(own, "y", 1)
    after = shifted(own, "y", -1)
    far_lo = shifted(prev[:half], "y", 1)
    far_hi = shifted(after[half:], "y", -1)
    blocks = (own, prev, after, far_lo, far_hi)

    f_lo, f_hi, u_lo, u_hi, d_lo, d_hi, o, da, db = expert(tp, blocks, wg, wu, wd)

    from_prev = shifted(f_lo, "y", 1)
    from_next = shifted(f_hi, "y", -1)
    prev_hi = shifted(u_hi, "y", 1)
    next_lo = shifted(d_lo, "y", -1)
    added = lambda a, b: (a.astype(F32) + b.astype(F32)).astype(BF)
    prev_lo = shifted(added(u_lo, from_prev), "y", 1)
    next_hi = shifted(added(d_hi, from_next), "y", -1)
    got_prev = jnp.concatenate([prev_lo, prev_hi], axis=0).astype(F32)
    got_next = jnp.concatenate([next_lo, next_hi], axis=0).astype(F32)
    total = (o.astype(F32) + got_prev + got_next).astype(BF)
    back = lax.all_to_all(
        total.reshape(64, MAIN, total.shape[1]), SP, split_axis=0, concat_axis=0, tiled=True
    ).reshape(total.shape)

    residual_grad = combine(tp, rows, back, cotangent)
    res_blocks = (
        residual_grad,
        shifted(residual_grad, "y", 1),
        shifted(residual_grad, "y", -1),
        shifted(residual_grad, "y", 2),
    )

    taps_f = taps.astype(F32)
    gated = c_gate.astype(F32) * x_in.astype(F32)
    earlier = from_behind(gated[tok_rows - 2 :], 1)
    padded = jnp.concatenate([earlier, gated], axis=0)
    conv = (
        taps_f[0] * padded[0:tok_rows]
        + taps_f[1] * padded[1 : tok_rows + 1]
        + taps_f[2] * padded[2 : tok_rows + 2]
    )
    y_short = (b_gate.astype(F32) * conv).astype(BF)

    grad_b, d_conv, mine, other = mixer(where, res_blocks, w_out, conv, y_short, b_gate)
    following = from_behind(d_conv[0:2], -1)
    later = jnp.concatenate([d_conv, following], axis=0)
    d_v = (
        taps_f[2] * later[0:tok_rows]
        + taps_f[1] * later[1 : tok_rows + 1]
        + taps_f[0] * later[2 : tok_rows + 2]
    )
    grad_c = (d_v * x_in.astype(F32)).astype(BF)
    grad_x = (d_v * c_gate.astype(F32)).astype(BF)

    chip = added(mine, shifted(other, "c", 1)).reshape(32, 32, mine.shape[1])
    parts = lax.all_to_all(chip, ("z", "x"), split_axis=0, concat_axis=0, tiled=True)
    out_proj_grad = jnp.sum(parts.astype(F32), axis=0)

    gg, gu, gd = weight_grads(tp, blocks, da, db)
    return (gg[None], gu[None], gd[None], out_proj_grad, residual_grad, grad_b, grad_c, grad_x)


def solution(mesh):
    fine = Mesh(mesh.devices.reshape(8, 4, 2, 4), ("z", "x", "c", "y"))
    rows = P(SP, None)
    both = P(SP, "y")
    return jax.shard_map(
        per_device,
        mesh=fine,
        in_specs=(
            rows, rows, rows, rows,
            P(SP, None, "y"), P(SP, None, "y"), P(SP, "y", None),
            both, both, both, P(None, "y"), P(None, "y"),
        ),
        out_specs=(P(SP, None, "y"), P(SP, None, "y"), P(SP, "y", None), both, both, both, both, both),
        check_vma=False,
    )
```

time: 340 us -> 237 us (0.70)
  blocking collectives: 102 us -> 52 us
  local copies, waits for them, and re-layouts: 40.7 us -> 4.03 us
  Pallas kernels: 0 us -> 28.4 us
  matrix products: 25.4 us -> 0 us
  between operations: 14.6 us -> 0.85 us
  starting transfers between devices: 28.6 us -> 41.3 us
  waiting for transfers between devices: 112 us -> 101 us
  other arithmetic: 15.7 us -> 8.96 us
    ppermute x2 -> x16, waiting for transfers between devices: 0.69 us -> 80.2 us  [the longest x14 77.1 us: shifted(): return lax.ppermute(x, axis, [(i, (i + by) % n) for i in range(n)])]
    all_gather x1 -> x0, waiting for transfers between devices: 66 us -> none  [sent_together(): lax.all_gather(both, axis, axis=dim, tiled=True)]
    all_to_all x2 -> x1, blocking collectives: 102 us -> 52 us  [per_device(): lax.all_to_all(sent.reshape(64, MAIN, 3 * share), SP, split_axis=0, conca...]
    pallas_call x0 -> x5, Pallas kernels: none -> 28.4 us  [the longest x1 10.7 us: expert(): pl.pallas_call(expert_kernel, in_specs=[pl.BlockSpec(memory_space=pltpu.S...]
    dot_general x10 -> x0, matrix products: 25.4 us -> none  [the longest x1 4.02 us: per_device(): jnp.einsum('erd,erf->edf', rows_h, d_pre, preferred_element_type=jnp.floa...]
    all_to_all x3 -> x2, waiting for transfers between devices: 44.9 us -> 20.5 us  [the longest x1 19.3 us: per_device(): lax.all_to_all(total.reshape(64, MAIN, total.shape[1]), SP, split_axis=0,...]
    ppermute x2 -> x16, starting transfers between devices: 6.17 us -> 23.3 us  [the longest x14 17.2 us: shifted(): return lax.ppermute(x, axis, [(i, (i + by) % n) for i in range(n)])]
    gather x5 -> x0, local copies, waits for them, and re-layouts: 15.7 us -> none  [the longest x2 5.42 us: per_device(): rows_src[token_of]]
  transfers between devices with their start and end apart: 6 -> 18, of which waited for: 5 -> 11; matrix products, arithmetic and copies ran while one was open for 4% -> 2% of each run, Pallas kernels for 0% -> 5%
where the time goes in v1:
time: 237 us; the launch traced here: 236 us
  waiting for transfers between devices  101 us (43%)
  blocking collectives  52 us (22%)
  starting transfers between devices  41.3 us (17%)
  Pallas kernels  28.4 us (12%)
  other arithmetic  8.96 us (4%)
  local copies, waits for them, and re-layouts  4.03 us (2%)
    ppermute x14, waiting for transfers between devices, shifted(): return lax.ppermute(x, axis, [(i, (i + by) % n) for i in range(n)])  77.1 us
    all_to_all x1, blocking collectives, per_device(): lax.all_to_all(sent.reshape(64, MAIN, 3 * share), SP, split_axis=0, conca...  52 us
    all_to_all x1, waiting for transfers between devices, per_device(): lax.all_to_all(total.reshape(64, MAIN, total.shape[1]), SP, split_axis=0,...  19.3 us
    ppermute x14, starting transfers between devices, shifted(): return lax.ppermute(x, axis, [(i, (i + by) % n) for i in range(n)])  17.2 us
    all_to_all x1, starting transfers between devices, per_device(): lax.all_to_all(total.reshape(64, MAIN, total.shape[1]), SP, split_axis=0,...  13.4 us
    pallas_call x1, Pallas kernels, expert(): pl.pallas_call(expert_kernel, in_specs=[pl.BlockSpec(memory_space=pltpu.S...  10.7 us
    pallas_call x1, Pallas kernels, weight_grads(): pl.pallas_call(weights_kernel, in_specs=[pl.BlockSpec(memory_space=pltpu....  8.25 us
    ppermute x2, starting transfers between devices, from_behind(): lax.ppermute(x, SP, [(i, i + by) for i in range(n) if 0 <= i + by < n])  6.1 us
  transfers between devices with their start and end apart: 18, of which 11 were waited for; matrix products, arithmetic and copies ran while one was open for 2% of the time, Pallas kernels for 5%

profile of v1, /device:TPU:1, one launch (start us, length us, event | category | flops | bytes accessed | tf_op | source)
XLA Modules:
  0.0 236.3 jit_solution(207501179139851325)
XLA Ops:
  0.6 3.4 %route.1 = (bf16[512,1536]{1,0:T(8,128)(2,1)}, s32[4,256]{1,0:T(4,128)}) custom-call(s32[1]{0:T(128)} %bitcast.tp_ref, s32[2,256]{1,0:T(2,128)} %bitcast.34, f32[2,256]{1,0:T(2,128)} %bitcast.35, bf16[256,2048]{1,0:T(8,128)(2,1)} %h_ref.1, bf16[256,2048]{1,0:T(8,128)(2,1)} %c_ref.3), custom_call_target="tpu_custom_call" | custom-call | tf_op jit(solution)/shard_map/route/pallas_call | solution.py:88
  4.0 52.0 %all_to_all.15 = bf16[64,8,1536]{2,1,0:T(8,128)(2,1)S(1)} all-to-all(bf16[64,8,1536]{2,1,0:T(8,128)(2,1)} %bitcast.24), channel_id=1, replica_groups=mesh['z'=8,'x'=4,'c'=2,'y'=4] {'z','x','c'}, dimensions={0} | all-to-all | bytes 3145728 | tf_op jit(solution)/shard_map/all_to_all | solution.py:350
  58.8 33.0 %collective-permute-done.prev_ref = bf16[512,1536]{1,0:T(8,128)(2,1)S(1)} collective-permute-done((bf16[512,1536]{1,0:T(8,128)(2,1)S(1)}, bf16[512,1536]{1,0:T(8,128)(2,1)S(1)}, u32[]{:S(2)}, u32[]{:S(2)}) %collective-permute-start) | collective-permute-done | bytes 1572896 | tf_op jit(solution)/shard_map/ppermute | solution.py:35
  94.8 15.2 %collective-permute-done.2.far_lo_ref = bf16[256,1536]{1,0:T(8,128)(2,1)S(1)} collective-permute-done((bf16[256,1536]{1,0:T(8,128)(2,1)S(1)}, bf16[256,1536]{1,0:T(8,128)(2,1)S(1)}, u32[]{:S(2)}, u32[]{:S(2)}) %collective-permute-start.2) | collective-permute-done | bytes 786464 | tf_op jit(solution)/shard_map/ppermute | solution.py:35
  111.2 10.7 %expert.1 = (bf16[256,768]{1,0:T(8,128)(2,1)}, bf16[256,768]{1,0:T(8,128)(2,1)}, bf16[256,768]{1,0:T(8,128)(2,1)}, bf16[256,768]{1,0:T(8,128)(2,1)}, bf16[256,76...) custom-call(s32[1]{0:T(128)} %bitcast.tp_ref, ...), custom_call_target="tpu_custom_call" | custom-call | tf_op jit(solution)/shard_map/expert/pallas_call | solution.py:230
  121.9 2.3 collective-permute-start.8
  124.2 2.7 %collective-permute-start.7 = (bf16[256,768]{1,0:T(8,128)(2,1)}, bf16[256,768]{1,0:T(8,128)(2,1)S(1)}, u32[]{:S(2)}, u32[]{:S(2)}) collective-permute-start(bf16[256,768]{1,0:T(8,128)(2,1)} %get-tuple-element.37), channel_id=1, source_target_pairs={{0,3},{1,0},{2,1},{3,2},{4,7},{5,4},{6,5},{7,6},{8,11},{9,8},{10,9... | collective-permute-start | bytes 1179656 | tf_op jit(solution)/shard_map/ppermute | solution.py:35
  126.9 2.8 %collective-permute-done.8 = bf16[256,768]{1,0:T(8,128)(2,1)S(1)} collective-permute-done((bf16[256,768]{1,0:T(8,128)(2,1)}, bf16[256,768]{1,0:T(8,128)(2,1)S(1)}, u32[]{:S(2)}, u32[]{:S(2)}) %collective-permute-start.8) | collective-permute-done | bytes 393248 | tf_op jit(solution)/shard_map/ppermute | solution.py:35
  130.8 3.3 %collective-permute-start.9 = (bf16[256,768]{1,0:T(8,128)(2,1)S(1)}, bf16[256,768]{1,0:T(8,128)(2,1)S(1)}, u32[]{:S(2)}, u32[]{:S(2)}) collective-permute-start(bf16[256,768]{1,0:T(8,128)(2,1)S(1)} %add_convert_fusion.2), channel_id=1, source_target_pairs={{0,3},{1,0},{2,1},{3,2},{4,7},{5,4},{6,5},{7,6},{8,11},{9,8},{10,9... | collective-permute-start | bytes 1179656 | tf_op jit(solution)/shard_map/ppermute | solution.py:35
  135.3 5.8 %collective-permute-done.6 = bf16[256,768]{1,0:T(8,128)(2,1)S(1)} collective-permute-done((bf16[256,768]{1,0:T(8,128)(2,1)}, bf16[256,768]{1,0:T(8,128)(2,1)S(1)}, u32[]{:S(2)}, u32[]{:S(2)}) %collective-permute-start.6) | collective-permute-done | bytes 393248 | tf_op jit(solution)/shard_map/ppermute | solution.py:35
  141.1 5.5 %collective-permute-done.9 = bf16[256,768]{1,0:T(8,128)(2,1)S(1)} collective-permute-done((bf16[256,768]{1,0:T(8,128)(2,1)S(1)}, bf16[256,768]{1,0:T(8,128)(2,1)S(1)}, u32[]{:S(2)}, u32[]{:S(2)}) %collective-permute-start.9) | collective-permute-done | bytes 393248 | tf_op jit(solution)/shard_map/ppermute | solution.py:35
  146.6 2.9 %collective-permute-done.5 = bf16[256,768]{1,0:T(8,128)(2,1)S(1)} collective-permute-done((bf16[256,768]{1,0:T(8,128)(2,1)S(1)}, bf16[256,768]{1,0:T(8,128)(2,1)S(1)}, u32[]{:S(2)}, u32[]{:S(2)}) %collective-permute-start.5) | collective-permute-done | bytes 393248 | tf_op jit(solution)/shard_map/ppermute | solution.py:35
  150.7 13.4 %all-to-all-start.1 = ((bf16[64,8,768]{2,1,0:T(8,128)(2,1)}), bf16[64,8,768]{2,1,0:T(8,128)(2,1)S(1)}, u32[]{:S(2)}, u32[]{:S(2)}) async-start(bf16[64,8,768]{2,1,0:T(8,128)(2,1)} %fusion), calls=%async_computation.1 | async-start | bytes 1572864 | tf_op jit(solution)/shard_map/all_to_all | solution.py:372
  164.2 3.5 %collective-permute-start.13 = (f32[2,256]{1,0:T(2,128)S(1)}, f32[2,256]{1,0:T(2,128)S(1)}, u32[]{:S(2)}, u32[]{:S(2)}) collective-permute-start(f32[2,256]{1,0:T(2,128)S(1)} %slice.50), channel_id=1, source_target_pairs={{0,4},{4,8},{8,12},{12,16},{16,20},{20,24},{24,28},{28,32},{32,36}... | collective-permute-start | bytes 6152 | tf_op jit(solution)/shard_map/ppermute | solution.py:336
  167.7 19.3 %all-to-all-done.1 = bf16[64,8,768]{2,1,0:T(8,128)(2,1)S(1)} async-done(((bf16[64,8,768]{2,1,0:T(8,128)(2,1)}), bf16[64,8,768]{2,1,0:T(8,128)(2,1)S(1)}, u32[]{:S(2)}, u32[]{:S(2)}) %all-to-all-start.1) | async-done | bytes 786464 | tf_op jit(solution)/shard_map/all_to_all | solution.py:372
  188.0 2.5 %combine.1.own_ref = bf16[256,512]{1,0:T(8,128)(2,1)} custom-call(s32[1]{0:T(128)} %bitcast.tp_ref, s32[4,256]{1,0:T(4,128)} %get-tuple-element.32.rows_ref, bf16[512,768]{1,0:T(8,128)(2,1)} %bitcast.23, bf16[256,2048]{1,0:T(8,128)(2,1)} %c_ref.3), custom_call_target="tpu_custom_call" | custom-call | tf_op jit(solution)/shard_map/combine/pallas_call | solution.py:124
  190.5 2.7 %collective-permute-start.11 = (bf16[256,512]{1,0:T(8,128)(2,1)}, bf16[256,512]{1,0:T(8,128)(2,1)S(1)}, u32[]{:S(2)}, u32[]{:S(2)}) collective-permute-start(bf16[256,512]{1,0:T(8,128)(2,1)} %combine.1.own_ref), channel_id=1, source_target_pairs={{0,3},{1,0},{2,1},{3,2},{4,7},{5,4},{6,5},{7,6},{8,11},{9,8},{10,9... | collective-permute-start | bytes 786440 | tf_op jit(solution)/shard_map/ppermute | solution.py:35
  194.6 10.1 %collective-permute-done.10.prev_ref = bf16[256,512]{1,0:T(8,128)(2,1)S(1)} collective-permute-done((bf16[256,512]{1,0:T(8,128)(2,1)}, bf16[256,512]{1,0:T(8,128)(2,1)S(1)}, u32[]{:S(2)}, u32[]{:S(2)}) %collective-permute-start.10) | collective-permute-done | bytes 262176 | tf_op jit(solution)/shard_map/ppermute | solution.py:35
  205.6 3.5 %mixer.1 = (bf16[256,256]{1,0:T(8,128)(2,1)}, f32[256,256]{1,0:T(8,128)}, bf16[1024,256]{1,0:T(8,128)(2,1)}, bf16[1024,256]{1,0:T(8,128)(2,1)}) custom-call(s32[2]{0:T(128)} %pad_add_fusion.where_ref, bf16[256,512]{1,0:T(8,128)(2,1)} %combine.1.own_ref, bf16[256,512]{1,0:T(8,128)(2,1)} %copy-done.11, bf16[256,512]{1,0:T(8,128)(2,1)} %copy-done.12, ...), custom_call_target="tpu_custom_call" | custom-call | tf_op jit(solution)/shard_map/mixer/pallas_call | solution.py:319
  212.4 2.0 add_convert_fusion.1
  214.4 4.6 %all-to-all-start.2 = ((bf16[32,32,256]{2,1,0:T(8,128)(2,1)}), bf16[32,32,256]{2,1,0:T(8,128)(2,1)S(1)}, u32[]{:S(2)}, u32[]{:S(2)}) async-start(bf16[32,32,256]{2,1,0:T(8,128)(2,1)} %bitcast.17), calls=%async_computation.2 | async-start | bytes 1048576 | tf_op jit(solution)/shard_map/all_to_all | solution.py:407
  219.0 8.2 %weight_grads.1 = (bf16[2048,256]{1,0:T(8,128)(2,1)}, bf16[2048,256]{1,0:T(8,128)(2,1)}, bf16[256,2048]{1,0:T(8,128)(2,1)}) custom-call(s32[1]{0:T(128)} %bitcast.tp_ref, bf16[512,1536]{1,0:T(8,128)(2,1)} %bitcast.22, bf16[512,1536]{1,0:T(8,128)(2,1)} %copy-done.1, bf16[512,1536]{1,0:T(8,128)(2,1)} %copy-done.2, bf16[256,1536]{1,0:T(8,128)(2,1)} %copy-done.4, ...), custom_call_target="tpu_custom_call" | custom-call | tf_op jit(solution)/shard_map/weight_grads/pallas_call | solution.py:279
  227.2 2.6 %collective-permute-start.15 = (f32[2,256]{1,0:T(2,128)S(1)}, f32[2,256]{1,0:T(2,128)S(1)}, u32[]{:S(2)}, u32[]{:S(2)}) collective-permute-start(f32[2,256]{1,0:T(2,128)S(1)} %slice.44), channel_id=1, source_target_pairs={{4,0},{8,4},{12,8},{16,12},{20,16},{24,20},{28,24},{32,28},{36,32}... | collective-permute-start | bytes 6152 | tf_op jit(solution)/shard_map/ppermute | solution.py:336
  229.8 3.1 %collective-permute-done.15 = f32[2,256]{1,0:T(2,128)S(1)} collective-permute-done((f32[2,256]{1,0:T(2,128)S(1)}, f32[2,256]{1,0:T(2,128)S(1)}, u32[]{:S(2)}, u32[]{:S(2)}) %collective-permute-start.15) | collective-permute-done | bytes 2080 | tf_op jit(solution)/shard_map/ppermute | solution.py:336
  (65 shorter events, 20.2 us)
Async XLA Ops:
  56.1 36.0 %copy-start = (bf16[64,8,1536]{2,1,0:T(8,128)(2,1)}, bf16[64,8,1536]{2,1,0:T(8,128)(2,1)S(1)}, u32[]{:S(2)}) copy-start(bf16[64,8,1536]{2,1,0:T(8,128)(2,1)S(1)} %all_to_all.15) | copy-start | bytes 4718596
  56.1 35.8 %collective-permute-start = (bf16[512,1536]{1,0:T(8,128)(2,1)S(1)}, bf16[512,1536]{1,0:T(8,128)(2,1)S(1)}, u32[]{:S(2)}, u32[]{:S(2)}) collective-permute-start(bf16[512,1536]{1,0:T(8,128)(2,1)S(1)} %bitcast.19), channel_id=1, source_target_pairs={{0,1},{1,2},{2,3},{3,0},{4,5},{5,6},{6,7},{7,4},{8,9},{9,10},{10,1... | collective-permute-start | bytes 4718600 | tf_op jit(solution)/shard_map/ppermute | solution.py:35
  57.3 34.6 %collective-permute-start.1 = (bf16[512,1536]{1,0:T(8,128)(2,1)S(1)}, bf16[512,1536]{1,0:T(8,128)(2,1)S(1)}, u32[]{:S(2)}, u32[]{:S(2)}) collective-permute-start(bf16[512,1536]{1,0:T(8,128)(2,1)S(1)} %bitcast.20), channel_id=1, source_target_pairs={{0,3},{1,0},{2,1},{3,2},{4,7},{5,4},{6,5},{7,6},{8,11},{9,8},{10,9... | collective-permute-start | bytes 4718600 | tf_op jit(solution)/shard_map/ppermute | solution.py:35
  91.9 18.1 %collective-permute-start.2 = (bf16[256,1536]{1,0:T(8,128)(2,1)S(1)}, bf16[256,1536]{1,0:T(8,128)(2,1)S(1)}, u32[]{:S(2)}, u32[]{:S(2)}) collective-permute-start(bf16[256,1536]{1,0:T(8,128)(2,1)S(1)} %slice.47), channel_id=1, source_target_pairs={{0,1},{1,2},{2,3},{3,0},{4,5},{5,6},{6,7},{7,4},{8,9},{9,10},{10,1... | collective-permute-start | bytes 2359304 | tf_op jit(solution)/shard_map/ppermute | solution.py:35
  92.0 18.0 %copy-start.2 = (bf16[512,1536]{1,0:T(8,128)(2,1)}, bf16[512,1536]{1,0:T(8,128)(2,1)S(1)}, u32[]{:S(2)}) copy-start(bf16[512,1536]{1,0:T(8,128)(2,1)S(1)} %collective-permute-done.1.next_ref) | copy-start | bytes 4718596
  93.0 17.0 %collective-permute-start.3 = (bf16[256,1536]{1,0:T(8,128)(2,1)S(1)}, bf16[256,1536]{1,0:T(8,128)(2,1)S(1)}, u32[]{:S(2)}, u32[]{:S(2)}) collective-permute-start(bf16[256,1536]{1,0:T(8,128)(2,1)S(1)} %slice.48), channel_id=1, source_target_pairs={{0,3},{1,0},{2,1},{3,2},{4,7},{5,4},{6,5},{7,6},{8,11},{9,8},{10,9... | collective-permute-start | bytes 2359304 | tf_op jit(solution)/shard_map/ppermute | solution.py:35
  121.9 27.6 %copy-start.7 = (bf16[512,768]{1,0:T(8,128)(2,1)S(1)}, bf16[512,768]{1,0:T(8,128)(2,1)}, u32[]{:S(2)}) copy-start(bf16[512,768]{1,0:T(8,128)(2,1)} %get-tuple-element.33) | copy-start | bytes 2359300
  121.9 7.8 %collective-permute-start.8 = (bf16[256,768]{1,0:T(8,128)(2,1)}, bf16[256,768]{1,0:T(8,128)(2,1)S(1)}, u32[]{:S(2)}, u32[]{:S(2)}) collective-permute-start(bf16[256,768]{1,0:T(8,128)(2,1)} %get-tuple-element.39), channel_id=1, source_target_pairs={{0,3},{1,0},{2,1},{3,2},{4,7},{5,4},{6,5},{7,6},{8,11},{9,8},{10,9... | collective-permute-start | bytes 1179656 | tf_op jit(solution)/shard_map/ppermute | solution.py:35
  124.2 9.8 %collective-permute-start.4 = (bf16[256,768]{1,0:T(8,128)(2,1)}, bf16[256,768]{1,0:T(8,128)(2,1)S(1)}, u32[]{:S(2)}, u32[]{:S(2)}) collective-permute-start(bf16[256,768]{1,0:T(8,128)(2,1)} %get-tuple-element.35), channel_id=1, source_target_pairs={{0,1},{1,2},{2,3},{3,0},{4,5},{5,6},{6,7},{7,4},{8,9},{9,10},{10,1... | collective-permute-start | bytes 1179656 | tf_op jit(solution)/shard_map/ppermute | solution.py:35
  124.2 16.8 %collective-permute-start.6 = (bf16[256,768]{1,0:T(8,128)(2,1)}, bf16[256,768]{1,0:T(8,128)(2,1)S(1)}, u32[]{:S(2)}, u32[]{:S(2)}) collective-permute-start(bf16[256,768]{1,0:T(8,128)(2,1)} %get-tuple-element.36), channel_id=1, source_target_pairs={{0,1},{1,2},{2,3},{3,0},{4,5},{5,6},{6,7},{7,4},{8,9},{9,10},{10,1... | collective-permute-start | bytes 1179656 | tf_op jit(solution)/shard_map/ppermute | solution.py:35
  124.2 16.8 %collective-permute-start.7 = (bf16[256,768]{1,0:T(8,128)(2,1)}, bf16[256,768]{1,0:T(8,128)(2,1)S(1)}, u32[]{:S(2)}, u32[]{:S(2)}) collective-permute-start(bf16[256,768]{1,0:T(8,128)(2,1)} %get-tuple-element.37), channel_id=1, source_target_pairs={{0,3},{1,0},{2,1},{3,2},{4,7},{5,4},{6,5},{7,6},{8,11},{9,8},{10,9... | collective-permute-start | bytes 1179656 | tf_op jit(solution)/shard_map/ppermute | solution.py:35
  130.8 15.8 %collective-permute-start.9 = (bf16[256,768]{1,0:T(8,128)(2,1)S(1)}, bf16[256,768]{1,0:T(8,128)(2,1)S(1)}, u32[]{:S(2)}, u32[]{:S(2)}) collective-permute-start(bf16[256,768]{1,0:T(8,128)(2,1)S(1)} %add_convert_fusion.2), channel_id=1, source_target_pairs={{0,3},{1,0},{2,1},{3,2},{4,7},{5,4},{6,5},{7,6},{8,11},{9,8},{10,9... | collective-permute-start | bytes 1179656 | tf_op jit(solution)/shard_map/ppermute | solution.py:35
  135.2 14.3 %collective-permute-start.5 = (bf16[256,768]{1,0:T(8,128)(2,1)S(1)}, bf16[256,768]{1,0:T(8,128)(2,1)S(1)}, u32[]{:S(2)}, u32[]{:S(2)}) collective-permute-start(bf16[256,768]{1,0:T(8,128)(2,1)S(1)} %add_convert_fusion.3), channel_id=1, source_target_pairs={{0,1},{1,2},{2,3},{3,0},{4,5},{5,6},{6,7},{7,4},{8,9},{9,10},{10,1... | collective-permute-start | bytes 1179656 | tf_op jit(solution)/shard_map/ppermute | solution.py:35
  150.7 13.4 %copy-start.10 = (bf16[256,256]{1,0:T(8,128)(2,1)S(1)}, bf16[256,256]{1,0:T(8,128)(2,1)}, u32[]{:S(2)}) copy-start(bf16[256,256]{1,0:T(8,128)(2,1)} %param.21) | copy-start | bytes 393220
  150.7 17.1 %copy-start.14 = (bf16[3,256]{1,0:T(4,128)(2,1)S(1)}, bf16[3,256]{1,0:T(4,128)(2,1)}, u32[]{:S(2)}) copy-start(bf16[3,256]{1,0:T(4,128)(2,1)} %param.22) | copy-start | bytes 4612
  150.7 36.4 %all-to-all-start.1 = ((bf16[64,8,768]{2,1,0:T(8,128)(2,1)}), bf16[64,8,768]{2,1,0:T(8,128)(2,1)S(1)}, u32[]{:S(2)}, u32[]{:S(2)}) async-start(bf16[64,8,768]{2,1,0:T(8,128)(2,1)} %fusion), calls=%async_computation.1 | async-start | bytes 1572864 | tf_op jit(solution)/shard_map/all_to_all | solution.py:372
  164.1 29.7 %copy-start.8 = (bf16[256,256]{1,0:T(8,128)(2,1)S(1)}, bf16[256,256]{1,0:T(8,128)(2,1)}, u32[]{:S(2)}) copy-start(bf16[256,256]{1,0:T(8,128)(2,1)} %b_ref.1) | copy-start | bytes 393220
  164.2 29.6 %collective-permute-start.13 = (f32[2,256]{1,0:T(2,128)S(1)}, f32[2,256]{1,0:T(2,128)S(1)}, u32[]{:S(2)}, u32[]{:S(2)}) collective-permute-start(f32[2,256]{1,0:T(2,128)S(1)} %slice.50), channel_id=1, source_target_pairs={{0,4},{4,8},{8,12},{12,16},{16,20},{20,24},{24,28},{28,32},{32,36}... | collective-permute-start | bytes 6152 | tf_op jit(solution)/shard_map/ppermute | solution.py:336
  190.5 14.2 %collective-permute-start.10 = (bf16[256,512]{1,0:T(8,128)(2,1)}, bf16[256,512]{1,0:T(8,128)(2,1)S(1)}, u32[]{:S(2)}, u32[]{:S(2)}) collective-permute-start(bf16[256,512]{1,0:T(8,128)(2,1)} %combine.1.own_ref), channel_id=1, source_target_pairs={{0,1},{1,2},{2,3},{3,0},{4,5},{5,6},{6,7},{7,4},{8,9},{9,10},{10,1... | collective-permute-start | bytes 786440 | tf_op jit(solution)/shard_map/ppermute | solution.py:35
  190.5 14.2 %collective-permute-start.11 = (bf16[256,512]{1,0:T(8,128)(2,1)}, bf16[256,512]{1,0:T(8,128)(2,1)S(1)}, u32[]{:S(2)}, u32[]{:S(2)}) collective-permute-start(bf16[256,512]{1,0:T(8,128)(2,1)} %combine.1.own_ref), channel_id=1, source_target_pairs={{0,3},{1,0},{2,1},{3,2},{4,7},{5,4},{6,5},{7,6},{8,11},{9,8},{10,9... | collective-permute-start | bytes 786440 | tf_op jit(solution)/shard_map/ppermute | solution.py:35
  193.2 11.5 %collective-permute-start.12 = (bf16[256,512]{1,0:T(8,128)(2,1)}, bf16[256,512]{1,0:T(8,128)(2,1)S(1)}, u32[]{:S(2)}, u32[]{:S(2)}) collective-permute-start(bf16[256,512]{1,0:T(8,128)(2,1)} %combine.1.own_ref), channel_id=1, source_target_pairs={{0,2},{1,3},{2,0},{3,1},{4,6},{5,7},{6,4},{7,5},{8,10},{9,11},{10,... | collective-permute-start | bytes 786440 | tf_op jit(solution)/shard_map/ppermute | solution.py:35
  209.1 3.3 %collective-permute-start.14 = (bf16[1024,256]{1,0:T(8,128)(2,1)}, bf16[1024,256]{1,0:T(8,128)(2,1)S(1)}, u32[]{:S(2)}, u32[]{:S(2)}) collective-permute-start(bf16[1024,256]{1,0:T(8,128)(2,1)} %get-tuple-element.41), channel_id=1, source_target_pairs={{0,4},{4,0},{1,5},{5,1},{2,6},{6,2},{3,7},{7,3},{8,12},{12,8},{9,1... | collective-permute-start | bytes 1572872 | tf_op jit(solution)/shard_map/ppermute | solution.py:35
  214.4 21.2 %all-to-all-start.2 = ((bf16[32,32,256]{2,1,0:T(8,128)(2,1)}), bf16[32,32,256]{2,1,0:T(8,128)(2,1)S(1)}, u32[]{:S(2)}, u32[]{:S(2)}) async-start(bf16[32,32,256]{2,1,0:T(8,128)(2,1)} %bitcast.17), calls=%async_computation.2 | async-start | bytes 1048576 | tf_op jit(solution)/shard_map/all_to_all | solution.py:407
  227.2 5.7 %collective-permute-start.15 = (f32[2,256]{1,0:T(2,128)S(1)}, f32[2,256]{1,0:T(2,128)S(1)}, u32[]{:S(2)}, u32[]{:S(2)}) collective-permute-start(f32[2,256]{1,0:T(2,128)S(1)} %slice.44), channel_id=1, source_target_pairs={{4,0},{8,4},{12,8},{16,12},{20,16},{24,20},{28,24},{32,28},{36,32}... | collective-permute-start | bytes 6152 | tf_op jit(solution)/shard_map/ppermute | solution.py:336
  (9 other events, 28.2 us)

commit v2 on v1

v2 whole, which is shorter than its diff:
```python
import jax
import jax.numpy as jnp
from jax import lax
from jax.experimental import pallas as pl
from jax.experimental.pallas import tpu as pltpu
from jax.sharding import Mesh, PartitionSpec as P

BF = jnp.bfloat16
F32 = jnp.float32
SP = ("z", "x", "c")
MAIN = 8
VMEM_LIMIT = 56 * 1024 * 1024


def dot(a, b, contract):
    return lax.dot_general(a, b, ((contract[0], contract[1]), ((), ())), preferred_element_type=F32)


def nn(a, b):
    return dot(a, b, ((1,), (0,)))


def nt(a, b):
    return dot(a, b, ((1,), (1,)))


def tn(a, b):
    return dot(a, b, ((0,), (0,)))


def shifted(x, axis, by):
    n = lax.axis_size(axis)
    return lax.ppermute(x, axis, [(i, (i + by) % n) for i in range(n)])


def selection(row, base=0):
    n_rows = 64 * MAIN
    at = lax.broadcasted_iota(jnp.int32, (n_rows, row.shape[1]), 0)
    return at == (row + base)


def route_kernel(tp_ref, ids_ref, w_ref, h_ref, c_ref, hd_ref, cd_ref, out_ref, direct_ref, rows_ref):
    tokens = ids_ref.shape[1]
    expert = lax.broadcasted_iota(jnp.int32, (64, tokens), 0)
    upper = (
        lax.broadcasted_iota(jnp.int32, (tokens, tokens), 0)
        < lax.broadcasted_iota(jnp.int32, (tokens, tokens), 1)
    ).astype(F32).astype(BF)
    ids0, ids1 = ids_ref[0:1, :], ids_ref[1:2, :]
    hot0 = (expert == ids0).astype(F32)
    hot1 = (expert == ids1).astype(F32)
    before0 = nn(hot0.astype(BF), upper)
    before1 = nn(hot1.astype(BF), upper) + jnp.sum(hot0, axis=1, keepdims=True)
    pos0 = jnp.sum(hot0 * before0, axis=0, keepdims=True).astype(jnp.int32)
    pos1 = jnp.sum(hot1 * before1, axis=0, keepdims=True).astype(jnp.int32)
    w0, w1 = w_ref[0:1, :], w_ref[1:2, :]
    none = jnp.full_like(ids0, -64)
    a0 = jnp.where(pos0 < MAIN, ids0 * MAIN + pos0, none)
    a1 = jnp.where(pos1 < MAIN, ids1 * MAIN + pos1, none)
    b0 = jnp.where((pos0 >= MAIN) & (pos0 < MAIN + 4), ids0 * MAIN + pos0 - MAIN, none)
    b1 = jnp.where((pos1 >= MAIN) & (pos1 < MAIN + 4), ids1 * MAIN + pos1 - MAIN, none)
    rows_ref[0:1, :] = a0
    rows_ref[1:2, :] = a1
    rows_ref[2:3, :] = b0
    rows_ref[3:4, :] = b1

    def picked(r0, r1, base):
        s0, s1 = selection(r0, base), selection(r1, base)
        weight = jnp.sum(jnp.where(s0, w0, 0.0) + jnp.where(s1, w1, 0.0), axis=1, keepdims=True)
        return (s0 | s1).astype(F32).astype(BF), weight

    sel, weight = picked(a0, a1, 0)
    sel_h, _ = picked(b0, b1, 0)
    sel_s, weight_s = picked(b0, b1, 4)
    for h_in, c_in, to in ((h_ref, c_ref, out_ref), (hd_ref, cd_ref, direct_ref)):
        h, c = h_in[...], c_in[...]
        width = h.shape[1]
        to[:, 0:width] = nn(sel, h).astype(BF)
        to[:, width : 2 * width] = (nn(sel, c) * weight).astype(BF)
        to[:, 2 * width :] = (nn(sel_h, h) + nn(sel_s, c) * weight_s).astype(BF)


def route(tp, ids, weights, hidden_in, cotangent):
    tokens, width = hidden_in.shape
    direct = width // 4
    ring = (width - direct) // 4
    share = pl.BlockSpec((tokens, ring), lambda i, t: (0, t[0]))
    last = pl.BlockSpec((tokens, direct), lambda i, t: (0, 3))
    whole = lambda shape: pl.BlockSpec(shape, lambda i, t: (0, 0))
    return pl.pallas_call(
        route_kernel,
        grid_spec=pltpu.PrefetchScalarGridSpec(
            num_scalar_prefetch=1,
            grid=(1,),
            in_specs=[whole(ids.shape), whole(weights.shape), share, share, last, last],
            out_specs=[whole((64 * MAIN, 3 * ring)), whole((64 * MAIN, 3 * direct)), whole((4, tokens))],
        ),
        out_shape=[
            jax.ShapeDtypeStruct((64 * MAIN, 3 * ring), BF),
            jax.ShapeDtypeStruct((64 * MAIN, 3 * direct), BF),
            jax.ShapeDtypeStruct((4, tokens), jnp.int32),
        ],
        compiler_params=pltpu.CompilerParams(vmem_limit_bytes=VMEM_LIMIT),
        name="route",
    )(tp, ids, weights, hidden_in, cotangent, hidden_in, cotangent)


def combine_kernel(tp_ref, rows_ref, back_ref, c_ref, out_ref):
    width = c_ref.shape[1]
    a0, a1, b0, b1 = (rows_ref[k : k + 1, :] for k in range(4))

    def sel(r0, r1, base):
        return (selection(r0, base) | selection(r1, base)).astype(F32).astype(BF)

    main = tn(sel(a0, a1, 0), back_ref[:, 0:width])
    rest = back_ref[:, width:]
    low = tn(sel(b0, b1, 0), rest)
    high = tn(sel(b0, b1, 4), rest)
    half = width // 2
    out_ref[:, 0:half] = (c_ref[:, 0:half].astype(F32) + (main[:, 0:half] + low)).astype(BF)
    out_ref[:, half:] = (c_ref[:, half:].astype(F32) + (main[:, half:] + high)).astype(BF)


def combine(tp, rows, back, cotangent):
    tokens, width = cotangent.shape[0], cotangent.shape[1] // 4
    whole = lambda shape: pl.BlockSpec(shape, lambda i, t: (0, 0))
    return pl.pallas_call(
        combine_kernel,
        grid_spec=pltpu.PrefetchScalarGridSpec(
            num_scalar_prefetch=1,
            grid=(1,),
            in_specs=[
                whole(rows.shape),
                whole(back.shape),
                pl.BlockSpec((tokens, width), lambda i, t: (0, t[0])),
            ],
            out_specs=whole((tokens, width)),
        ),
        out_shape=jax.ShapeDtypeStruct((tokens, width), BF),
        compiler_params=pltpu.CompilerParams(vmem_limit_bytes=VMEM_LIMIT),
        name="combine",
    )(tp, rows, back, cotangent)


def block_at(tp, by):
    return lax.rem(tp + by, 4)


def vmem_specs(n):
    return [pl.BlockSpec(memory_space=pltpu.VMEM) for _ in range(n)]


def local_call(kernel, scalars, arrays, outs, scratch=()):
    return pl.pallas_call(
        kernel,
        in_specs=[pl.BlockSpec(memory_space=pltpu.SMEM)] + vmem_specs(len(arrays)),
        out_specs=vmem_specs(len(outs)),
        out_shape=[jax.ShapeDtypeStruct(shape, dtype) for shape, dtype in outs],
        scratch_shapes=list(scratch),
        compiler_params=pltpu.CompilerParams(vmem_limit_bytes=VMEM_LIMIT),
    )(scalars, *arrays)


def block_rows(tp, by, width):
    return pl.ds(pl.multiple_of(block_at(tp, by) * width, width), width)


def gather_products(sums, lo, x_ref, wg, wu, wd, first):
    ga, ua, da, gb, ub, db = sums
    width = x_ref.shape[1] // 3
    to = slice(lo, lo + x_ref.shape[0])
    h, s, m = x_ref[:, 0:width], x_ref[:, width : 2 * width], x_ref[:, 2 * width :]

    def add(ref, x):
        ref[to, :] = x if first else ref[to, :] + x

    add(ga, nn(h, wg))
    add(ua, nn(h, wu))
    add(da, nt(s, wd))
    add(gb, nn(m, wg))
    add(ub, nn(m, wu))
    add(db, nt(m, wd))


def early_kernel(tp_ref, own_ref, prev_ref, next_ref, wg_ref, wu_ref, wd_ref, *sums):
    tp = tp_ref[0]
    width = own_ref.shape[1] // 3
    for ref, by in ((own_ref, 0), (prev_ref, 3), (next_ref, 1)):
        at = block_rows(tp, by, width)
        gather_products(sums, 0, ref, wg_ref[at, :], wu_ref[at, :], wd_ref[:, at], by == 0)


def partial_rows(da, db, high_p, high_q, wg, wu):
    ff = wg.shape[1]
    cut = wg.shape[0] // 2
    main = nt(da[:, 0:ff], wg) + nt(da[:, ff : 2 * ff], wu)
    rest = nt(db[:, 0:ff], wg[0:cut]) + nt(db[:, ff : 2 * ff], wu[0:cut])
    rest = rest + nt(high_p, wg[cut:]) + nt(high_q, wu[cut:])
    return main.astype(BF), rest.astype(BF)


def write_rows(refs, main, rest):
    at = 0
    for ref in refs:
        n, width = ref.shape[0], main.shape[1]
        ref[:, 0:width] = main[at : at + n]
        ref[:, width:] = rest[at : at + n]
        at += n


def late_kernel(
    tp_ref, ga_in, ua_in, da_in, gb_in, ub_in, db_in, far_lo_ref, far_hi_ref, direct_ref,
    wg_ref, wu_ref, wd_ref, da_out, db_out, far_lo_out, far_hi_out, ga, ua, da, gb, ub, db,
):
    tp = tp_ref[0]
    n_rows = direct_ref.shape[0]
    model, ff = wg_ref.shape
    sums = (ga, ua, da, gb, ub, db)
    for ref, start in zip(sums, (ga_in, ua_in, da_in, gb_in, ub_in, db_in)):
        ref[...] = start[...]
    width = far_lo_ref.shape[1] // 3
    at = block_rows(tp, 2, width)
    wg, wu, wd = wg_ref[at, :], wu_ref[at, :], wd_ref[:, at]
    gather_products(sums, 0, far_lo_ref, wg, wu, wd, False)
    gather_products(sums, n_rows // 2, far_hi_ref, wg, wu, wd, False)
    at = slice(4 * width, model)
    gather_products(sums, 0, direct_ref, wg_ref[at, :], wu_ref[at, :], wd_ref[:, at], False)

    def local(g, u, d):
        sigma = 1.0 / (1.0 + jnp.exp(-g))
        silu = g * sigma
        return d * u * sigma * (1.0 + g * (1.0 - sigma)), d * silu, silu * u

    p, q, r = local(ga[...], ua[...], da[...])
    da_out[:, 0:ff] = p.astype(BF)
    da_out[:, ff : 2 * ff] = q.astype(BF)
    da_out[:, 2 * ff : 3 * ff] = r.astype(BF)
    keep = lax.rem(lax.broadcasted_iota(jnp.int32, (n_rows, ff), 0), 8) < 4
    p, q, r = local(gb[...], ub[...], pltpu.roll(db[...], n_rows - 4, 0))
    p, q, r = (jnp.where(keep, v, 0.0) for v in (p, q, r))
    db_out[:, 0:ff] = p.astype(BF)
    db_out[:, ff : 2 * ff] = q.astype(BF)
    db_out[:, 2 * ff : 3 * ff] = pltpu.roll(r, 4, 0).astype(BF)
    db_out[:, 3 * ff : 4 * ff] = pltpu.roll(p, 4, 0).astype(BF)
    db_out[:, 4 * ff :] = pltpu.roll(q, 4, 0).astype(BF)
    share = model // 4
    at = block_rows(tp, 2, share)
    high_p, high_q = db_out[:, 3 * ff : 4 * ff], db_out[:, 4 * ff :]
    write_rows(
        (far_lo_out, far_hi_out),
        *partial_rows(da_out, db_out, high_p, high_q, wg_ref[at, :], wu_ref[at, :]),
    )


def near_kernel(
    tp_ref, da, db, wg_ref, wu_ref, up_lo_out, up_hi_out, down_lo_out, down_hi_out, own_out
):
    tp = tp_ref[0]
    model, ff = wg_ref.shape
    high_p, high_q = db[:, 3 * ff : 4 * ff], db[:, 4 * ff :]
    for by, refs in ((1, (up_lo_out, up_hi_out)), (3, (down_lo_out, down_hi_out)), (0, (own_out,))):
        at = block_rows(tp, by, model // 4)
        write_rows(refs, *partial_rows(da, db, high_p, high_q, wg_ref[at, :], wu_ref[at, :]))


def weights_kernel(
    tp_ref, own_ref, prev_ref, next_ref, far_lo_ref, far_hi_ref, direct_ref, da_ref, db_ref,
    gg_ref, gu_ref, gd_ref,
):
    tp = tp_ref[0]
    width = own_ref.shape[1] // 3
    half = own_ref.shape[0] // 2
    ff, model = gd_ref.shape

    def sums(x_ref, lo):
        n, wide = x_ref.shape[0], x_ref.shape[1] // 3
        da, db = da_ref[lo : lo + n, :], db_ref[lo : lo + n, :]
        h, s, m = x_ref[:, 0:wide], x_ref[:, wide : 2 * wide], x_ref[:, 2 * wide :]
        both = tn(h, da[:, 0 : 2 * ff]) + tn(m, db[:, 0 : 2 * ff])
        down = tn(da[:, 2 * ff : 3 * ff], s) + tn(db[:, 2 * ff : 3 * ff], m)
        return both, down

    def put(at, both, down):
        gg_ref[at, :] = both[:, 0:ff].astype(BF)
        gu_ref[at, :] = both[:, ff:].astype(BF)
        gd_ref[:, at] = down.astype(BF)

    put(block_rows(tp, 0, width), *sums(own_ref, 0))
    put(block_rows(tp, 3, width), *sums(prev_ref, 0))
    put(block_rows(tp, 1, width), *sums(next_ref, 0))
    both, down = sums(far_lo_ref, 0)
    both_hi, down_hi = sums(far_hi_ref, half)
    put(block_rows(tp, 2, width), both + both_hi, down + down_hi)
    put(slice(4 * width, model), *sums(direct_ref, 0))


def mixer_kernel(
    where_ref, res_ref, wo_own, wo_prev, wo_next, wo_far, y_own, y_prev, y_next, y_far,
    dy_own, dy_prev, dy_next, dy_far, mine_ref, other_ref,
):
    tp, core = where_ref[0], where_ref[1]
    res = res_ref[...]
    width = res.shape[1]
    for w_ref, y_ref, dy_ref, by in (
        (wo_own, y_own, dy_own, 0),
        (wo_prev, y_prev, dy_prev, 3),
        (wo_next, y_next, dy_next, 1),
        (wo_far, y_far, dy_far, 2),
    ):
        dy_ref[...] = nn(res, w_ref[...]).astype(dy_ref.dtype)
        grad = tn(res, y_ref[...]).astype(BF).reshape(width // 64, 2, 32, y_ref.shape[1])
        low, high = grad[:, 0], grad[:, 1]
        shape = (width // 2, y_ref.shape[1])
        to = block_rows(tp, by, width // 2)
        first = core == 0
        mine_ref[to, :] = jnp.where(first, low, high).reshape(shape)
        other_ref[to, :] = jnp.where(first, high, low).reshape(shape)


def from_behind(x, by):
    n = lax.axis_size(SP)
    return lax.ppermute(x, SP, [(i, i + by) for i in range(n) if 0 <= i + by < n])


def ring(x):
    half = x.shape[0] // 2
    prev = shifted(x, "y", 1)
    after = shifted(x, "y", -1)
    return prev, after, shifted(prev[:half], "y", 1), shifted(after[half:], "y", -1)


def per_device(
    hidden_in, cotangent, routes, routing_weights, w_gate, w_up, w_down, b_gate, c_gate, x_in, taps, w_out
):
    tok_rows, model_width = hidden_in.shape
    share = model_width // 4
    chan = w_out.shape[1]
    y_at = lax.axis_index("y").astype(jnp.int32)
    tp = y_at.reshape(1)
    where = jnp.stack([y_at, lax.axis_index("c").astype(jnp.int32)])
    wg, wu, wd = w_gate[0], w_up[0], w_down[0]
    ff = wg.shape[1]

    sent, sent_direct, rows = route(tp, routes.T, routing_weights.T, hidden_in, cotangent)
    to_experts = lambda v: lax.all_to_all(
        v.reshape(64, MAIN, v.shape[1]), SP, split_axis=0, concat_axis=0, tiled=True
    ).reshape(v.shape)
    tail = slice(tok_rows - 2, tok_rows)
    earlier = from_behind(c_gate[tail].astype(F32) * x_in[tail].astype(F32), 1)
    sent, earlier = lax.optimization_barrier((sent, earlier))
    own = to_experts(sent)

    taps_f = taps.astype(F32)
    gated = c_gate.astype(F32) * x_in.astype(F32)
    padded = jnp.concatenate([earlier, gated], axis=0)
    conv = (
        taps_f[0] * padded[0:tok_rows]
        + taps_f[1] * padded[1 : tok_rows + 1]
        + taps_f[2] * padded[2 : tok_rows + 2]
    )
    y_short = (b_gate.astype(F32) * conv).astype(BF)
    y_blocks = (y_short, shifted(y_short, "y", 1), shifted(y_short, "y", -1), shifted(y_short, "y", 2))
    part = lambda by: lax.dynamic_slice_in_dim(w_out, lax.rem(y_at + by, 4) * share, share, 0)
    wo_blocks = (part(0), shifted(part(1), "y", 1), shifted(part(3), "y", -1), shifted(part(2), "y", 2))
    own, sent_direct, conv, *held = lax.optimization_barrier(
        (own, sent_direct, conv, *y_blocks, *wo_blocks)
    )
    y_blocks, wo_blocks = held[:4], held[4:]

    prev, after, far_lo, far_hi = ring(own)
    direct = to_experts(sent_direct)

    n_rows, half = own.shape[0], own.shape[0] // 2
    out_width = share + share // 2
    sums = local_call(early_kernel, tp, (own, prev, after, wg, wu, wd), [((n_rows, ff), F32)] * 6)
    da, db, f_lo, f_hi = local_call(
        late_kernel, tp, (*sums, far_lo, far_hi, direct, wg, wu, wd),
        [((n_rows, 3 * ff), BF), ((n_rows, 5 * ff), BF), ((half, out_width), BF), ((half, out_width), BF)],
        [pltpu.VMEM((n_rows, ff), F32)] * 6,
    )
    u_lo, u_hi, d_lo, d_hi, o = local_call(
        near_kernel, tp, (da, db, wg, wu),
        [((half, out_width), BF)] * 4 + [((n_rows, out_width), BF)],
    )

    from_prev = shifted(f_lo, "y", 1)
    from_next = shifted(f_hi, "y", -1)
    prev_hi = shifted(u_hi, "y", 1)
    next_lo = shifted(d_lo, "y", -1)
    added = lambda a, b: (a.astype(F32) + b.astype(F32)).astype(BF)
    prev_lo = shifted(added(u_lo, from_prev), "y", 1)
    next_hi = shifted(added(d_hi, from_next), "y", -1)
    got_prev = jnp.concatenate([prev_lo, prev_hi], axis=0).astype(F32)
    got_next = jnp.concatenate([next_lo, next_hi], axis=0).astype(F32)
    total = (o.astype(F32) + got_prev + got_next).astype(BF)
    back = to_experts(total)
    gg, gu, gd = local_call(
        weights_kernel, tp, (own, prev, after, far_lo, far_hi, direct, da, db),
        [((model_width, ff), BF), ((model_width, ff), BF), ((ff, model_width), BF)],
    )
    back, gg, gu, gd = lax.optimization_barrier((back, gg, gu, gd))

    residual_grad = combine(tp, rows, back, cotangent)
    dy, dy_prev, dy_next, dy_far, mine, other = local_call(
        mixer_kernel, where, (residual_grad, *wo_blocks, *y_blocks),
        [((tok_rows, chan), F32)] + [((tok_rows, chan), BF)] * 3 + [((2 * share, chan), BF)] * 2,
    )
    chip = added(mine, shifted(other, "c", 1)).reshape(32, 32, chan)
    d_y = (
        dy
        + shifted(dy_prev, "y", -1).astype(F32)
        + shifted(dy_next, "y", 1).astype(F32)
        + shifted(dy_far, "y", 2).astype(F32)
    )
    grad_b = (d_y * conv).astype(BF)
    d_conv = b_gate.astype(F32) * d_y
    following = from_behind(d_conv[0:2], -1)
    later = jnp.concatenate([d_conv, following], axis=0)
    d_v = (
        taps_f[2] * later[0:tok_rows]
        + taps_f[1] * later[1 : tok_rows + 1]
        + taps_f[0] * later[2 : tok_rows + 2]
    )
    grad_c = (d_v * x_in.astype(F32)).astype(BF)
    grad_x = (d_v * c_gate.astype(F32)).astype(BF)

    parts = lax.all_to_all(chip, ("z", "x"), split_axis=0, concat_axis=0, tiled=True)
    piece = jnp.sum(parts.astype(F32), axis=0)
    at = lambda z, x, c, y: ((z * 4 + x) * 2 + c) * 4 + y
    pairs = [
        (at(z, x, c, y), at(2 * y + z % 2, x, c, z // 2))
        for z in range(8) for x in range(4) for c in range(2) for y in range(4)
    ]
    out_proj_grad = lax.ppermute(piece, ("z", "x", "c", "y"), pairs)

    return (gg[None], gu[None], gd[None], out_proj_grad, residual_grad, grad_b, grad_c, grad_x)


def solution(mesh):
    fine = Mesh(mesh.devices.reshape(8, 4, 2, 4), ("z", "x", "c", "y"))
    rows = P(SP, None)
    both = P(SP, "y")
    return jax.shard_map(
        per_device,
        mesh=fine,
        in_specs=(
            rows, rows, rows, rows,
            P(SP, None, "y"), P(SP, None, "y"), P(SP, "y", None),
            both, both, both, P(None, "y"), P(None, "y"),
        ),
        out_specs=(P(SP, None, "y"), P(SP, None, "y"), P(SP, "y", None), both, both, both, both, both),
        check_vma=False,
    )
```

time: 237 us -> 223 us (0.941)
  the two profiles are of different devices: /device:TPU:1 before, /device:TPU:135 now
where the time goes in v2:
time: 223 us; the launch traced here: 222 us
  waiting for transfers between devices  90.2 us (40%)
  starting transfers between devices  79.5 us (36%)
  Pallas kernels  37.4 us (17%)
  other arithmetic  9.78 us (4%)
  local copies, waits for them, and re-layouts  4.62 us (2%)
    ppermute x20, waiting for transfers between devices, shifted(): return lax.ppermute(x, axis, [(i, (i + by) % n) for i in range(n)])  64.3 us
    all_to_all x3, starting transfers between devices, per_device(): lax.all_to_all(v.reshape(64, MAIN, v.shape[1]), SP, split_axis=0, concat_...  33.9 us
    pallas_call x5, Pallas kernels, local_call(): pl.pallas_call(kernel, in_specs=[pl.BlockSpec(memory_space=pltpu.SMEM)] +...  30.7 us
    ppermute x20, starting transfers between devices, shifted(): return lax.ppermute(x, axis, [(i, (i + by) % n) for i in range(n)])  27.9 us
    all_to_all x3, waiting for transfers between devices, per_device(): lax.all_to_all(v.reshape(64, MAIN, v.shape[1]), SP, split_axis=0, concat_...  13.8 us
    all_to_all x1, starting transfers between devices, per_device(): lax.all_to_all(chip, ('z', 'x'), split_axis=0, concat_axis=0, tiled=True)  9.35 us
    ppermute x1, waiting for transfers between devices, per_device(): out_proj_grad = lax.ppermute(piece, ('z', 'x', 'c', 'y'), pairs)  8.35 us
    ppermute x2, starting transfers between devices, from_behind(): lax.ppermute(x, SP, [(i, i + by) for i in range(n) if 0 <= i + by < n])  6.44 us
  transfers between devices with their start and end apart: 27, of which 15 were waited for; matrix products, arithmetic and copies ran while one was open for 3% of the time, Pallas kernels for 11%

profile of v2, /device:TPU:135, one launch (start us, length us, event | category | flops | bytes accessed | tf_op | source)
XLA Modules:
  0.0 222.5 jit_solution(7164077267014050518)
XLA Ops:
  4.5 4.2 %route.1 = (bf16[512,1152]{1,0:T(8,128)(2,1)}, bf16[512,1536]{1,0:T(8,128)(2,1)}, s32[4,256]{1,0:T(4,128)}) custom-call(s32[1]{0:T(128)} %bitcast.tp_ref, s32[2,256]{1,0:T(2,128)} %bitcast.44, f32[2,256]{1,0:T(2,128)} %bitcast.45, bf16[256,2048]{1,0:T(8,128)(2,1)} %hd_ref.1, bf16[256,2048]{1,0:T(8,128)(2,1)} %c_ref.3, bf16[256,2048]{1,0:T(8,128)(2,1)} %hd_ref.1, ...), custom_call_target="tpu_custom_call" | custom-call | tf_op jit(solution)/shard_map/route/pallas_call | solution.py:90
  8.6 10.4 %all-to-all-start = ((bf16[64,8,1152]{2,1,0:T(8,128)(2,1)}), bf16[64,8,1152]{2,1,0:T(8,128)(2,1)S(1)}, u32[]{:S(2)}, u32[]{:S(2)}) async-start(bf16[64,8,1152]{2,1,0:T(8,128)(2,1)} %bitcast.37), calls=%async_computation | async-start | bytes 2359296 | tf_op jit(solution)/shard_map/all_to_all | solution.py:345
  28.0 3.8 %collective-permute-done.3.y_far = bf16[256,256]{1,0:T(8,128)(2,1)S(1)} collective-permute-done((bf16[256,256]{1,0:T(8,128)(2,1)S(1)}, bf16[256,256]{1,0:T(8,128)(2,1)S(1)}, u32[]{:S(2)}, u32[]{:S(2)}) %collective-permute-start.3) | collective-permute-done | bytes 131104 | tf_op jit(solution)/shard_map/ppermute | solution.py:33
  33.1 7.5 %collective-permute-done.2.y_next = bf16[256,256]{1,0:T(8,128)(2,1)S(1)} collective-permute-done((bf16[256,256]{1,0:T(8,128)(2,1)S(1)}, bf16[256,256]{1,0:T(8,128)(2,1)S(1)}, u32[]{:S(2)}, u32[]{:S(2)}) %collective-permute-start.2) | collective-permute-done | bytes 131104 | tf_op jit(solution)/shard_map/ppermute | solution.py:33
  40.9 4.7 %all-to-all-done = bf16[64,8,1152]{2,1,0:T(8,128)(2,1)S(1)} async-done(((bf16[64,8,1152]{2,1,0:T(8,128)(2,1)}), bf16[64,8,1152]{2,1,0:T(8,128)(2,1)S(1)}, u32[]{:S(2)}, u32[]{:S(2)}) %all-to-all-start) | async-done | bytes 1179680 | tf_op jit(solution)/shard_map/all_to_all | solution.py:345
  45.7 10.6 %all-to-all-start.1 = ((bf16[64,8,1536]{2,1,0:T(8,128)(2,1)}), bf16[64,8,1536]{2,1,0:T(8,128)(2,1)S(1)}, u32[]{:S(2)}, u32[]{:S(2)}) async-start(bf16[64,8,1536]{2,1,0:T(8,128)(2,1)} %bitcast.36), calls=%async_computation.1 | async-start | bytes 3145728 | tf_op jit(solution)/shard_map/all_to_all | solution.py:345
  59.2 24.9 %collective-permute-done.8.next_ref = bf16[512,1152]{1,0:T(8,128)(2,1)S(1)} collective-permute-done((bf16[512,1152]{1,0:T(8,128)(2,1)S(1)}, bf16[512,1152]{1,0:T(8,128)(2,1)S(1)}, u32[]{:S(2)}, u32[]{:S(2)}) %collective-permute-start.8) | collective-permute-done | bytes 1179680 | tf_op jit(solution)/shard_map/ppermute | solution.py:33
  84.1 3.5 %collective-permute-start.10 = (bf16[256,1152]{1,0:T(8,128)(2,1)S(1)}, bf16[256,1152]{1,0:T(8,128)(2,1)S(1)}, u32[]{:S(2)}, u32[]{:S(2)}) collective-permute-start(bf16[256,1152]{1,0:T(8,128)(2,1)S(1)} %slice.57), channel_id=1, source_target_pairs={{0,3},{1,0},{2,1},{3,2},{4,7},{5,4},{6,5},{7,6},{8,11},{9,8},{10,9... | collective-permute-start | bytes 1769480 | tf_op jit(solution)/shard_map/ppermute | solution.py:33
  88.7 6.6 %shard_map.179 = (f32[512,256]{1,0:T(8,128)}, f32[512,256]{1,0:T(8,128)}, f32[512,256]{1,0:T(8,128)}, f32[512,256]{1,0:T(8,128)}, f32[512,256]{1,0:T(8,128)}, /*index=5*/f32[512,256]{1,0:T(8,128)}) custom-call(s32[1]{0:T(128)} %bitcast.tp_ref, bf16[512,1152]{1,0:T(8,128)(2,1)} %bitcast.25, bf16[512,1152]{1,0:T(8,128)(2,1)} %copy-done.3, ...), custom_call_target="tpu_custom_call" | custom-call | tf_op jit(solution)/shard_map/pallas_call | solution.py:154
  95.3 3.8 %collective-permute-done.10.far_hi_ref = bf16[256,1152]{1,0:T(8,128)(2,1)S(1)} collective-permute-done((bf16[256,1152]{1,0:T(8,128)(2,1)S(1)}, bf16[256,1152]{1,0:T(8,128)(2,1)S(1)}, u32[]{:S(2)}, u32[]{:S(2)}) %collective-permute-start.10) | collective-permute-done | bytes 589856 | tf_op jit(solution)/shard_map/ppermute | solution.py:33
  99.1 3.4 %collective-permute-done.9.far_lo_ref = bf16[256,1152]{1,0:T(8,128)(2,1)S(1)} collective-permute-done((bf16[256,1152]{1,0:T(8,128)(2,1)S(1)}, bf16[256,1152]{1,0:T(8,128)(2,1)S(1)}, u32[]{:S(2)}, u32[]{:S(2)}) %collective-permute-start.9) | collective-permute-done | bytes 589856 | tf_op jit(solution)/shard_map/ppermute | solution.py:33
  104.0 7.4 %shard_map.180 = (bf16[512,768]{1,0:T(8,128)(2,1)}, bf16[512,1280]{1,0:T(8,128)(2,1)}, bf16[256,768]{1,0:T(8,128)(2,1)}, bf16[256,768]{1,0:T(8,128)(2,1)}) custom-call(s32[1]{0:T(128)} %bitcast.tp_ref, f32[512,256]{1,0:T(8,128)} %get-tuple-element.57.ga_in, f32[512,256]{1,0:T(8,128)} %get-tuple-element.58.ua_in, f32[512,256]{1,0:T(8,128)} %get-tuple-element.59.da_in, ...), custom_call_target="tpu_custom_call" | custom-call | tf_op jit(solution)/shard_map/pallas_call | solution.py:154
  114.1 4.9 %shard_map.181 = (bf16[256,768]{1,0:T(8,128)(2,1)}, bf16[256,768]{1,0:T(8,128)(2,1)}, bf16[256,768]{1,0:T(8,128)(2,1)}, bf16[256,768]{1,0:T(8,128)(2,1)}, bf16[512,768]{1,0:T(8,128)(2,1)}) custom-call(s32[1]{0:T(128)} %bitcast.tp_ref, bf16[512,768]{1,0:T(8,128)(2,1)} %get-tuple-element.64.da.da_ref, bf16[512,1280]{1,0:T(8,128)(2,1)} %get-tuple-element.65.db.db_ref, ...), custom_call_target="tpu_custom_call" | custom-call | tf_op jit(solution)/shard_map/pallas_call | solution.py:154
  126.7 3.2 %collective-permute-done.13 = bf16[256,768]{1,0:T(8,128)(2,1)S(1)} collective-permute-done((bf16[256,768]{1,0:T(8,128)(2,1)}, bf16[256,768]{1,0:T(8,128)(2,1)S(1)}, u32[]{:S(2)}, u32[]{:S(2)}) %collective-permute-start.13) | collective-permute-done | bytes 393248 | tf_op jit(solution)/shard_map/ppermute | solution.py:33
  129.8 8.4 %collective-permute-done.12 = bf16[256,768]{1,0:T(8,128)(2,1)S(1)} collective-permute-done((bf16[256,768]{1,0:T(8,128)(2,1)S(1)}, bf16[256,768]{1,0:T(8,128)(2,1)S(1)}, u32[]{:S(2)}, u32[]{:S(2)}) %collective-permute-start.12) | collective-permute-done | bytes 393248 | tf_op jit(solution)/shard_map/ppermute | solution.py:33
  139.5 12.9 %all-to-all-start.2 = ((bf16[64,8,768]{2,1,0:T(8,128)(2,1)}), bf16[64,8,768]{2,1,0:T(8,128)(2,1)S(1)}, u32[]{:S(2)}, u32[]{:S(2)}) async-start(bf16[64,8,768]{2,1,0:T(8,128)(2,1)} %fusion), calls=%async_computation.2 | async-start | bytes 1572864 | tf_op jit(solution)/shard_map/all_to_all | solution.py:345
  152.9 8.5 %shard_map.182 = (bf16[2048,256]{1,0:T(8,128)(2,1)}, bf16[2048,256]{1,0:T(8,128)(2,1)}, bf16[256,2048]{1,0:T(8,128)(2,1)}) custom-call(s32[1]{0:T(128)} %bitcast.tp_ref, bf16[512,1152]{1,0:T(8,128)(2,1)} %bitcast.26, bf16[512,1152]{1,0:T(8,128)(2,1)} %copy-done.3, bf16[512,1152]{1,0:T(8,128)(2,1)} %copy-done.2, bf16[256,1152]{1,0:T(8,128)(2,1)} %copy-done.6, ...), custom_call_target="tpu_custom_call" | custom-call | tf_op jit(solution)/shard_map/pallas_call | solution.py:154
  161.5 9.1 %all-to-all-done.2 = bf16[64,8,768]{2,1,0:T(8,128)(2,1)S(1)} async-done(((bf16[64,8,768]{2,1,0:T(8,128)(2,1)}), bf16[64,8,768]{2,1,0:T(8,128)(2,1)S(1)}, u32[]{:S(2)}, u32[]{:S(2)}) %all-to-all-start.2) | async-done | bytes 786464 | tf_op jit(solution)/shard_map/all_to_all | solution.py:345
  174.0 3.2 %shard_map.183 = (f32[256,256]{1,0:T(8,128)}, bf16[256,256]{1,0:T(8,128)(2,1)}, bf16[256,256]{1,0:T(8,128)(2,1)}, bf16[256,256]{1,0:T(8,128)(2,1)}, bf16[1024,25...) custom-call(s32[2]{0:T(128)} %pad_add_fusion.where_ref, bf16[256,512]{1,0:T(8,128)(2,1)} %combine.1.res_ref, ...), custom_call_target="tpu_custom_call" | custom-call | tf_op jit(solution)/shard_map/pallas_call | solution.py:154
  181.6 9.3 %all-to-all-start.3 = ((bf16[32,32,256]{2,1,0:T(8,128)(2,1)}), bf16[32,32,256]{2,1,0:T(8,128)(2,1)S(1)}, u32[]{:S(2)}, u32[]{:S(2)}) async-start(bf16[32,32,256]{2,1,0:T(8,128)(2,1)} %bitcast.19), calls=%async_computation.3 | async-start | bytes 1048576 | tf_op jit(solution)/shard_map/all_to_all | solution.py:427
  195.7 6.6 %collective-permute-done.20 = bf16[256,256]{1,0:T(8,128)(2,1)S(1)} collective-permute-done((bf16[256,256]{1,0:T(8,128)(2,1)S(1)}, bf16[256,256]{1,0:T(8,128)(2,1)S(1)}, u32[]{:S(2)}, u32[]{:S(2)}) %collective-permute-start.20) | collective-permute-done | bytes 131104 | tf_op jit(solution)/shard_map/ppermute | solution.py:33
  203.0 3.3 %collective-permute-start.22 = (f32[2,256]{1,0:T(2,128)S(1)}, f32[2,256]{1,0:T(2,128)S(1)}, u32[]{:S(2)}, u32[]{:S(2)}) collective-permute-start(f32[2,256]{1,0:T(2,128)S(1)} %slice.58), channel_id=1, source_target_pairs={{4,0},{8,4},{12,8},{16,12},{20,16},{24,20},{28,24},{32,28},{36,32}... | collective-permute-start | bytes 6152 | tf_op jit(solution)/shard_map/ppermute | solution.py:322
  206.4 3.7 %collective-permute-done.22 = f32[2,256]{1,0:T(2,128)S(1)} collective-permute-done((f32[2,256]{1,0:T(2,128)S(1)}, f32[2,256]{1,0:T(2,128)S(1)}, u32[]{:S(2)}, u32[]{:S(2)}) %collective-permute-start.22) | collective-permute-done | bytes 2080 | tf_op jit(solution)/shard_map/ppermute | solution.py:322
  213.5 8.3 %collective-permute-done.18 = f32[32,256]{1,0:T(8,128)S(1)} collective-permute-done((f32[32,256]{1,0:T(8,128)S(1)}, f32[32,256]{1,0:T(8,128)S(1)}, u32[]{:S(2)}, u32[]{:S(2)}) %collective-permute-start.18) | collective-permute-done | bytes 32800 | tf_op jit(solution)/shard_map/ppermute | solution.py:434
  (109 shorter events, 49.2 us)
Async XLA Ops:
  1.3 7.3 %collective-permute-start = (f32[2,256]{1,0:T(2,128)S(1)}, f32[2,256]{1,0:T(2,128)S(1)}, u32[]{:S(2)}, u32[]{:S(2)}) collective-permute-start(f32[2,256]{1,0:T(2,128)S(1)} %convert_multiply_fusion.5), channel_id=1, source_target_pairs={{0,4},{4,8},{8,12},{12,16},{16,20},{20,24},{24,28},{28,32},{32,36}... | collective-permute-start | bytes 6152 | tf_op jit(solution)/shard_map/ppermute | solution.py:322
  8.6 37.0 %all-to-all-start = ((bf16[64,8,1152]{2,1,0:T(8,128)(2,1)}), bf16[64,8,1152]{2,1,0:T(8,128)(2,1)S(1)}, u32[]{:S(2)}, u32[]{:S(2)}) async-start(bf16[64,8,1152]{2,1,0:T(8,128)(2,1)} %bitcast.37), calls=%async_computation | async-start | bytes 2359296 | tf_op jit(solution)/shard_map/all_to_all | solution.py:345
  19.9 21.0 %collective-permute-start.6 = (bf16[512,256]{1,0:T(8,128)(2,1)S(1)}, bf16[512,256]{1,0:T(8,128)(2,1)S(1)}, u32[]{:S(2)}, u32[]{:S(2)}) collective-permute-start(bf16[512,256]{1,0:T(8,128)(2,1)S(1)} %get-tuple-element.100), channel_id=1, source_target_pairs={{0,2},{1,3},{2,0},{3,1},{4,6},{5,7},{6,4},{7,5},{8,10},{9,11},{10,... | collective-permute-start | bytes 786440 | tf_op jit(solution)/shard_map/ppermute | solution.py:33
  23.7 8.0 %collective-permute-start.3 = (bf16[256,256]{1,0:T(8,128)(2,1)S(1)}, bf16[256,256]{1,0:T(8,128)(2,1)S(1)}, u32[]{:S(2)}, u32[]{:S(2)}) collective-permute-start(bf16[256,256]{1,0:T(8,128)(2,1)S(1)} %get-tuple-element.85.y_own), channel_id=1, source_target_pairs={{0,2},{1,3},{2,0},{3,1},{4,6},{5,7},{6,4},{7,5},{8,10},{9,11},{10,... | collective-permute-start | bytes 393224 | tf_op jit(solution)/shard_map/ppermute | solution.py:33
  23.9 17.0 %collective-permute-start.4 = (bf16[512,256]{1,0:T(8,128)(2,1)S(1)}, bf16[512,256]{1,0:T(8,128)(2,1)S(1)}, u32[]{:S(2)}, u32[]{:S(2)}) collective-permute-start(bf16[512,256]{1,0:T(8,128)(2,1)S(1)} %get-tuple-element.101), channel_id=1, source_target_pairs={{0,1},{1,2},{2,3},{3,0},{4,5},{5,6},{6,7},{7,4},{8,9},{9,10},{10,1... | collective-permute-start | bytes 786440 | tf_op jit(solution)/shard_map/ppermute | solution.py:33
  25.1 15.8 %collective-permute-start.5 = (bf16[512,256]{1,0:T(8,128)(2,1)S(1)}, bf16[512,256]{1,0:T(8,128)(2,1)S(1)}, u32[]{:S(2)}, u32[]{:S(2)}) collective-permute-start(bf16[512,256]{1,0:T(8,128)(2,1)S(1)} %get-tuple-element.103), channel_id=1, source_target_pairs={{0,3},{1,0},{2,1},{3,2},{4,7},{5,4},{6,5},{7,6},{8,11},{9,8},{10,9... | collective-permute-start | bytes 786440 | tf_op jit(solution)/shard_map/ppermute | solution.py:33
  26.6 13.9 %collective-permute-start.2 = (bf16[256,256]{1,0:T(8,128)(2,1)S(1)}, bf16[256,256]{1,0:T(8,128)(2,1)S(1)}, u32[]{:S(2)}, u32[]{:S(2)}) collective-permute-start(bf16[256,256]{1,0:T(8,128)(2,1)S(1)} %get-tuple-element.85.y_own), channel_id=1, source_target_pairs={{0,3},{1,0},{2,1},{3,2},{4,7},{5,4},{6,5},{7,6},{8,11},{9,8},{10,9... | collective-permute-start | bytes 393224 | tf_op jit(solution)/shard_map/ppermute | solution.py:33
  31.8 9.1 %collective-permute-start.1 = (bf16[256,256]{1,0:T(8,128)(2,1)S(1)}, bf16[256,256]{1,0:T(8,128)(2,1)S(1)}, u32[]{:S(2)}, u32[]{:S(2)}) collective-permute-start(bf16[256,256]{1,0:T(8,128)(2,1)S(1)} %get-tuple-element.85.y_own), channel_id=1, source_target_pairs={{0,1},{1,2},{2,3},{3,0},{4,5},{5,6},{6,7},{7,4},{8,9},{9,10},{10,1... | collective-permute-start | bytes 393224 | tf_op jit(solution)/shard_map/ppermute | solution.py:33
  45.7 56.8 %all-to-all-start.1 = ((bf16[64,8,1536]{2,1,0:T(8,128)(2,1)}), bf16[64,8,1536]{2,1,0:T(8,128)(2,1)S(1)}, u32[]{:S(2)}, u32[]{:S(2)}) async-start(bf16[64,8,1536]{2,1,0:T(8,128)(2,1)} %bitcast.36), calls=%async_computation.1 | async-start | bytes 3145728 | tf_op jit(solution)/shard_map/all_to_all | solution.py:345
  56.3 27.8 %collective-permute-start.8 = (bf16[512,1152]{1,0:T(8,128)(2,1)S(1)}, bf16[512,1152]{1,0:T(8,128)(2,1)S(1)}, u32[]{:S(2)}, u32[]{:S(2)}) collective-permute-start(bf16[512,1152]{1,0:T(8,128)(2,1)S(1)} %bitcast.23), channel_id=1, source_target_pairs={{0,3},{1,0},{2,1},{3,2},{4,7},{5,4},{6,5},{7,6},{8,11},{9,8},{10,9... | collective-permute-start | bytes 3538952 | tf_op jit(solution)/shard_map/ppermute | solution.py:33
  59.2 28.5 %collective-permute-start.7 = (bf16[512,1152]{1,0:T(8,128)(2,1)S(1)}, bf16[512,1152]{1,0:T(8,128)(2,1)S(1)}, u32[]{:S(2)}, u32[]{:S(2)}) collective-permute-start(bf16[512,1152]{1,0:T(8,128)(2,1)S(1)} %bitcast.24), channel_id=1, source_target_pairs={{0,1},{1,2},{2,3},{3,0},{4,5},{5,6},{6,7},{7,4},{8,9},{9,10},{10,1... | collective-permute-start | bytes 3538952 | tf_op jit(solution)/shard_map/ppermute | solution.py:33
  84.1 14.9 %collective-permute-start.10 = (bf16[256,1152]{1,0:T(8,128)(2,1)S(1)}, bf16[256,1152]{1,0:T(8,128)(2,1)S(1)}, u32[]{:S(2)}, u32[]{:S(2)}) collective-permute-start(bf16[256,1152]{1,0:T(8,128)(2,1)S(1)} %slice.57), channel_id=1, source_target_pairs={{0,3},{1,0},{2,1},{3,2},{4,7},{5,4},{6,5},{7,6},{8,11},{9,8},{10,9... | collective-permute-start | bytes 1769480 | tf_op jit(solution)/shard_map/ppermute | solution.py:33
  87.7 14.8 %collective-permute-start.9 = (bf16[256,1152]{1,0:T(8,128)(2,1)S(1)}, bf16[256,1152]{1,0:T(8,128)(2,1)S(1)}, u32[]{:S(2)}, u32[]{:S(2)}) collective-permute-start(bf16[256,1152]{1,0:T(8,128)(2,1)S(1)} %slice.56), channel_id=1, source_target_pairs={{0,1},{1,2},{2,3},{3,0},{4,5},{5,6},{6,7},{7,4},{8,9},{9,10},{10,1... | collective-permute-start | bytes 1769480 | tf_op jit(solution)/shard_map/ppermute | solution.py:33
  111.4 10.3 %collective-permute-start.11 = (bf16[256,768]{1,0:T(8,128)(2,1)}, bf16[256,768]{1,0:T(8,128)(2,1)S(1)}, u32[]{:S(2)}, u32[]{:S(2)}) collective-permute-start(bf16[256,768]{1,0:T(8,128)(2,1)} %get-tuple-element.68), channel_id=1, source_target_pairs={{0,1},{1,2},{2,3},{3,0},{4,5},{5,6},{6,7},{7,4},{8,9},{9,10},{10,1... | collective-permute-start | bytes 1179656 | tf_op jit(solution)/shard_map/ppermute | solution.py:33
  111.4 11.4 %collective-permute-start.15 = (bf16[256,768]{1,0:T(8,128)(2,1)}, bf16[256,768]{1,0:T(8,128)(2,1)S(1)}, u32[]{:S(2)}, u32[]{:S(2)}) collective-permute-start(bf16[256,768]{1,0:T(8,128)(2,1)} %get-tuple-element.72), channel_id=1, source_target_pairs={{0,3},{1,0},{2,1},{3,2},{4,7},{5,4},{6,5},{7,6},{8,11},{9,8},{10,9... | collective-permute-start | bytes 1179656 | tf_op jit(solution)/shard_map/ppermute | solution.py:33
  119.0 10.9 %collective-permute-start.13 = (bf16[256,768]{1,0:T(8,128)(2,1)}, bf16[256,768]{1,0:T(8,128)(2,1)S(1)}, u32[]{:S(2)}, u32[]{:S(2)}) collective-permute-start(bf16[256,768]{1,0:T(8,128)(2,1)} %get-tuple-element.69), channel_id=1, source_target_pairs={{0,1},{1,2},{2,3},{3,0},{4,5},{5,6},{6,7},{7,4},{8,9},{9,10},{10,1... | collective-permute-start | bytes 1179656 | tf_op jit(solution)/shard_map/ppermute | solution.py:33
  119.0 10.9 %collective-permute-start.14 = (bf16[256,768]{1,0:T(8,128)(2,1)}, bf16[256,768]{1,0:T(8,128)(2,1)S(1)}, u32[]{:S(2)}, u32[]{:S(2)}) collective-permute-start(bf16[256,768]{1,0:T(8,128)(2,1)} %get-tuple-element.70), channel_id=1, source_target_pairs={{0,3},{1,0},{2,1},{3,2},{4,7},{5,4},{6,5},{7,6},{8,11},{9,8},{10,9... | collective-permute-start | bytes 1179656 | tf_op jit(solution)/shard_map/ppermute | solution.py:33
  122.7 15.5 %collective-permute-start.12 = (bf16[256,768]{1,0:T(8,128)(2,1)S(1)}, bf16[256,768]{1,0:T(8,128)(2,1)S(1)}, u32[]{:S(2)}, u32[]{:S(2)}) collective-permute-start(bf16[256,768]{1,0:T(8,128)(2,1)S(1)} %add_convert_fusion.3), channel_id=1, source_target_pairs={{0,1},{1,2},{2,3},{3,0},{4,5},{5,6},{6,7},{7,4},{8,9},{9,10},{10,1... | collective-permute-start | bytes 1179656 | tf_op jit(solution)/shard_map/ppermute | solution.py:33
  123.9 14.3 %collective-permute-start.16 = (bf16[256,768]{1,0:T(8,128)(2,1)S(1)}, bf16[256,768]{1,0:T(8,128)(2,1)S(1)}, u32[]{:S(2)}, u32[]{:S(2)}) collective-permute-start(bf16[256,768]{1,0:T(8,128)(2,1)S(1)} %add_convert_fusion.2), channel_id=1, source_target_pairs={{0,3},{1,0},{2,1},{3,2},{4,7},{5,4},{6,5},{7,6},{8,11},{9,8},{10,9... | collective-permute-start | bytes 1179656 | tf_op jit(solution)/shard_map/ppermute | solution.py:33
  139.5 31.1 %all-to-all-start.2 = ((bf16[64,8,768]{2,1,0:T(8,128)(2,1)}), bf16[64,8,768]{2,1,0:T(8,128)(2,1)S(1)}, u32[]{:S(2)}, u32[]{:S(2)}) async-start(bf16[64,8,768]{2,1,0:T(8,128)(2,1)} %fusion), calls=%async_computation.2 | async-start | bytes 1572864 | tf_op jit(solution)/shard_map/all_to_all | solution.py:345
  181.6 29.2 %all-to-all-start.3 = ((bf16[32,32,256]{2,1,0:T(8,128)(2,1)}), bf16[32,32,256]{2,1,0:T(8,128)(2,1)S(1)}, u32[]{:S(2)}, u32[]{:S(2)}) async-start(bf16[32,32,256]{2,1,0:T(8,128)(2,1)} %bitcast.19), calls=%async_computation.3 | async-start | bytes 1048576 | tf_op jit(solution)/shard_map/all_to_all | solution.py:427
  193.8 8.5 %collective-permute-start.20 = (bf16[256,256]{1,0:T(8,128)(2,1)S(1)}, bf16[256,256]{1,0:T(8,128)(2,1)S(1)}, u32[]{:S(2)}, u32[]{:S(2)}) collective-permute-start(bf16[256,256]{1,0:T(8,128)(2,1)S(1)} %copy-done.25), channel_id=1, source_target_pairs={{0,1},{1,2},{2,3},{3,0},{4,5},{5,6},{6,7},{7,4},{8,9},{9,10},{10,1... | collective-permute-start | bytes 393224 | tf_op jit(solution)/shard_map/ppermute | solution.py:33
  193.8 8.5 %collective-permute-start.21 = (bf16[256,256]{1,0:T(8,128)(2,1)S(1)}, bf16[256,256]{1,0:T(8,128)(2,1)S(1)}, u32[]{:S(2)}, u32[]{:S(2)}) collective-permute-start(bf16[256,256]{1,0:T(8,128)(2,1)S(1)} %copy-done.24), channel_id=1, source_target_pairs={{0,2},{1,3},{2,0},{3,1},{4,6},{5,7},{6,4},{7,5},{8,10},{9,11},{10,... | collective-permute-start | bytes 393224 | tf_op jit(solution)/shard_map/ppermute | solution.py:33
  210.9 11.0 %collective-permute-start.18 = (f32[32,256]{1,0:T(8,128)S(1)}, f32[32,256]{1,0:T(8,128)S(1)}, u32[]{:S(2)}, u32[]{:S(2)}) collective-permute-start(f32[32,256]{1,0:T(8,128)S(1)} %convert_reduce_fusion), channel_id=1, source_target_pairs={{0,0},{1,64},{2,128},{3,192},{4,4},{5,68},{6,132},{7,196},{8,8},{9... | collective-permute-start | bytes 98312 | tf_op jit(solution)/shard_map/ppermute | solution.py:434
  (30 other events, 326.9 us)

commit v3 on v2

--- a/solution.py
+++ b/solution.py
@@ -10,6 +10,7 @@
 SP = ("z", "x", "c")
 MAIN = 8
 VMEM_LIMIT = 56 * 1024 * 1024
+SMALL_LIMIT = 20 * 1024 * 1024
 
 
 def dot(a, b, contract):
@@ -105,7 +106,10 @@
     )(tp, ids, weights, hidden_in, cotangent, hidden_in, cotangent)
 
 
-def combine_kernel(tp_ref, rows_ref, back_ref, c_ref, out_ref):
+def combine_kernel(
+    tp_ref, rows_ref, back_ref, c_ref, wo_own, wo_prev, wo_next, wo_far,
+    out_ref, dy_own, dy_prev, dy_next, dy_far,
+):
     width = c_ref.shape[1]
     a0, a1, b0, b1 = (rows_ref[k : k + 1, :] for k in range(4))
 
@@ -119,10 +123,14 @@
     half = width // 2
     out_ref[:, 0:half] = (c_ref[:, 0:half].astype(F32) + (main[:, 0:half] + low)).astype(BF)
     out_ref[:, half:] = (c_ref[:, half:].astype(F32) + (main[:, half:] + high)).astype(BF)
-
-
-def combine(tp, rows, back, cotangent):
+    res = out_ref[...]
+    for w_ref, dy in ((wo_own, dy_own), (wo_prev, dy_prev), (wo_next, dy_next), (wo_far, dy_far)):
+        dy[...] = nn(res, w_ref[...]).astype(dy.dtype)
+
+
+def combine(tp, rows, back, cotangent, wo_blocks):
     tokens, width = cotangent.shape[0], cotangent.shape[1] // 4
+    chan = wo_blocks[0].shape[1]
     whole = lambda shape: pl.BlockSpec(shape, lambda i, t: (0, 0))
     return pl.pallas_call(
         combine_kernel,
@@ -133,13 +141,15 @@
                 whole(rows.shape),
                 whole(back.shape),
                 pl.BlockSpec((tokens, width), lambda i, t: (0, t[0])),
-            ],
-            out_specs=whole((tokens, width)),
+            ]
+            + [whole((width, chan))] * 4,
+            out_specs=[whole((tokens, width))] + [whole((tokens, chan))] * 4,
         ),
-        out_shape=jax.ShapeDtypeStruct((tokens, width), BF),
-        compiler_params=pltpu.CompilerParams(vmem_limit_bytes=VMEM_LIMIT),
+        out_shape=[jax.ShapeDtypeStruct((tokens, width), BF), jax.ShapeDtypeStruct((tokens, chan), F32)]
+        + [jax.ShapeDtypeStruct((tokens, chan), BF)] * 3,
+        compiler_params=pltpu.CompilerParams(vmem_limit_bytes=SMALL_LIMIT),
         name="combine",
-    )(tp, rows, back, cotangent)
+    )(tp, rows, back, in_hbm(cotangent), *map(in_hbm, wo_blocks))
 
 
 def block_at(tp, by):
@@ -150,14 +160,17 @@
     return [pl.BlockSpec(memory_space=pltpu.VMEM) for _ in range(n)]
 
 
-def local_call(kernel, scalars, arrays, outs, scratch=()):
+def in_hbm(x):
+    return pltpu.with_memory_space_constraint(x, pltpu.HBM)
+
+
+def local_call(kernel, scalars, arrays, outs, limit=VMEM_LIMIT):
     return pl.pallas_call(
         kernel,
         in_specs=[pl.BlockSpec(memory_space=pltpu.SMEM)] + vmem_specs(len(arrays)),
         out_specs=vmem_specs(len(outs)),
         out_shape=[jax.ShapeDtypeStruct(shape, dtype) for shape, dtype in outs],
-        scratch_shapes=list(scratch),
-        compiler_params=pltpu.CompilerParams(vmem_limit_bytes=VMEM_LIMIT),
+        compiler_params=pltpu.CompilerParams(vmem_limit_bytes=limit),
     )(scalars, *arrays)
 
 
@@ -209,47 +222,84 @@
 
 
 def late_kernel(
-    tp_ref, ga_in, ua_in, da_in, gb_in, ub_in, db_in, far_lo_ref, far_hi_ref, direct_ref,
-    wg_ref, wu_ref, wd_ref, da_out, db_out, far_lo_out, far_hi_out, ga, ua, da, gb, ub, db,
+    tp_ref, ga_in, ua_in, da_in, gb_in, ub_in, db_in, far_lo_in, far_hi_in, direct_in,
+    wg_in, wu_in, wd_in, da_out, db_out, far_lo_out, far_hi_out,
+    ga, ua, da, gb, ub, db, ga_s, ua_s, da_s, gb_s, ub_s, db_s,
+    far, wg_d, wu_d, wd_d, wg_f, wu_f, wd_f, wg_o, wu_o, sems,
 ):
     tp = tp_ref[0]
-    n_rows = direct_ref.shape[0]
-    model, ff = wg_ref.shape
+    n_rows, ff = ga.shape
+    half = n_rows // 2
+    width, tail = wg_f.shape[0], wg_d.shape[0]
+    last = slice(4 * width, 4 * width + tail)
+    opposite = block_rows(tp, 2, width)
+    share = block_rows(tp, 2, wg_o.shape[0])
+    moves = [
+        (wg_in.at[last, :], wg_d), (wu_in.at[last, :], wu_d), (wd_in.at[:, last], wd_d),
+        (far_lo_in, far.at[0:half, :]), (far_hi_in, far.at[half:n_rows, :]),
+        (wg_in.at[opposite, :], wg_f), (wu_in.at[opposite, :], wu_f), (wd_in.at[:, opposite], wd_f),
+        (ga_in, ga_s), (ua_in, ua_s), (da_in, da_s), (gb_in, gb_s), (ub_in, ub_s), (db_in, db_s),
+        (wg_in.at[share, :], wg_o), (wu_in.at[share, :], wu_o),
+    ]
+    copies = [pltpu.make_async_copy(src, dst, sems.at[k]) for k, (src, dst) in enumerate(moves)]
+    for copy in copies:
+        copy.start()
     sums = (ga, ua, da, gb, ub, db)
-    for ref, start in zip(sums, (ga_in, ua_in, da_in, gb_in, ub_in, db_in)):
-        ref[...] = start[...]
-    width = far_lo_ref.shape[1] // 3
-    at = block_rows(tp, 2, width)
-    wg, wu, wd = wg_ref[at, :], wu_ref[at, :], wd_ref[:, at]
-    gather_products(sums, 0, far_lo_ref, wg, wu, wd, False)
-    gather_products(sums, n_rows // 2, far_hi_ref, wg, wu, wd, False)
-    at = slice(4 * width, model)
-    gather_products(sums, 0, direct_ref, wg_ref[at, :], wu_ref[at, :], wd_ref[:, at], False)
+    for copy in copies[0:3]:
+        copy.wait()
+    gather_products(sums, 0, direct_in, wg_d[...], wu_d[...], wd_d[...], True)
+    for copy in copies[3:8]:
+        copy.wait()
+    gather_products(sums, 0, far, wg_f[...], wu_f[...], wd_f[...], False)
+    for copy in copies[8:16]:
+        copy.wait()
 
     def local(g, u, d):
         sigma = 1.0 / (1.0 + jnp.exp(-g))
         silu = g * sigma
         return d * u * sigma * (1.0 + g * (1.0 - sigma)), d * silu, silu * u
 
-    p, q, r = local(ga[...], ua[...], da[...])
+    p, q, r = local(ga[...] + ga_s[...], ua[...] + ua_s[...], da[...] + da_s[...])
     da_out[:, 0:ff] = p.astype(BF)
     da_out[:, ff : 2 * ff] = q.astype(BF)
     da_out[:, 2 * ff : 3 * ff] = r.astype(BF)
     keep = lax.rem(lax.broadcasted_iota(jnp.int32, (n_rows, ff), 0), 8) < 4
-    p, q, r = local(gb[...], ub[...], pltpu.roll(db[...], n_rows - 4, 0))
+    p, q, r = local(gb[...] + gb_s[...], ub[...] + ub_s[...], pltpu.roll(db[...] + db_s[...], n_rows - 4, 0))
     p, q, r = (jnp.where(keep, v, 0.0) for v in (p, q, r))
     db_out[:, 0:ff] = p.astype(BF)
     db_out[:, ff : 2 * ff] = q.astype(BF)
     db_out[:, 2 * ff : 3 * ff] = pltpu.roll(r, 4, 0).astype(BF)
     db_out[:, 3 * ff : 4 * ff] = pltpu.roll(p, 4, 0).astype(BF)
     db_out[:, 4 * ff :] = pltpu.roll(q, 4, 0).astype(BF)
+    high_p, high_q = db_out[:, 3 * ff : 4 * ff], db_out[:, 4 * ff :]
+    write_rows((far_lo_out, far_hi_out), *partial_rows(da_out, db_out, high_p, high_q, wg_o[...], wu_o[...]))
+
+
+def late(tp, sums, far_lo, far_hi, direct, wg, wu, wd):
+    n_rows, ff = sums[0].shape
+    model = wg.shape[0]
+    width, tail = far_lo.shape[1] // 3, direct.shape[1] // 3
     share = model // 4
-    at = block_rows(tp, 2, share)
-    high_p, high_q = db_out[:, 3 * ff : 4 * ff], db_out[:, 4 * ff :]
-    write_rows(
-        (far_lo_out, far_hi_out),
-        *partial_rows(da_out, db_out, high_p, high_q, wg_ref[at, :], wu_ref[at, :]),
-    )
+    piece = jax.ShapeDtypeStruct((n_rows // 2, share + share // 2), BF)
+    vmem = pltpu.VMEM
+    return pl.pallas_call(
+        late_kernel,
+        in_specs=[pl.BlockSpec(memory_space=pltpu.SMEM)]
+        + [pl.BlockSpec(memory_space=pltpu.HBM)] * 8
+        + vmem_specs(1)
+        + [pl.BlockSpec(memory_space=pltpu.HBM)] * 3,
+        out_specs=vmem_specs(4),
+        out_shape=[
+            jax.ShapeDtypeStruct((n_rows, 3 * ff), BF), jax.ShapeDtypeStruct((n_rows, 5 * ff), BF), piece, piece,
+        ],
+        scratch_shapes=[vmem((n_rows, ff), F32)] * 12
+        + [vmem((n_rows, 3 * width), BF)]
+        + [vmem((tail, ff), BF), vmem((tail, ff), BF), vmem((ff, tail), BF)]
+        + [vmem((width, ff), BF), vmem((width, ff), BF), vmem((ff, width), BF)]
+        + [vmem((share, ff), BF), vmem((share, ff), BF), pltpu.SemaphoreType.DMA((16,))],
+        compiler_params=pltpu.CompilerParams(vmem_limit_bytes=SMALL_LIMIT),
+        name="late",
+    )(tp, *map(in_hbm, sums), far_lo, far_hi, direct, in_hbm(wg), in_hbm(wu), in_hbm(wd))
 
 
 def near_kernel(
@@ -294,27 +344,16 @@
     put(slice(4 * width, model), *sums(direct_ref, 0))
 
 
-def mixer_kernel(
-    where_ref, res_ref, wo_own, wo_prev, wo_next, wo_far, y_own, y_prev, y_next, y_far,
-    dy_own, dy_prev, dy_next, dy_far, mine_ref, other_ref,
-):
-    tp, core = where_ref[0], where_ref[1]
-    res = res_ref[...]
-    width = res.shape[1]
-    for w_ref, y_ref, dy_ref, by in (
-        (wo_own, y_own, dy_own, 0),
-        (wo_prev, y_prev, dy_prev, 3),
-        (wo_next, y_next, dy_next, 1),
-        (wo_far, y_far, dy_far, 2),
-    ):
-        dy_ref[...] = nn(res, w_ref[...]).astype(dy_ref.dtype)
-        grad = tn(res, y_ref[...]).astype(BF).reshape(width // 64, 2, 32, y_ref.shape[1])
-        low, high = grad[:, 0], grad[:, 1]
-        shape = (width // 2, y_ref.shape[1])
-        to = block_rows(tp, by, width // 2)
-        first = core == 0
-        mine_ref[to, :] = jnp.where(first, low, high).reshape(shape)
-        other_ref[to, :] = jnp.where(first, high, low).reshape(shape)
+def mixer_kernel(where_ref, res_ref, res_o_ref, y_ref, y_o_ref, out_ref):
+    tp, core = lax.rem(where_ref[0], 4), lax.div(where_ref[0], 4)
+    width = res_ref.shape[1]
+    chan = out_ref.shape[1]
+    for k, by in enumerate((0, 3, 1, 2)):
+        at = slice(k * chan, (k + 1) * chan)
+        grad = tn(res_ref[...], y_ref[:, at]) + tn(res_o_ref[...], y_o_ref[:, at])
+        grad = grad.reshape(width // 64, 2, 32, chan)
+        mine = jnp.where(core == 0, grad[:, 0], grad[:, 1]).reshape(width // 2, chan)
+        out_ref[block_rows(tp, by, width // 2), :] = mine.astype(BF)
 
 
 def from_behind(x, by):
@@ -337,7 +376,7 @@
     chan = w_out.shape[1]
     y_at = lax.axis_index("y").astype(jnp.int32)
     tp = y_at.reshape(1)
-    where = jnp.stack([y_at, lax.axis_index("c").astype(jnp.int32)])
+    where = (y_at + 4 * lax.axis_index("c").astype(jnp.int32)).reshape(1)
     wg, wu, wd = w_gate[0], w_up[0], w_down[0]
     ff = wg.shape[1]
 
@@ -359,28 +398,27 @@
         + taps_f[2] * padded[2 : tok_rows + 2]
     )
     y_short = (b_gate.astype(F32) * conv).astype(BF)
-    y_blocks = (y_short, shifted(y_short, "y", 1), shifted(y_short, "y", -1), shifted(y_short, "y", 2))
+    y_all = jnp.concatenate(
+        (y_short, shifted(y_short, "y", 1), shifted(y_short, "y", -1), shifted(y_short, "y", 2)), axis=1
+    )
     part = lambda by: lax.dynamic_slice_in_dim(w_out, lax.rem(y_at + by, 4) * share, share, 0)
     wo_blocks = (part(0), shifted(part(1), "y", 1), shifted(part(3), "y", -1), shifted(part(2), "y", 2))
-    own, sent_direct, conv, *held = lax.optimization_barrier(
-        (own, sent_direct, conv, *y_blocks, *wo_blocks)
-    )
-    y_blocks, wo_blocks = held[:4], held[4:]
+    own, sent_direct, conv, y_all, *wo_blocks = lax.optimization_barrier(
+        (own, sent_direct, conv, y_all, *wo_blocks)
+    )
+    y_other = shifted(y_all, "c", 1)
 
     prev, after, far_lo, far_hi = ring(own)
+    far_lo, far_hi = in_hbm(far_lo), in_hbm(far_hi)
     direct = to_experts(sent_direct)
 
     n_rows, half = own.shape[0], own.shape[0] // 2
     out_width = share + share // 2
     sums = local_call(early_kernel, tp, (own, prev, after, wg, wu, wd), [((n_rows, ff), F32)] * 6)
-    da, db, f_lo, f_hi = local_call(
-        late_kernel, tp, (*sums, far_lo, far_hi, direct, wg, wu, wd),
-        [((n_rows, 3 * ff), BF), ((n_rows, 5 * ff), BF), ((half, out_width), BF), ((half, out_width), BF)],
-        [pltpu.VMEM((n_rows, ff), F32)] * 6,
-    )
+    da, db, f_lo, f_hi = late(tp, sums, far_lo, far_hi, direct, wg, wu, wd)
     u_lo, u_hi, d_lo, d_hi, o = local_call(
-        near_kernel, tp, (da, db, wg, wu),
-        [((half, out_width), BF)] * 4 + [((n_rows, out_width), BF)],
+        near_kernel, tp, (da, db, in_hbm(wg), in_hbm(wu)),
+        [((half, out_width), BF)] * 4 + [((n_rows, out_width), BF)], SMALL_LIMIT,
     )
 
     from_prev = shifted(f_lo, "y", 1)
@@ -398,14 +436,14 @@
         weights_kernel, tp, (own, prev, after, far_lo, far_hi, direct, da, db),
         [((model_width, ff), BF), ((model_width, ff), BF), ((ff, model_width), BF)],
     )
-    back, gg, gu, gd = lax.optimization_barrier((back, gg, gu, gd))
-
-    residual_grad = combine(tp, rows, back, cotangent)
-    dy, dy_prev, dy_next, dy_far, mine, other = local_call(
-        mixer_kernel, where, (residual_grad, *wo_blocks, *y_blocks),
-        [((tok_rows, chan), F32)] + [((tok_rows, chan), BF)] * 3 + [((2 * share, chan), BF)] * 2,
-    )
-    chip = added(mine, shifted(other, "c", 1)).reshape(32, 32, chan)
+    back, gg, gu, gd, y_other = lax.optimization_barrier((back, gg, gu, gd, y_other))
+
+    residual_grad, dy, dy_prev, dy_next, dy_far = combine(tp, rows, back, cotangent, wo_blocks)
+    res_other = shifted(residual_grad, "c", 1)
+    (chip,) = local_call(
+        mixer_kernel, where, (in_hbm(residual_grad), res_other, in_hbm(y_all), in_hbm(y_other)),
+        [((2 * share, chan), BF)], SMALL_LIMIT,
+    )
     d_y = (
         dy
         + shifted(dy_prev, "y", -1).astype(F32)
@@ -424,7 +462,7 @@
     grad_c = (d_v * x_in.astype(F32)).astype(BF)
     grad_x = (d_v * c_gate.astype(F32)).astype(BF)
 
-    parts = lax.all_to_all(chip, ("z", "x"), split_axis=0, concat_axis=0, tiled=True)
+    parts = lax.all_to_all(chip.reshape(32, 32, chan), ("z", "x"), split_axis=0, concat_axis=0, tiled=True)
     piece = jnp.sum(parts.astype(F32), axis=0)
     at = lambda z, x, c, y: ((z * 4 + x) * 2 + c) * 4 + y
     pairs = [

time: 223 us -> 215 us (0.964)
  the two profiles are of different devices: /device:TPU:135 before, /device:TPU:16 now
where the time goes in v3:
time: 215 us; the launch traced here: 214 us
  waiting for transfers between devices  104 us (48%)
  starting transfers between devices  67.3 us (31%)
  Pallas kernels  33.1 us (15%)
  other arithmetic  6.12 us (3%)
  local copies, waits for them, and re-layouts  2.4 us (1%)
    ppermute x21, waiting for transfers between devices, shifted(): return lax.ppermute(x, axis, [(i, (i + by) % n) for i in range(n)])  69.6 us
    all_to_all x3, starting transfers between devices, per_device(): lax.all_to_all(v.reshape(64, MAIN, v.shape[1]), SP, split_axis=0, concat_...  29.4 us
    ppermute x21, starting transfers between devices, shifted(): return lax.ppermute(x, axis, [(i, (i + by) % n) for i in range(n)])  24.1 us
    all_to_all x3, waiting for transfers between devices, per_device(): lax.all_to_all(v.reshape(64, MAIN, v.shape[1]), SP, split_axis=0, concat_...  23.1 us
    pallas_call x4, Pallas kernels, local_call(): pl.pallas_call(kernel, in_specs=[pl.BlockSpec(memory_space=pltpu.SMEM)] +...  21.5 us
    ppermute x1, starting transfers between devices, per_device(): out_proj_grad = lax.ppermute(piece, ('z', 'x', 'c', 'y'), pairs)  5.78 us
    ppermute x1, waiting for transfers between devices, per_device(): out_proj_grad = lax.ppermute(piece, ('z', 'x', 'c', 'y'), pairs)  5.64 us
    all_to_all x1, starting transfers between devices, per_device(): lax.all_to_all(chip.reshape(32, 32, chan), ('z', 'x'), split_axis=0, conc...  5.05 us
  transfers between devices with their start and end apart: 28, of which 19 were waited for; matrix products, arithmetic and copies ran while one was open for 2% of the time, Pallas kernels for 11%

profile of v3, /device:TPU:16, one launch (start us, length us, event | category | flops | bytes accessed | tf_op | source)
XLA Modules:
  0.0 214.2 jit_solution(14515095707846721797)
XLA Ops:
  3.1 4.1 %route.1 = (bf16[512,1152]{1,0:T(8,128)(2,1)}, bf16[512,1536]{1,0:T(8,128)(2,1)}, s32[4,256]{1,0:T(4,128)}) custom-call(s32[1]{0:T(128)} %bitcast.tp_ref, s32[2,256]{1,0:T(2,128)} %bitcast.44, f32[2,256]{1,0:T(2,128)} %bitcast.45, bf16[256,2048]{1,0:T(8,128)(2,1)} %hd_ref.1, bf16[256,2048]{1,0:T(8,128)(2,1)} %c_ref.3, bf16[256,2048]{1,0:T(8,128)(2,1)} %hd_ref.1, ...), custom_call_target="tpu_custom_call" | custom-call | tf_op jit(solution)/shard_map/route/pallas_call | solution.py:91
  7.2 13.2 %all-to-all-start = ((bf16[64,8,1152]{2,1,0:T(8,128)(2,1)}), bf16[64,8,1152]{2,1,0:T(8,128)(2,1)S(1)}, u32[]{:S(2)}, u32[]{:S(2)}) async-start(bf16[64,8,1152]{2,1,0:T(8,128)(2,1)} %bitcast.37), calls=%async_computation | async-start | bytes 2359296 | tf_op jit(solution)/shard_map/all_to_all | solution.py:384
  24.9 4.0 %collective-permute-start.6 = (bf16[512,256]{1,0:T(8,128)(2,1)S(1)}, bf16[512,256]{1,0:T(8,128)(2,1)S(1)}, u32[]{:S(2)}, u32[]{:S(2)}) collective-permute-start(bf16[512,256]{1,0:T(8,128)(2,1)S(1)} %get-tuple-element.94), channel_id=1, source_target_pairs={{0,2},{1,3},{2,0},{3,1},{4,6},{5,7},{6,4},{7,5},{8,10},{9,11},{10,... | collective-permute-start | bytes 786440 | tf_op jit(solution)/shard_map/ppermute | solution.py:34
  30.9 10.4 %collective-permute-done.2 = bf16[256,256]{1,0:T(8,128)(2,1)S(1)} collective-permute-done((bf16[256,256]{1,0:T(8,128)(2,1)S(1)}, bf16[256,256]{1,0:T(8,128)(2,1)S(1)}, u32[]{:S(2)}, u32[]{:S(2)}) %collective-permute-start.2) | collective-permute-done | bytes 131104 | tf_op jit(solution)/shard_map/ppermute | solution.py:34
  43.3 8.8 %all-to-all-done = bf16[64,8,1152]{2,1,0:T(8,128)(2,1)S(1)} async-done(((bf16[64,8,1152]{2,1,0:T(8,128)(2,1)}), bf16[64,8,1152]{2,1,0:T(8,128)(2,1)S(1)}, u32[]{:S(2)}, u32[]{:S(2)}) %all-to-all-start) | async-done | bytes 1179680 | tf_op jit(solution)/shard_map/all_to_all | solution.py:384
  52.1 5.6 %all-to-all-start.1 = ((bf16[64,8,1536]{2,1,0:T(8,128)(2,1)}), bf16[64,8,1536]{2,1,0:T(8,128)(2,1)S(1)}, u32[]{:S(2)}, u32[]{:S(2)}) async-start(bf16[64,8,1536]{2,1,0:T(8,128)(2,1)} %bitcast.36), calls=%async_computation.1 | async-start | bytes 3145728 | tf_op jit(solution)/shard_map/all_to_all | solution.py:384
  59.8 25.9 %collective-permute-done.7.prev_ref = bf16[512,1152]{1,0:T(8,128)(2,1)S(1)} collective-permute-done((bf16[512,1152]{1,0:T(8,128)(2,1)S(1)}, bf16[512,1152]{1,0:T(8,128)(2,1)S(1)}, u32[]{:S(2)}, u32[]{:S(2)}) %collective-permute-start.7) | collective-permute-done | bytes 1179680 | tf_op jit(solution)/shard_map/ppermute | solution.py:34
  88.1 6.6 %shard_map.179 = (f32[512,256]{1,0:T(8,128)}, f32[512,256]{1,0:T(8,128)}, f32[512,256]{1,0:T(8,128)}, f32[512,256]{1,0:T(8,128)}, f32[512,256]{1,0:T(8,128)}, /*index=5*/f32[512,256]{1,0:T(8,128)}) custom-call(s32[1]{0:T(128)} %bitcast.tp_ref, bf16[512,1152]{1,0:T(8,128)(2,1)} %bitcast.26, bf16[512,1152]{1,0:T(8,128)(2,1)} %copy-done.5, ...), custom_call_target="tpu_custom_call" | custom-call | tf_op jit(solution)/shard_map/pallas_call | solution.py:168
  94.8 5.5 %collective-permute-done.9.far_lo_in.far_lo_ref = bf16[256,1152]{1,0:T(8,128)(2,1)S(1)} collective-permute-done((bf16[256,1152]{1,0:T(8,128)(2,1)S(1)}, bf16[256,1152]{1,0:T(8,128)(2,1)S(1)}, u32[]{:S(2)}, u32[]{:S(2)}) %collective-permute-start.9) | collective-permute-done | bytes 589856 | tf_op jit(solution)/shard_map/ppermute | solution.py:34
  102.4 4.7 %late.1 = (bf16[512,768]{1,0:T(8,128)(2,1)S(1)}, bf16[512,1280]{1,0:T(8,128)(2,1)S(1)}, bf16[256,768]{1,0:T(8,128)(2,1)S(1)}, bf16[256,768]{1,0:T(8,128)(2,1)S(1)}) custom-call(s32[1]{0:T(128)} %bitcast.tp_ref, f32[512,256]{1,0:T(8,128)} %get-tuple-element.54.ga_in, f32[512,256]{1,0:T(8,128)} %get-tuple-element.55.ua_in, ...), custom_call_target="tpu_custom_call" | custom-call | tf_op jit(solution)/shard_map/late/pallas_call | solution.py:285
  107.1 2.8 %collective-permute-start.11 = (bf16[256,768]{1,0:T(8,128)(2,1)S(1)}, bf16[256,768]{1,0:T(8,128)(2,1)S(1)}, u32[]{:S(2)}, u32[]{:S(2)}) collective-permute-start(bf16[256,768]{1,0:T(8,128)(2,1)S(1)} %get-tuple-element.65), channel_id=1, source_target_pairs={{0,1},{1,2},{2,3},{3,0},{4,5},{5,6},{6,7},{7,4},{8,9},{9,10},{10,1... | collective-permute-start | bytes 1179656 | tf_op jit(solution)/shard_map/ppermute | solution.py:34
  110.0 3.4 %shard_map.180 = (bf16[256,768]{1,0:T(8,128)(2,1)S(1)}, bf16[256,768]{1,0:T(8,128)(2,1)S(1)}, bf16[256,768]{1,0:T(8,128)(2,1)S(1)}, bf16[256,768]{1,0:T(8,128)(2,1)S(1)}, bf16[512,768]{1,0:T(8,128)(2,1)S(1)}) custom-call(s32[1]{0:T(128)} %bitcast.tp_ref, bf16[512,768]{1,0:T(8,128)(2,1)S(1)} %get-tuple-element.61.da.da_ref, ...), custom_call_target="tpu_custom_call" | custom-call | tf_op jit(solution)/shard_map/pallas_call | solution.py:168
  115.5 4.0 %collective-permute-done.11 = bf16[256,768]{1,0:T(8,128)(2,1)S(1)} collective-permute-done((bf16[256,768]{1,0:T(8,128)(2,1)S(1)}, bf16[256,768]{1,0:T(8,128)(2,1)S(1)}, u32[]{:S(2)}, u32[]{:S(2)}) %collective-permute-start.11) | collective-permute-done | bytes 393248 | tf_op jit(solution)/shard_map/ppermute | solution.py:34
  122.3 5.6 %collective-permute-done.13 = bf16[256,768]{1,0:T(8,128)(2,1)S(1)} collective-permute-done((bf16[256,768]{1,0:T(8,128)(2,1)S(1)}, bf16[256,768]{1,0:T(8,128)(2,1)S(1)}, u32[]{:S(2)}, u32[]{:S(2)}) %collective-permute-start.13) | collective-permute-done | bytes 393248 | tf_op jit(solution)/shard_map/ppermute | solution.py:34
  130.4 3.1 %collective-permute-done.12 = bf16[256,768]{1,0:T(8,128)(2,1)S(1)} collective-permute-done((bf16[256,768]{1,0:T(8,128)(2,1)S(1)}, bf16[256,768]{1,0:T(8,128)(2,1)S(1)}, u32[]{:S(2)}, u32[]{:S(2)}) %collective-permute-start.12) | collective-permute-done | bytes 393248 | tf_op jit(solution)/shard_map/ppermute | solution.py:34
  136.9 10.6 %all-to-all-start.2 = ((bf16[64,8,768]{2,1,0:T(8,128)(2,1)}), bf16[64,8,768]{2,1,0:T(8,128)(2,1)S(1)}, u32[]{:S(2)}, u32[]{:S(2)}) async-start(bf16[64,8,768]{2,1,0:T(8,128)(2,1)} %fusion), calls=%async_computation.2 | async-start | bytes 1572864 | tf_op jit(solution)/shard_map/all_to_all | solution.py:384
  147.9 8.5 %shard_map.181 = (bf16[2048,256]{1,0:T(8,128)(2,1)}, bf16[2048,256]{1,0:T(8,128)(2,1)}, bf16[256,2048]{1,0:T(8,128)(2,1)}) custom-call(s32[1]{0:T(128)} %bitcast.tp_ref, bf16[512,1152]{1,0:T(8,128)(2,1)} %bitcast.27, bf16[512,1152]{1,0:T(8,128)(2,1)} %copy-done.5, bf16[512,1152]{1,0:T(8,128)(2,1)} %copy-done.6, bf16[256,1152]{1,0:T(8,128)(2,1)} %copy-done.7, ...), custom_call_target="tpu_custom_call" | custom-call | tf_op jit(solution)/shard_map/pallas_call | solution.py:168
  156.5 14.3 %all-to-all-done.2 = bf16[64,8,768]{2,1,0:T(8,128)(2,1)S(1)} async-done(((bf16[64,8,768]{2,1,0:T(8,128)(2,1)}), bf16[64,8,768]{2,1,0:T(8,128)(2,1)S(1)}, u32[]{:S(2)}, u32[]{:S(2)}) %all-to-all-start.2) | async-done | bytes 786464 | tf_op jit(solution)/shard_map/all_to_all | solution.py:384
  175.3 2.9 %shard_map.182 = bf16[1024,256]{1,0:T(8,128)(2,1)} custom-call(s32[1]{0:T(128)} %bitcast.18.where_ref, bf16[256,512]{1,0:T(8,128)(2,1)} %get-tuple-element.115.res_ref, bf16[256,512]{1,0:T(8,128)(2,1)S(1)} %collective-permute-done.18.res_o_ref, bf16[256,1024]{1,0:T(8,128)(2,1)} %pad_maximum_fusion.y_ref, bf16[256,1024]{1,0:T(8,128)(2,1)} %copy-done.15), custom_call_target="tpu_custom_call" | custom-call | tf_op jit(solution)/shard_map/pallas_call | solution.py:168
  178.3 5.1 %all-to-all-start.3 = ((bf16[32,32,256]{2,1,0:T(8,128)(2,1)}), bf16[32,32,256]{2,1,0:T(8,128)(2,1)S(1)}, u32[]{:S(2)}, u32[]{:S(2)}) async-start(bf16[32,32,256]{2,1,0:T(8,128)(2,1)} %bitcast.19), calls=%async_computation.3 | async-start | bytes 1048576 | tf_op jit(solution)/shard_map/all_to_all | solution.py:465
  186.5 4.7 %collective-permute-done.22 = bf16[256,256]{1,0:T(8,128)(2,1)S(1)} collective-permute-done((bf16[256,256]{1,0:T(8,128)(2,1)S(1)}, bf16[256,256]{1,0:T(8,128)(2,1)S(1)}, u32[]{:S(2)}, u32[]{:S(2)}) %collective-permute-start.22) | collective-permute-done | bytes 131104 | tf_op jit(solution)/shard_map/ppermute | solution.py:34
  197.2 4.3 %all-to-all-done.3 = bf16[32,32,256]{2,1,0:T(8,128)(2,1)S(1)} async-done(((bf16[32,32,256]{2,1,0:T(8,128)(2,1)}), bf16[32,32,256]{2,1,0:T(8,128)(2,1)S(1)}, u32[]{:S(2)}, u32[]{:S(2)}) %all-to-all-start.3) | async-done | bytes 524320 | tf_op jit(solution)/shard_map/all_to_all | solution.py:465
  201.5 5.8 %collective-permute-start.19 = (f32[32,256]{1,0:T(8,128)S(1)}, f32[32,256]{1,0:T(8,128)S(1)}, u32[]{:S(2)}, u32[]{:S(2)}) collective-permute-start(f32[32,256]{1,0:T(8,128)S(1)} %convert_reduce_fusion), channel_id=1, source_target_pairs={{0,0},{1,64},{2,128},{3,192},{4,4},{5,68},{6,132},{7,196},{8,8},{9... | collective-permute-start | bytes 98312 | tf_op jit(solution)/shard_map/ppermute | solution.py:472
  208.0 5.6 %collective-permute-done.19 = f32[32,256]{1,0:T(8,128)S(1)} collective-permute-done((f32[32,256]{1,0:T(8,128)S(1)}, f32[32,256]{1,0:T(8,128)S(1)}, u32[]{:S(2)}, u32[]{:S(2)}) %collective-permute-start.19) | collective-permute-done | bytes 32800 | tf_op jit(solution)/shard_map/ppermute | solution.py:472
  (100 shorter events, 43.7 us)
Async XLA Ops:
  7.2 44.8 %all-to-all-start = ((bf16[64,8,1152]{2,1,0:T(8,128)(2,1)}), bf16[64,8,1152]{2,1,0:T(8,128)(2,1)S(1)}, u32[]{:S(2)}, u32[]{:S(2)}) async-start(bf16[64,8,1152]{2,1,0:T(8,128)(2,1)} %bitcast.37), calls=%async_computation | async-start | bytes 2359296 | tf_op jit(solution)/shard_map/all_to_all | solution.py:384
  21.4 7.9 %collective-permute-start.3 = (bf16[256,256]{1,0:T(8,128)(2,1)S(1)}, bf16[256,256]{1,0:T(8,128)(2,1)S(1)}, u32[]{:S(2)}, u32[]{:S(2)}) collective-permute-start(bf16[256,256]{1,0:T(8,128)(2,1)S(1)} %get-tuple-element.92), channel_id=1, source_target_pairs={{0,2},{1,3},{2,0},{3,1},{4,6},{5,7},{6,4},{7,5},{8,10},{9,11},{10,... | collective-permute-start | bytes 393224 | tf_op jit(solution)/shard_map/ppermute | solution.py:34
  22.5 20.7 %collective-permute-start.4 = (bf16[512,256]{1,0:T(8,128)(2,1)S(1)}, bf16[512,256]{1,0:T(8,128)(2,1)S(1)}, u32[]{:S(2)}, u32[]{:S(2)}) collective-permute-start(bf16[512,256]{1,0:T(8,128)(2,1)S(1)} %get-tuple-element.95), channel_id=1, source_target_pairs={{0,1},{1,2},{2,3},{3,0},{4,5},{5,6},{6,7},{7,4},{8,9},{9,10},{10,1... | collective-permute-start | bytes 786440 | tf_op jit(solution)/shard_map/ppermute | solution.py:34
  24.7 18.6 %collective-permute-start.5 = (bf16[512,256]{1,0:T(8,128)(2,1)S(1)}, bf16[512,256]{1,0:T(8,128)(2,1)S(1)}, u32[]{:S(2)}, u32[]{:S(2)}) collective-permute-start(bf16[512,256]{1,0:T(8,128)(2,1)S(1)} %get-tuple-element.97), channel_id=1, source_target_pairs={{0,3},{1,0},{2,1},{3,2},{4,7},{5,4},{6,5},{7,6},{8,11},{9,8},{10,9... | collective-permute-start | bytes 786440 | tf_op jit(solution)/shard_map/ppermute | solution.py:34
  24.9 18.4 %collective-permute-start.6 = (bf16[512,256]{1,0:T(8,128)(2,1)S(1)}, bf16[512,256]{1,0:T(8,128)(2,1)S(1)}, u32[]{:S(2)}, u32[]{:S(2)}) collective-permute-start(bf16[512,256]{1,0:T(8,128)(2,1)S(1)} %get-tuple-element.94), channel_id=1, source_target_pairs={{0,2},{1,3},{2,0},{3,1},{4,6},{5,7},{6,4},{7,5},{8,10},{9,11},{10,... | collective-permute-start | bytes 786440 | tf_op jit(solution)/shard_map/ppermute | solution.py:34
  28.9 12.5 %collective-permute-start.2 = (bf16[256,256]{1,0:T(8,128)(2,1)S(1)}, bf16[256,256]{1,0:T(8,128)(2,1)S(1)}, u32[]{:S(2)}, u32[]{:S(2)}) collective-permute-start(bf16[256,256]{1,0:T(8,128)(2,1)S(1)} %get-tuple-element.92), channel_id=1, source_target_pairs={{0,3},{1,0},{2,1},{3,2},{4,7},{5,4},{6,5},{7,6},{8,11},{9,8},{10,9... | collective-permute-start | bytes 393224 | tf_op jit(solution)/shard_map/ppermute | solution.py:34
  29.3 13.1 %collective-permute-start.1 = (bf16[256,256]{1,0:T(8,128)(2,1)S(1)}, bf16[256,256]{1,0:T(8,128)(2,1)S(1)}, u32[]{:S(2)}, u32[]{:S(2)}) collective-permute-start(bf16[256,256]{1,0:T(8,128)(2,1)S(1)} %get-tuple-element.92), channel_id=1, source_target_pairs={{0,1},{1,2},{2,3},{3,0},{4,5},{5,6},{6,7},{7,4},{8,9},{9,10},{10,1... | collective-permute-start | bytes 393224 | tf_op jit(solution)/shard_map/ppermute | solution.py:34
  52.1 49.5 %all-to-all-start.1 = ((bf16[64,8,1536]{2,1,0:T(8,128)(2,1)}), bf16[64,8,1536]{2,1,0:T(8,128)(2,1)S(1)}, u32[]{:S(2)}, u32[]{:S(2)}) async-start(bf16[64,8,1536]{2,1,0:T(8,128)(2,1)} %bitcast.36), calls=%async_computation.1 | async-start | bytes 3145728 | tf_op jit(solution)/shard_map/all_to_all | solution.py:384
  57.7 28.0 %collective-permute-start.7 = (bf16[512,1152]{1,0:T(8,128)(2,1)S(1)}, bf16[512,1152]{1,0:T(8,128)(2,1)S(1)}, u32[]{:S(2)}, u32[]{:S(2)}) collective-permute-start(bf16[512,1152]{1,0:T(8,128)(2,1)S(1)} %bitcast.24), channel_id=1, source_target_pairs={{0,1},{1,2},{2,3},{3,0},{4,5},{5,6},{6,7},{7,4},{8,9},{9,10},{10,1... | collective-permute-start | bytes 3538952 | tf_op jit(solution)/shard_map/ppermute | solution.py:34
  59.0 28.1 %collective-permute-start.8 = (bf16[512,1152]{1,0:T(8,128)(2,1)S(1)}, bf16[512,1152]{1,0:T(8,128)(2,1)S(1)}, u32[]{:S(2)}, u32[]{:S(2)}) collective-permute-start(bf16[512,1152]{1,0:T(8,128)(2,1)S(1)} %bitcast.25), channel_id=1, source_target_pairs={{0,3},{1,0},{2,1},{3,2},{4,7},{5,4},{6,5},{7,6},{8,11},{9,8},{10,9... | collective-permute-start | bytes 3538952 | tf_op jit(solution)/shard_map/ppermute | solution.py:34
  85.7 14.5 %collective-permute-start.9 = (bf16[256,1152]{1,0:T(8,128)(2,1)S(1)}, bf16[256,1152]{1,0:T(8,128)(2,1)S(1)}, u32[]{:S(2)}, u32[]{:S(2)}) collective-permute-start(bf16[256,1152]{1,0:T(8,128)(2,1)S(1)} %slice.56), channel_id=1, source_target_pairs={{0,1},{1,2},{2,3},{3,0},{4,5},{5,6},{6,7},{7,4},{8,9},{9,10},{10,1... | collective-permute-start | bytes 1769480 | tf_op jit(solution)/shard_map/ppermute | solution.py:34
  87.1 14.4 %collective-permute-start.10 = (bf16[256,1152]{1,0:T(8,128)(2,1)S(1)}, bf16[256,1152]{1,0:T(8,128)(2,1)S(1)}, u32[]{:S(2)}, u32[]{:S(2)}) collective-permute-start(bf16[256,1152]{1,0:T(8,128)(2,1)S(1)} %slice.57), channel_id=1, source_target_pairs={{0,3},{1,0},{2,1},{3,2},{4,7},{5,4},{6,5},{7,6},{8,11},{9,8},{10,9... | collective-permute-start | bytes 1769480 | tf_op jit(solution)/shard_map/ppermute | solution.py:34
  107.1 12.3 %collective-permute-start.11 = (bf16[256,768]{1,0:T(8,128)(2,1)S(1)}, bf16[256,768]{1,0:T(8,128)(2,1)S(1)}, u32[]{:S(2)}, u32[]{:S(2)}) collective-permute-start(bf16[256,768]{1,0:T(8,128)(2,1)S(1)} %get-tuple-element.65), channel_id=1, source_target_pairs={{0,1},{1,2},{2,3},{3,0},{4,5},{5,6},{6,7},{7,4},{8,9},{9,10},{10,1... | collective-permute-start | bytes 1179656 | tf_op jit(solution)/shard_map/ppermute | solution.py:34
  110.0 12.2 %collective-permute-start.15 = (bf16[256,768]{1,0:T(8,128)(2,1)S(1)}, bf16[256,768]{1,0:T(8,128)(2,1)S(1)}, u32[]{:S(2)}, u32[]{:S(2)}) collective-permute-start(bf16[256,768]{1,0:T(8,128)(2,1)S(1)} %get-tuple-element.69), channel_id=1, source_target_pairs={{0,3},{1,0},{2,1},{3,2},{4,7},{5,4},{6,5},{7,6},{8,11},{9,8},{10,9... | collective-permute-start | bytes 1179656 | tf_op jit(solution)/shard_map/ppermute | solution.py:34
  113.4 14.5 %collective-permute-start.13 = (bf16[256,768]{1,0:T(8,128)(2,1)S(1)}, bf16[256,768]{1,0:T(8,128)(2,1)S(1)}, u32[]{:S(2)}, u32[]{:S(2)}) collective-permute-start(bf16[256,768]{1,0:T(8,128)(2,1)S(1)} %get-tuple-element.66), channel_id=1, source_target_pairs={{0,1},{1,2},{2,3},{3,0},{4,5},{5,6},{6,7},{7,4},{8,9},{9,10},{10,1... | collective-permute-start | bytes 1179656 | tf_op jit(solution)/shard_map/ppermute | solution.py:34
  115.5 14.9 %collective-permute-start.14 = (bf16[256,768]{1,0:T(8,128)(2,1)S(1)}, bf16[256,768]{1,0:T(8,128)(2,1)S(1)}, u32[]{:S(2)}, u32[]{:S(2)}) collective-permute-start(bf16[256,768]{1,0:T(8,128)(2,1)S(1)} %get-tuple-element.67), channel_id=1, source_target_pairs={{0,3},{1,0},{2,1},{3,2},{4,7},{5,4},{6,5},{7,6},{8,11},{9,8},{10,9... | collective-permute-start | bytes 1179656 | tf_op jit(solution)/shard_map/ppermute | solution.py:34
  119.6 13.9 %collective-permute-start.12 = (bf16[256,768]{1,0:T(8,128)(2,1)S(1)}, bf16[256,768]{1,0:T(8,128)(2,1)S(1)}, u32[]{:S(2)}, u32[]{:S(2)}) collective-permute-start(bf16[256,768]{1,0:T(8,128)(2,1)S(1)} %add_convert_fusion.2), channel_id=1, source_target_pairs={{0,1},{1,2},{2,3},{3,0},{4,5},{5,6},{6,7},{7,4},{8,9},{9,10},{10,1... | collective-permute-start | bytes 1179656 | tf_op jit(solution)/shard_map/ppermute | solution.py:34
  122.2 13.5 %collective-permute-start.16 = (bf16[256,768]{1,0:T(8,128)(2,1)S(1)}, bf16[256,768]{1,0:T(8,128)(2,1)S(1)}, u32[]{:S(2)}, u32[]{:S(2)}) collective-permute-start(bf16[256,768]{1,0:T(8,128)(2,1)S(1)} %add_convert_fusion.1), channel_id=1, source_target_pairs={{0,3},{1,0},{2,1},{3,2},{4,7},{5,4},{6,5},{7,6},{8,11},{9,8},{10,9... | collective-permute-start | bytes 1179656 | tf_op jit(solution)/shard_map/ppermute | solution.py:34
  136.9 33.9 %all-to-all-start.2 = ((bf16[64,8,768]{2,1,0:T(8,128)(2,1)}), bf16[64,8,768]{2,1,0:T(8,128)(2,1)S(1)}, u32[]{:S(2)}, u32[]{:S(2)}) async-start(bf16[64,8,768]{2,1,0:T(8,128)(2,1)} %fusion), calls=%async_computation.2 | async-start | bytes 1572864 | tf_op jit(solution)/shard_map/all_to_all | solution.py:384
  147.6 8.9 %collective-permute-start.17 = (bf16[256,1024]{1,0:T(8,128)(2,1)S(1)}, bf16[256,1024]{1,0:T(8,128)(2,1)S(1)}, u32[]{:S(2)}, u32[]{:S(2)}) collective-permute-start(bf16[256,1024]{1,0:T(8,128)(2,1)S(1)} %copy-done.9), channel_id=1, source_target_pairs={{0,4},{4,0},{1,5},{5,1},{2,6},{6,2},{3,7},{7,3},{8,12},{12,8},{9,1... | collective-permute-start | bytes 1572872 | tf_op jit(solution)/shard_map/ppermute | solution.py:34
  178.3 23.2 %all-to-all-start.3 = ((bf16[32,32,256]{2,1,0:T(8,128)(2,1)}), bf16[32,32,256]{2,1,0:T(8,128)(2,1)S(1)}, u32[]{:S(2)}, u32[]{:S(2)}) async-start(bf16[32,32,256]{2,1,0:T(8,128)(2,1)} %bitcast.19), calls=%async_computation.3 | async-start | bytes 1048576 | tf_op jit(solution)/shard_map/all_to_all | solution.py:465
  183.3 8.0 %collective-permute-start.22 = (bf16[256,256]{1,0:T(8,128)(2,1)S(1)}, bf16[256,256]{1,0:T(8,128)(2,1)S(1)}, u32[]{:S(2)}, u32[]{:S(2)}) collective-permute-start(bf16[256,256]{1,0:T(8,128)(2,1)S(1)} %get-tuple-element.88), channel_id=1, source_target_pairs={{0,2},{1,3},{2,0},{3,1},{4,6},{5,7},{6,4},{7,5},{8,10},{9,11},{10,... | collective-permute-start | bytes 393224 | tf_op jit(solution)/shard_map/ppermute | solution.py:34
  184.2 8.4 %collective-permute-start.21 = (bf16[256,256]{1,0:T(8,128)(2,1)S(1)}, bf16[256,256]{1,0:T(8,128)(2,1)S(1)}, u32[]{:S(2)}, u32[]{:S(2)}) collective-permute-start(bf16[256,256]{1,0:T(8,128)(2,1)S(1)} %get-tuple-element.87), channel_id=1, source_target_pairs={{0,1},{1,2},{2,3},{3,0},{4,5},{5,6},{6,7},{7,4},{8,9},{9,10},{10,1... | collective-permute-start | bytes 393224 | tf_op jit(solution)/shard_map/ppermute | solution.py:34
  201.5 12.1 %collective-permute-start.19 = (f32[32,256]{1,0:T(8,128)S(1)}, f32[32,256]{1,0:T(8,128)S(1)}, u32[]{:S(2)}, u32[]{:S(2)}) collective-permute-start(f32[32,256]{1,0:T(8,128)S(1)} %convert_reduce_fusion), channel_id=1, source_target_pairs={{0,0},{1,64},{2,128},{3,192},{4,4},{5,68},{6,132},{7,196},{8,8},{9... | collective-permute-start | bytes 98312 | tf_op jit(solution)/shard_map/ppermute | solution.py:472
  (26 other events, 254.3 us)

commit v4 on v3

--- a/solution.py
+++ b/solution.py
@@ -106,10 +106,7 @@
     )(tp, ids, weights, hidden_in, cotangent, hidden_in, cotangent)
 
 
-def combine_kernel(
-    tp_ref, rows_ref, back_ref, c_ref, wo_own, wo_prev, wo_next, wo_far,
-    out_ref, dy_own, dy_prev, dy_next, dy_far,
-):
+def combine_kernel(tp_ref, rows_ref, back_ref, c_ref, out_ref):
     width = c_ref.shape[1]
     a0, a1, b0, b1 = (rows_ref[k : k + 1, :] for k in range(4))
 
@@ -123,14 +120,10 @@
     half = width // 2
     out_ref[:, 0:half] = (c_ref[:, 0:half].astype(F32) + (main[:, 0:half] + low)).astype(BF)
     out_ref[:, half:] = (c_ref[:, half:].astype(F32) + (main[:, half:] + high)).astype(BF)
-    res = out_ref[...]
-    for w_ref, dy in ((wo_own, dy_own), (wo_prev, dy_prev), (wo_next, dy_next), (wo_far, dy_far)):
-        dy[...] = nn(res, w_ref[...]).astype(dy.dtype)
-
-
-def combine(tp, rows, back, cotangent, wo_blocks):
+
+
+def combine(tp, rows, back, cotangent):
     tokens, width = cotangent.shape[0], cotangent.shape[1] // 4
-    chan = wo_blocks[0].shape[1]
     whole = lambda shape: pl.BlockSpec(shape, lambda i, t: (0, 0))
     return pl.pallas_call(
         combine_kernel,
@@ -141,15 +134,18 @@
                 whole(rows.shape),
                 whole(back.shape),
                 pl.BlockSpec((tokens, width), lambda i, t: (0, t[0])),
-            ]
-            + [whole((width, chan))] * 4,
-            out_specs=[whole((tokens, width))] + [whole((tokens, chan))] * 4,
+            ],
+            out_specs=whole((tokens, width)),
         ),
-        out_shape=[jax.ShapeDtypeStruct((tokens, width), BF), jax.ShapeDtypeStruct((tokens, chan), F32)]
-        + [jax.ShapeDtypeStruct((tokens, chan), BF)] * 3,
+        out_shape=jax.ShapeDtypeStruct((tokens, width), BF),
         compiler_params=pltpu.CompilerParams(vmem_limit_bytes=SMALL_LIMIT),
         name="combine",
-    )(tp, rows, back, in_hbm(cotangent), *map(in_hbm, wo_blocks))
+    )(tp, rows, back, in_hbm(cotangent))
+
+
+def d_y_kernel(tp_ref, res_ref, wo_own, wo_prev, wo_next, wo_far, dy_own, dy_prev, dy_next, dy_far):
+    for w_ref, dy in ((wo_own, dy_own), (wo_prev, dy_prev), (wo_next, dy_next), (wo_far, dy_far)):
+        dy[...] = nn(res_ref[...], w_ref[...]).astype(dy.dtype)
 
 
 def block_at(tp, by):
@@ -353,7 +349,7 @@
         grad = tn(res_ref[...], y_ref[:, at]) + tn(res_o_ref[...], y_o_ref[:, at])
         grad = grad.reshape(width // 64, 2, 32, chan)
         mine = jnp.where(core == 0, grad[:, 0], grad[:, 1]).reshape(width // 2, chan)
-        out_ref[block_rows(tp, by, width // 2), :] = mine.astype(BF)
+        out_ref[block_rows(tp, by + 2, width // 2), :] = mine.astype(BF)
 
 
 def from_behind(x, by):
@@ -386,27 +382,11 @@
     ).reshape(v.shape)
     tail = slice(tok_rows - 2, tok_rows)
     earlier = from_behind(c_gate[tail].astype(F32) * x_in[tail].astype(F32), 1)
-    sent, earlier = lax.optimization_barrier((sent, earlier))
     own = to_experts(sent)
 
-    taps_f = taps.astype(F32)
-    gated = c_gate.astype(F32) * x_in.astype(F32)
-    padded = jnp.concatenate([earlier, gated], axis=0)
-    conv = (
-        taps_f[0] * padded[0:tok_rows]
-        + taps_f[1] * padded[1 : tok_rows + 1]
-        + taps_f[2] * padded[2 : tok_rows + 2]
-    )
-    y_short = (b_gate.astype(F32) * conv).astype(BF)
-    y_all = jnp.concatenate(
-        (y_short, shifted(y_short, "y", 1), shifted(y_short, "y", -1), shifted(y_short, "y", 2)), axis=1
-    )
     part = lambda by: lax.dynamic_slice_in_dim(w_out, lax.rem(y_at + by, 4) * share, share, 0)
     wo_blocks = (part(0), shifted(part(1), "y", 1), shifted(part(3), "y", -1), shifted(part(2), "y", 2))
-    own, sent_direct, conv, y_all, *wo_blocks = lax.optimization_barrier(
-        (own, sent_direct, conv, y_all, *wo_blocks)
-    )
-    y_other = shifted(y_all, "c", 1)
+    own, sent_direct, *wo_blocks = lax.optimization_barrier((own, sent_direct, *wo_blocks))
 
     prev, after, far_lo, far_hi = ring(own)
     far_lo, far_hi = in_hbm(far_lo), in_hbm(far_hi)
@@ -431,15 +411,34 @@
     got_prev = jnp.concatenate([prev_lo, prev_hi], axis=0).astype(F32)
     got_next = jnp.concatenate([next_lo, next_hi], axis=0).astype(F32)
     total = (o.astype(F32) + got_prev + got_next).astype(BF)
+    total, earlier = lax.optimization_barrier((total, earlier))
     back = to_experts(total)
+
+    taps_f = taps.astype(F32)
+    gated = c_gate.astype(F32) * x_in.astype(F32)
+    padded = jnp.concatenate([earlier, gated], axis=0)
+    conv = (
+        taps_f[0] * padded[0:tok_rows]
+        + taps_f[1] * padded[1 : tok_rows + 1]
+        + taps_f[2] * padded[2 : tok_rows + 2]
+    )
+    y_short = (b_gate.astype(F32) * conv).astype(BF)
+    y_all = jnp.concatenate(
+        (y_short, shifted(y_short, "y", 1), shifted(y_short, "y", -1), shifted(y_short, "y", 2)), axis=1
+    )
+    y_other = shifted(y_all, "c", 1)
     gg, gu, gd = local_call(
         weights_kernel, tp, (own, prev, after, far_lo, far_hi, direct, da, db),
         [((model_width, ff), BF), ((model_width, ff), BF), ((ff, model_width), BF)],
     )
     back, gg, gu, gd, y_other = lax.optimization_barrier((back, gg, gu, gd, y_other))
 
-    residual_grad, dy, dy_prev, dy_next, dy_far = combine(tp, rows, back, cotangent, wo_blocks)
+    residual_grad = combine(tp, rows, back, cotangent)
     res_other = shifted(residual_grad, "c", 1)
+    dy, dy_prev, dy_next, dy_far = local_call(
+        d_y_kernel, tp, (in_hbm(residual_grad), *map(in_hbm, wo_blocks)),
+        [((tok_rows, chan), F32)] + [((tok_rows, chan), BF)] * 3, SMALL_LIMIT,
+    )
     (chip,) = local_call(
         mixer_kernel, where, (in_hbm(residual_grad), res_other, in_hbm(y_all), in_hbm(y_other)),
         [((2 * share, chan), BF)], SMALL_LIMIT,
@@ -466,7 +465,7 @@
     piece = jnp.sum(parts.astype(F32), axis=0)
     at = lambda z, x, c, y: ((z * 4 + x) * 2 + c) * 4 + y
     pairs = [
-        (at(z, x, c, y), at(2 * y + z % 2, x, c, z // 2))
+        (at(z, x, c, y), at(2 * y + z % 2, x, c, (z // 2 + 2) % 4))
         for z in range(8) for x in range(4) for c in range(2) for y in range(4)
     ]
     out_proj_grad = lax.ppermute(piece, ("z", "x", "c", "y"), pairs)

time: 215 us -> 208 us (0.967)
  the two profiles are of different devices: /device:TPU:16 before, /device:TPU:1 now
where the time goes in v4:
time: 208 us; the launch traced here: 207 us
  waiting for transfers between devices  82.2 us (40%)
  starting transfers between devices  81.9 us (39%)
  Pallas kernels  34.2 us (16%)
  local copies, waits for them, and re-layouts  4.01 us (2%)
  other arithmetic  3.88 us (2%)
    ppermute x21, waiting for transfers between devices, shifted(): return lax.ppermute(x, axis, [(i, (i + by) % n) for i in range(n)])  57.5 us
    all_to_all x3, starting transfers between devices, per_device(): lax.all_to_all(v.reshape(64, MAIN, v.shape[1]), SP, split_axis=0, concat_...  32.5 us
    ppermute x21, starting transfers between devices, shifted(): return lax.ppermute(x, axis, [(i, (i + by) % n) for i in range(n)])  29.8 us
    pallas_call x5, Pallas kernels, local_call(): pl.pallas_call(kernel, in_specs=[pl.BlockSpec(memory_space=pltpu.SMEM)] +...  23.1 us
    all_to_all x3, waiting for transfers between devices, per_device(): lax.all_to_all(v.reshape(64, MAIN, v.shape[1]), SP, split_axis=0, concat_...  17.6 us
    ppermute x2, starting transfers between devices, from_behind(): lax.ppermute(x, SP, [(i, i + by) for i in range(n) if 0 <= i + by < n])  11.8 us
    all_to_all x1, starting transfers between devices, per_device(): lax.all_to_all(chip.reshape(32, 32, chan), ('z', 'x'), split_axis=0, conc...  5.92 us
    pallas_call x1, Pallas kernels, late(): pl.pallas_call(late_kernel, in_specs=[pl.BlockSpec(memory_space=pltpu.SME...  4.72 us
  transfers between devices with their start and end apart: 28, of which 15 were waited for; matrix products, arithmetic and copies ran while one was open for 2% of the time, Pallas kernels for 10%

profile of v4, /device:TPU:1, one launch (start us, length us, event | category | flops | bytes accessed | tf_op | source)
XLA Modules:
  0.0 207.2 jit_solution(10694068168130194269)
XLA Ops:
  0.6 4.1 %route.1 = (bf16[512,1152]{1,0:T(8,128)(2,1)}, bf16[512,1536]{1,0:T(8,128)(2,1)}, s32[4,256]{1,0:T(4,128)}) custom-call(s32[1]{0:T(128)} %bitcast.tp_ref, s32[2,256]{1,0:T(2,128)} %bitcast.43, f32[2,256]{1,0:T(2,128)} %bitcast.44, bf16[256,2048]{1,0:T(8,128)(2,1)} %hd_ref.1, bf16[256,2048]{1,0:T(8,128)(2,1)} %c_ref.3, bf16[256,2048]{1,0:T(8,128)(2,1)} %hd_ref.1, ...), custom_call_target="tpu_custom_call" | custom-call | tf_op jit(solution)/shard_map/route/pallas_call | solution.py:91
  4.7 13.1 %all-to-all-start = ((bf16[64,8,1152]{2,1,0:T(8,128)(2,1)}), bf16[64,8,1152]{2,1,0:T(8,128)(2,1)S(1)}, u32[]{:S(2)}, u32[]{:S(2)}) async-start(bf16[64,8,1152]{2,1,0:T(8,128)(2,1)} %bitcast.36), calls=%async_computation | async-start | bytes 2359296 | tf_op jit(solution)/shard_map/all_to_all | solution.py:380
  23.0 4.4 %collective-permute-done.wo_prev = bf16[512,256]{1,0:T(8,128)(2,1)S(1)} collective-permute-done((bf16[512,256]{1,0:T(8,128)(2,1)S(1)}, bf16[512,256]{1,0:T(8,128)(2,1)S(1)}, u32[]{:S(2)}, u32[]{:S(2)}) %collective-permute-start) | collective-permute-done | bytes 262176 | tf_op jit(solution)/shard_map/ppermute | solution.py:34
  28.8 5.4 %collective-permute-done.2.wo_far = bf16[512,256]{1,0:T(8,128)(2,1)} collective-permute-done((bf16[512,256]{1,0:T(8,128)(2,1)S(1)}, bf16[512,256]{1,0:T(8,128)(2,1)}, u32[]{:S(2)}, u32[]{:S(2)}) %collective-permute-start.2) | collective-permute-done | bytes 262176 | tf_op jit(solution)/shard_map/ppermute | solution.py:34
  34.2 14.2 %all-to-all-done = bf16[64,8,1152]{2,1,0:T(8,128)(2,1)S(1)} async-done(((bf16[64,8,1152]{2,1,0:T(8,128)(2,1)}), bf16[64,8,1152]{2,1,0:T(8,128)(2,1)S(1)}, u32[]{:S(2)}, u32[]{:S(2)}) %all-to-all-start) | async-done | bytes 1179680 | tf_op jit(solution)/shard_map/all_to_all | solution.py:380
  48.5 6.6 %all-to-all-start.1 = ((bf16[64,8,1536]{2,1,0:T(8,128)(2,1)}), bf16[64,8,1536]{2,1,0:T(8,128)(2,1)S(1)}, u32[]{:S(2)}, u32[]{:S(2)}) async-start(bf16[64,8,1536]{2,1,0:T(8,128)(2,1)} %bitcast.35), calls=%async_computation.1 | async-start | bytes 3145728 | tf_op jit(solution)/shard_map/all_to_all | solution.py:380
  58.0 25.6 %collective-permute-done.3.prev_ref = bf16[512,1152]{1,0:T(8,128)(2,1)S(1)} collective-permute-done((bf16[512,1152]{1,0:T(8,128)(2,1)S(1)}, bf16[512,1152]{1,0:T(8,128)(2,1)S(1)}, u32[]{:S(2)}, u32[]{:S(2)}) %collective-permute-start.3) | collective-permute-done | bytes 1179680 | tf_op jit(solution)/shard_map/ppermute | solution.py:34
  83.8 2.9 %collective-permute-start.6 = (bf16[256,1152]{1,0:T(8,128)(2,1)S(1)}, bf16[256,1152]{1,0:T(8,128)(2,1)S(1)}, u32[]{:S(2)}, u32[]{:S(2)}) collective-permute-start(bf16[256,1152]{1,0:T(8,128)(2,1)S(1)} %slice.52), channel_id=1, source_target_pairs={{0,3},{1,0},{2,1},{3,2},{4,7},{5,4},{6,5},{7,6},{8,11},{9,8},{10,9... | collective-permute-start | bytes 1769480 | tf_op jit(solution)/shard_map/ppermute | solution.py:34
  86.7 6.6 %shard_map.179 = (f32[512,256]{1,0:T(8,128)}, f32[512,256]{1,0:T(8,128)}, f32[512,256]{1,0:T(8,128)}, f32[512,256]{1,0:T(8,128)}, f32[512,256]{1,0:T(8,128)}, /*index=5*/f32[512,256]{1,0:T(8,128)}) custom-call(s32[1]{0:T(128)} %bitcast.tp_ref, bf16[512,1152]{1,0:T(8,128)(2,1)} %bitcast.25, bf16[512,1152]{1,0:T(8,128)(2,1)} %copy-done.5, ...), custom_call_target="tpu_custom_call" | custom-call | tf_op jit(solution)/shard_map/pallas_call | solution.py:164
  93.3 5.2 %collective-permute-done.5.far_lo_in.far_lo_ref = bf16[256,1152]{1,0:T(8,128)(2,1)S(1)} collective-permute-done((bf16[256,1152]{1,0:T(8,128)(2,1)S(1)}, bf16[256,1152]{1,0:T(8,128)(2,1)S(1)}, u32[]{:S(2)}, u32[]{:S(2)}) %collective-permute-start.5) | collective-permute-done | bytes 589856 | tf_op jit(solution)/shard_map/ppermute | solution.py:34
  99.6 4.7 %late.1 = (bf16[512,768]{1,0:T(8,128)(2,1)S(1)}, bf16[512,1280]{1,0:T(8,128)(2,1)S(1)}, bf16[256,768]{1,0:T(8,128)(2,1)S(1)}, bf16[256,768]{1,0:T(8,128)(2,1)S(1)}) custom-call(s32[1]{0:T(128)} %bitcast.tp_ref, f32[512,256]{1,0:T(8,128)} %get-tuple-element.49.ga_in, f32[512,256]{1,0:T(8,128)} %get-tuple-element.50.ua_in, ...), custom_call_target="tpu_custom_call" | custom-call | tf_op jit(solution)/shard_map/late/pallas_call | solution.py:281
  107.1 3.4 %shard_map.180 = (bf16[256,768]{1,0:T(8,128)(2,1)S(1)}, bf16[256,768]{1,0:T(8,128)(2,1)S(1)}, bf16[256,768]{1,0:T(8,128)(2,1)S(1)}, bf16[256,768]{1,0:T(8,128)(2,1)S(1)}, bf16[512,768]{1,0:T(8,128)(2,1)S(1)}) custom-call(s32[1]{0:T(128)} %bitcast.tp_ref, bf16[512,768]{1,0:T(8,128)(2,1)S(1)} %get-tuple-element.56.da.da_ref, ...), custom_call_target="tpu_custom_call" | custom-call | tf_op jit(solution)/shard_map/pallas_call | solution.py:164
  117.2 9.0 %collective-permute-start.13 = (f32[2,256]{1,0:T(2,128)S(1)}, f32[2,256]{1,0:T(2,128)S(1)}, u32[]{:S(2)}, u32[]{:S(2)}) collective-permute-start(f32[2,256]{1,0:T(2,128)S(1)} %convert_multiply_fusion.5), channel_id=1, source_target_pairs={{0,4},{4,8},{8,12},{12,16},{16,20},{20,24},{24,28},{28,32},{32,36}... | collective-permute-start | bytes 6152 | tf_op jit(solution)/shard_map/ppermute | solution.py:357
  126.3 5.0 %collective-permute-done.8 = bf16[256,768]{1,0:T(8,128)(2,1)S(1)} collective-permute-done((bf16[256,768]{1,0:T(8,128)(2,1)S(1)}, bf16[256,768]{1,0:T(8,128)(2,1)S(1)}, u32[]{:S(2)}, u32[]{:S(2)}) %collective-permute-start.8) | collective-permute-done | bytes 393248 | tf_op jit(solution)/shard_map/ppermute | solution.py:34
  132.6 12.8 %all-to-all-start.2 = ((bf16[64,8,768]{2,1,0:T(8,128)(2,1)}), bf16[64,8,768]{2,1,0:T(8,128)(2,1)S(1)}, u32[]{:S(2)}, u32[]{:S(2)}) async-start(bf16[64,8,768]{2,1,0:T(8,128)(2,1)} %bitcast.10), calls=%async_computation.2 | async-start | bytes 1572864 | tf_op jit(solution)/shard_map/all_to_all | solution.py:380
  151.6 3.1 %collective-permute-done.15 = bf16[256,256]{1,0:T(8,128)(2,1)S(1)} collective-permute-done((bf16[256,256]{1,0:T(8,128)(2,1)S(1)}, bf16[256,256]{1,0:T(8,128)(2,1)S(1)}, u32[]{:S(2)}, u32[]{:S(2)}) %collective-permute-start.15) | collective-permute-done | bytes 131104 | tf_op jit(solution)/shard_map/ppermute | solution.py:34
  156.4 8.5 %shard_map.181 = (bf16[2048,256]{1,0:T(8,128)(2,1)}, bf16[2048,256]{1,0:T(8,128)(2,1)}, bf16[256,2048]{1,0:T(8,128)(2,1)}) custom-call(s32[1]{0:T(128)} %bitcast.tp_ref, bf16[512,1152]{1,0:T(8,128)(2,1)} %bitcast.26, bf16[512,1152]{1,0:T(8,128)(2,1)} %copy-done.5, bf16[512,1152]{1,0:T(8,128)(2,1)} %copy-done.6, bf16[256,1152]{1,0:T(8,128)(2,1)} %copy-done.7, ...), custom_call_target="tpu_custom_call" | custom-call | tf_op jit(solution)/shard_map/pallas_call | solution.py:164
  165.0 3.4 %all-to-all-done.2 = bf16[64,8,768]{2,1,0:T(8,128)(2,1)S(1)} async-done(((bf16[64,8,768]{2,1,0:T(8,128)(2,1)}), bf16[64,8,768]{2,1,0:T(8,128)(2,1)S(1)}, u32[]{:S(2)}, u32[]{:S(2)}) %all-to-all-start.2) | async-done | bytes 786464 | tf_op jit(solution)/shard_map/all_to_all | solution.py:380
  172.8 2.8 %shard_map.182 = bf16[1024,256]{1,0:T(8,128)(2,1)} custom-call(s32[1]{0:T(128)} %bitcast.18.where_ref, bf16[256,512]{1,0:T(8,128)(2,1)} %combine.1.res_ref, bf16[256,512]{1,0:T(8,128)(2,1)S(1)} %collective-permute-done.18.res_o_ref, bf16[256,1024]{1,0:T(8,128)(2,1)} %copy-done.9, bf16[256,1024]{1,0:T(8,128)(2,1)} %copy-done.13), custom_call_target="tpu_custom_call" | custom-call | tf_op jit(solution)/shard_map/pallas_call | solution.py:164
  175.6 5.9 %all-to-all-start.3 = ((bf16[32,32,256]{2,1,0:T(8,128)(2,1)}), bf16[32,32,256]{2,1,0:T(8,128)(2,1)S(1)}, u32[]{:S(2)}, u32[]{:S(2)}) async-start(bf16[32,32,256]{2,1,0:T(8,128)(2,1)} %bitcast.19), calls=%async_computation.3 | async-start | bytes 1048576 | tf_op jit(solution)/shard_map/all_to_all | solution.py:464
  189.5 3.2 %collective-permute-done.21 = bf16[256,256]{1,0:T(8,128)(2,1)S(1)} collective-permute-done((bf16[256,256]{1,0:T(8,128)(2,1)S(1)}, bf16[256,256]{1,0:T(8,128)(2,1)S(1)}, u32[]{:S(2)}, u32[]{:S(2)}) %collective-permute-start.21) | collective-permute-done | bytes 131104 | tf_op jit(solution)/shard_map/ppermute | solution.py:34
  193.4 2.8 %collective-permute-start.23 = (f32[2,256]{1,0:T(2,128)S(1)}, f32[2,256]{1,0:T(2,128)S(1)}, u32[]{:S(2)}, u32[]{:S(2)}) collective-permute-start(f32[2,256]{1,0:T(2,128)S(1)} %slice.58), channel_id=1, source_target_pairs={{4,0},{8,4},{12,8},{16,12},{20,16},{24,20},{28,24},{32,28},{36,32}... | collective-permute-start | bytes 6152 | tf_op jit(solution)/shard_map/ppermute | solution.py:357
  196.2 2.7 %collective-permute-done.23 = f32[2,256]{1,0:T(2,128)S(1)} collective-permute-done((f32[2,256]{1,0:T(2,128)S(1)}, f32[2,256]{1,0:T(2,128)S(1)}, u32[]{:S(2)}, u32[]{:S(2)}) %collective-permute-start.23) | collective-permute-done | bytes 2080 | tf_op jit(solution)/shard_map/ppermute | solution.py:357
  202.2 4.3 %collective-permute-done.19 = f32[32,256]{1,0:T(8,128)S(1)} collective-permute-done((f32[32,256]{1,0:T(8,128)S(1)}, f32[32,256]{1,0:T(8,128)S(1)}, u32[]{:S(2)}, u32[]{:S(2)}) %collective-permute-start.19) | collective-permute-done | bytes 32800 | tf_op jit(solution)/shard_map/ppermute | solution.py:471
  (93 shorter events, 46.2 us)
Async XLA Ops:
  4.7 43.7 %all-to-all-start = ((bf16[64,8,1152]{2,1,0:T(8,128)(2,1)}), bf16[64,8,1152]{2,1,0:T(8,128)(2,1)S(1)}, u32[]{:S(2)}, u32[]{:S(2)}) async-start(bf16[64,8,1152]{2,1,0:T(8,128)(2,1)} %bitcast.36), calls=%async_computation | async-start | bytes 2359296 | tf_op jit(solution)/shard_map/all_to_all | solution.py:380
  18.7 8.7 %collective-permute-start = (bf16[512,256]{1,0:T(8,128)(2,1)S(1)}, bf16[512,256]{1,0:T(8,128)(2,1)S(1)}, u32[]{:S(2)}, u32[]{:S(2)}) collective-permute-start(bf16[512,256]{1,0:T(8,128)(2,1)S(1)} %get-tuple-element.89), channel_id=1, source_target_pairs={{0,1},{1,2},{2,3},{3,0},{4,5},{5,6},{6,7},{7,4},{8,9},{9,10},{10,1... | collective-permute-start | bytes 786440 | tf_op jit(solution)/shard_map/ppermute | solution.py:34
  20.0 7.4 %collective-permute-start.1 = (bf16[512,256]{1,0:T(8,128)(2,1)S(1)}, bf16[512,256]{1,0:T(8,128)(2,1)S(1)}, u32[]{:S(2)}, u32[]{:S(2)}) collective-permute-start(bf16[512,256]{1,0:T(8,128)(2,1)S(1)} %get-tuple-element.91), channel_id=1, source_target_pairs={{0,3},{1,0},{2,1},{3,2},{4,7},{5,4},{6,5},{7,6},{8,11},{9,8},{10,9... | collective-permute-start | bytes 786440 | tf_op jit(solution)/shard_map/ppermute | solution.py:34
  21.4 12.8 %collective-permute-start.2 = (bf16[512,256]{1,0:T(8,128)(2,1)S(1)}, bf16[512,256]{1,0:T(8,128)(2,1)}, u32[]{:S(2)}, u32[]{:S(2)}) collective-permute-start(bf16[512,256]{1,0:T(8,128)(2,1)S(1)} %get-tuple-element.88), channel_id=1, source_target_pairs={{0,2},{1,3},{2,0},{3,1},{4,6},{5,7},{6,4},{7,5},{8,10},{9,11},{10,... | collective-permute-start | bytes 786440 | tf_op jit(solution)/shard_map/ppermute | solution.py:34
  48.5 50.1 %all-to-all-start.1 = ((bf16[64,8,1536]{2,1,0:T(8,128)(2,1)}), bf16[64,8,1536]{2,1,0:T(8,128)(2,1)S(1)}, u32[]{:S(2)}, u32[]{:S(2)}) async-start(bf16[64,8,1536]{2,1,0:T(8,128)(2,1)} %bitcast.35), calls=%async_computation.1 | async-start | bytes 3145728 | tf_op jit(solution)/shard_map/all_to_all | solution.py:380
  55.1 28.5 %collective-permute-start.3 = (bf16[512,1152]{1,0:T(8,128)(2,1)S(1)}, bf16[512,1152]{1,0:T(8,128)(2,1)S(1)}, u32[]{:S(2)}, u32[]{:S(2)}) collective-permute-start(bf16[512,1152]{1,0:T(8,128)(2,1)S(1)} %bitcast.23), channel_id=1, source_target_pairs={{0,1},{1,2},{2,3},{3,0},{4,5},{5,6},{6,7},{7,4},{8,9},{9,10},{10,1... | collective-permute-start | bytes 3538952 | tf_op jit(solution)/shard_map/ppermute | solution.py:34
  56.4 27.3 %collective-permute-start.4 = (bf16[512,1152]{1,0:T(8,128)(2,1)S(1)}, bf16[512,1152]{1,0:T(8,128)(2,1)S(1)}, u32[]{:S(2)}, u32[]{:S(2)}) collective-permute-start(bf16[512,1152]{1,0:T(8,128)(2,1)S(1)} %bitcast.24), channel_id=1, source_target_pairs={{0,3},{1,0},{2,1},{3,2},{4,7},{5,4},{6,5},{7,6},{8,11},{9,8},{10,9... | collective-permute-start | bytes 3538952 | tf_op jit(solution)/shard_map/ppermute | solution.py:34
  83.6 14.9 %collective-permute-start.5 = (bf16[256,1152]{1,0:T(8,128)(2,1)S(1)}, bf16[256,1152]{1,0:T(8,128)(2,1)S(1)}, u32[]{:S(2)}, u32[]{:S(2)}) collective-permute-start(bf16[256,1152]{1,0:T(8,128)(2,1)S(1)} %slice.51), channel_id=1, source_target_pairs={{0,1},{1,2},{2,3},{3,0},{4,5},{5,6},{6,7},{7,4},{8,9},{9,10},{10,1... | collective-permute-start | bytes 1769480 | tf_op jit(solution)/shard_map/ppermute | solution.py:34
  83.8 14.8 %collective-permute-start.6 = (bf16[256,1152]{1,0:T(8,128)(2,1)S(1)}, bf16[256,1152]{1,0:T(8,128)(2,1)S(1)}, u32[]{:S(2)}, u32[]{:S(2)}) collective-permute-start(bf16[256,1152]{1,0:T(8,128)(2,1)S(1)} %slice.52), channel_id=1, source_target_pairs={{0,3},{1,0},{2,1},{3,2},{4,7},{5,4},{6,5},{7,6},{8,11},{9,8},{10,9... | collective-permute-start | bytes 1769480 | tf_op jit(solution)/shard_map/ppermute | solution.py:34
  104.3 9.9 %collective-permute-start.7 = (bf16[256,768]{1,0:T(8,128)(2,1)S(1)}, bf16[256,768]{1,0:T(8,128)(2,1)S(1)}, u32[]{:S(2)}, u32[]{:S(2)}) collective-permute-start(bf16[256,768]{1,0:T(8,128)(2,1)S(1)} %get-tuple-element.60), channel_id=1, source_target_pairs={{0,1},{1,2},{2,3},{3,0},{4,5},{5,6},{6,7},{7,4},{8,9},{9,10},{10,1... | collective-permute-start | bytes 1179656 | tf_op jit(solution)/shard_map/ppermute | solution.py:34
  104.4 10.0 %collective-permute-start.11 = (bf16[256,768]{1,0:T(8,128)(2,1)S(1)}, bf16[256,768]{1,0:T(8,128)(2,1)S(1)}, u32[]{:S(2)}, u32[]{:S(2)}) collective-permute-start(bf16[256,768]{1,0:T(8,128)(2,1)S(1)} %get-tuple-element.64), channel_id=1, source_target_pairs={{0,3},{1,0},{2,1},{3,2},{4,7},{5,4},{6,5},{7,6},{8,11},{9,8},{10,9... | collective-permute-start | bytes 1179656 | tf_op jit(solution)/shard_map/ppermute | solution.py:34
  110.5 15.8 %collective-permute-start.9 = (bf16[256,768]{1,0:T(8,128)(2,1)S(1)}, bf16[256,768]{1,0:T(8,128)(2,1)S(1)}, u32[]{:S(2)}, u32[]{:S(2)}) collective-permute-start(bf16[256,768]{1,0:T(8,128)(2,1)S(1)} %get-tuple-element.61), channel_id=1, source_target_pairs={{0,1},{1,2},{2,3},{3,0},{4,5},{5,6},{6,7},{7,4},{8,9},{9,10},{10,1... | collective-permute-start | bytes 1179656 | tf_op jit(solution)/shard_map/ppermute | solution.py:34
  110.6 15.7 %collective-permute-start.10 = (bf16[256,768]{1,0:T(8,128)(2,1)S(1)}, bf16[256,768]{1,0:T(8,128)(2,1)S(1)}, u32[]{:S(2)}, u32[]{:S(2)}) collective-permute-start(bf16[256,768]{1,0:T(8,128)(2,1)S(1)} %get-tuple-element.62), channel_id=1, source_target_pairs={{0,3},{1,0},{2,1},{3,2},{4,7},{5,4},{6,5},{7,6},{8,11},{9,8},{10,9... | collective-permute-start | bytes 1179656 | tf_op jit(solution)/shard_map/ppermute | solution.py:34
  114.3 17.1 %collective-permute-start.8 = (bf16[256,768]{1,0:T(8,128)(2,1)S(1)}, bf16[256,768]{1,0:T(8,128)(2,1)S(1)}, u32[]{:S(2)}, u32[]{:S(2)}) collective-permute-start(bf16[256,768]{1,0:T(8,128)(2,1)S(1)} %add_convert_fusion.2), channel_id=1, source_target_pairs={{0,1},{1,2},{2,3},{3,0},{4,5},{5,6},{6,7},{7,4},{8,9},{9,10},{10,1... | collective-permute-start | bytes 1179656 | tf_op jit(solution)/shard_map/ppermute | solution.py:34
  114.5 16.9 %collective-permute-start.12 = (bf16[256,768]{1,0:T(8,128)(2,1)S(1)}, bf16[256,768]{1,0:T(8,128)(2,1)S(1)}, u32[]{:S(2)}, u32[]{:S(2)}) collective-permute-start(bf16[256,768]{1,0:T(8,128)(2,1)S(1)} %add_convert_fusion.1), channel_id=1, source_target_pairs={{0,3},{1,0},{2,1},{3,2},{4,7},{5,4},{6,5},{7,6},{8,11},{9,8},{10,9... | collective-permute-start | bytes 1179656 | tf_op jit(solution)/shard_map/ppermute | solution.py:34
  117.2 15.3 %collective-permute-start.13 = (f32[2,256]{1,0:T(2,128)S(1)}, f32[2,256]{1,0:T(2,128)S(1)}, u32[]{:S(2)}, u32[]{:S(2)}) collective-permute-start(f32[2,256]{1,0:T(2,128)S(1)} %convert_multiply_fusion.5), channel_id=1, source_target_pairs={{0,4},{4,8},{8,12},{12,16},{16,20},{20,24},{24,28},{28,32},{32,36}... | collective-permute-start | bytes 6152 | tf_op jit(solution)/shard_map/ppermute | solution.py:357
  132.6 35.8 %all-to-all-start.2 = ((bf16[64,8,768]{2,1,0:T(8,128)(2,1)}), bf16[64,8,768]{2,1,0:T(8,128)(2,1)S(1)}, u32[]{:S(2)}, u32[]{:S(2)}) async-start(bf16[64,8,768]{2,1,0:T(8,128)(2,1)} %bitcast.10), calls=%async_computation.2 | async-start | bytes 1572864 | tf_op jit(solution)/shard_map/all_to_all | solution.py:380
  148.1 6.5 %collective-permute-start.15 = (bf16[256,256]{1,0:T(8,128)(2,1)S(1)}, bf16[256,256]{1,0:T(8,128)(2,1)S(1)}, u32[]{:S(2)}, u32[]{:S(2)}) collective-permute-start(bf16[256,256]{1,0:T(8,128)(2,1)S(1)} %get-tuple-element.86), channel_id=1, source_target_pairs={{0,3},{1,0},{2,1},{3,2},{4,7},{5,4},{6,5},{7,6},{8,11},{9,8},{10,9... | collective-permute-start | bytes 393224 | tf_op jit(solution)/shard_map/ppermute | solution.py:34
  154.8 10.2 %collective-permute-start.17 = (bf16[256,1024]{1,0:T(8,128)(2,1)S(1)}, bf16[256,1024]{1,0:T(8,128)(2,1)S(1)}, u32[]{:S(2)}, u32[]{:S(2)}) collective-permute-start(bf16[256,1024]{1,0:T(8,128)(2,1)S(1)} %pad_maximum_fusion.y_ref), channel_id=1, source_target_pairs={{0,4},{4,0},{1,5},{5,1},{2,6},{6,2},{3,7},{7,3},{8,12},{12,8},{9,1... | collective-permute-start | bytes 1572872 | tf_op jit(solution)/shard_map/ppermute | solution.py:34
  175.6 24.1 %all-to-all-start.3 = ((bf16[32,32,256]{2,1,0:T(8,128)(2,1)}), bf16[32,32,256]{2,1,0:T(8,128)(2,1)S(1)}, u32[]{:S(2)}, u32[]{:S(2)}) async-start(bf16[32,32,256]{2,1,0:T(8,128)(2,1)} %bitcast.19), calls=%async_computation.3 | async-start | bytes 1048576 | tf_op jit(solution)/shard_map/all_to_all | solution.py:464
  183.2 6.2 %collective-permute-start.22 = (bf16[256,256]{1,0:T(8,128)(2,1)S(1)}, bf16[256,256]{1,0:T(8,128)(2,1)S(1)}, u32[]{:S(2)}, u32[]{:S(2)}) collective-permute-start(bf16[256,256]{1,0:T(8,128)(2,1)S(1)} %get-tuple-element.83), channel_id=1, source_target_pairs={{0,2},{1,3},{2,0},{3,1},{4,6},{5,7},{6,4},{7,5},{8,10},{9,11},{10,... | collective-permute-start | bytes 393224 | tf_op jit(solution)/shard_map/ppermute | solution.py:34
  185.4 7.2 %collective-permute-start.21 = (bf16[256,256]{1,0:T(8,128)(2,1)S(1)}, bf16[256,256]{1,0:T(8,128)(2,1)S(1)}, u32[]{:S(2)}, u32[]{:S(2)}) collective-permute-start(bf16[256,256]{1,0:T(8,128)(2,1)S(1)} %get-tuple-element.82), channel_id=1, source_target_pairs={{0,1},{1,2},{2,3},{3,0},{4,5},{5,6},{6,7},{7,4},{8,9},{9,10},{10,1... | collective-permute-start | bytes 393224 | tf_op jit(solution)/shard_map/ppermute | solution.py:34
  186.2 6.4 %collective-permute-start.20 = (bf16[256,256]{1,0:T(8,128)(2,1)S(1)}, bf16[256,256]{1,0:T(8,128)(2,1)S(1)}, u32[]{:S(2)}, u32[]{:S(2)}) collective-permute-start(bf16[256,256]{1,0:T(8,128)(2,1)S(1)} %get-tuple-element.81), channel_id=1, source_target_pairs={{0,3},{1,0},{2,1},{3,2},{4,7},{5,4},{6,5},{7,6},{8,11},{9,8},{10,9... | collective-permute-start | bytes 393224 | tf_op jit(solution)/shard_map/ppermute | solution.py:34
  199.8 6.8 %collective-permute-start.19 = (f32[32,256]{1,0:T(8,128)S(1)}, f32[32,256]{1,0:T(8,128)S(1)}, u32[]{:S(2)}, u32[]{:S(2)}) collective-permute-start(f32[32,256]{1,0:T(8,128)S(1)} %convert_reduce_fusion), channel_id=1, source_target_pairs={{0,2},{1,66},{2,130},{3,194},{4,6},{5,70},{6,134},{7,198},{8,10},{... | collective-permute-start | bytes 98312 | tf_op jit(solution)/shard_map/ppermute | solution.py:471
  (22 other events, 139.1 us)
